TPU v7x, 512 devices: a whole 4x8x8 slice. The times are simulated.
512 devices in a mesh: ep: 128 (over z, y, core), tp: 4 (over x).
Axes of the slice: x: 4, y: 8, z: 8, core: 2. Of those that a mesh axis runs over, the one named last changes fastest.
Arguments:
- tokens: bfloat16 [16384, 2048], P('ep'), may hold values from -24 to 24
- cotangent: bfloat16 [16384, 2048], P('ep'), may hold values from -6 to 6
- routing: int32 [16384, 2], P('ep'), may hold values from 0 to 127, all different within a row; in each aligned block of 128 rows (0 to 127, 128 to 255, ...) at most 4 rows name the same one
- router_weight: bfloat16 [2048, 128], replicated, may hold values from -0.125 to 0.125
- gate_weight: bfloat16 [128, 2048, 512], P('ep', None, 'tp'), may hold values from -0.125 to 0.125
- up_weight: bfloat16 [128, 2048, 512], P('ep', None, 'tp'), may hold values from -0.125 to 0.125
- down_weight: bfloat16 [128, 512, 2048], P('ep', 'tp'), may hold values from -0.25 to 0.25
Outputs:
- grad_tokens: bfloat16 [16384, 2048], P('ep', 'tp')
- grad_gating: float32 [16384, 2], P('ep')
- grad_router: float32 [2048, 128], P('ep')
- grad_gate_weight: bfloat16 [128, 2048, 512], P('ep', None, 'tp')
- grad_up_weight: bfloat16 [128, 2048, 512], P('ep', None, 'tp')
- grad_down_weight: bfloat16 [128, 512, 2048], P('ep', 'tp')
- in_norms: float32 [128, 2, 2048], P('ep')
- down_norms: float32 [128, 512], P('ep', 'tp')
- router_norms: float32 [2048], P('ep')
Inputs may be any that keep to these rules, and one draw needn't show every extreme that they name: `routing`: each row names 2 different experts. Among the rows of one index of ep no expert is named by more than 4 rows, a bound that some block reaches in some of them.
All inputs are finite; a program needn't handle non-finite values.
Results may differ from a plain program's by a relative error of at most 0.014.
Values may be sent and summed in bfloat16 or wider, within the bound.
No kernel may reach another device: no remote copies, remote signals or barrier semaphores. Data moves between devices by JAX's collectives and lax.ppermute only.
A program may use at most 64 MiB of HBM per device.

v0:
```python
import functools

import jax
import jax.numpy as jnp
from jax import lax
from jax.experimental import pallas as pl
from jax.experimental.pallas import tpu as pltpu
from jax.sharding import Mesh
from jax.sharding import PartitionSpec as P


EP = ("ep_0", "ep_1", "ep_2")
F32 = jnp.float32
BF16 = jnp.bfloat16


TOK = 128
D = 2048
EXPERTS = 128
TP = 4
DQ = D // TP
F = 512
FQ = F // TP
SENT = EXPERTS * 8
CH = D // 8


def dot(a, b, ca=1, cb=0):
    return lax.dot_general(a, b, (((ca,), (cb,)), ((), ())), preferred_element_type=F32)


def iota(shape, dim):
    return lax.broadcasted_iota(jnp.int32, shape, dim)


def pieces(x):
    hi = x.astype(BF16).astype(F32)
    rest = x - hi
    mid = rest.astype(BF16).astype(F32)
    return hi, mid, rest - mid


def aligned(x, n):
    return pl.multiple_of(x * n, n)


def spread(u):
    row = iota((SENT, 128), 0)
    return ((row // 8 == iota((SENT, 128), 1)) & (row % 8 == u)).astype(BF16)


def gather(u):
    row = iota((128, SENT), 1)
    return ((row // 8 == iota((128, SENT), 0)) & (row % 8 == u)).astype(BF16)


def every():
    return (iota((SENT, 128), 0) // 8 == iota((SENT, 128), 1)).astype(BF16)


ON_CHIP = pl.BlockSpec(memory_space=pltpu.VMEM)


def call(kernel, scalars, ins, outs, scratch=()):
    arrays = []
    specs = []
    for x in ins:
        if isinstance(x, tuple):
            arrays.append(x[0])
            specs.append(x[1])
        else:
            arrays.append(pltpu.with_memory_space_constraint(x, pltpu.VMEM))
            specs.append(ON_CHIP)
    return pl.pallas_call(
        kernel,
        grid_spec=pltpu.PrefetchScalarGridSpec(
            num_scalar_prefetch=1,
            grid=(1,),
            in_specs=tuple(specs),
            out_specs=(ON_CHIP,) * len(outs),
            scratch_shapes=scratch,
        ),
        out_shape=tuple(outs),
        compiler_params=pltpu.CompilerParams(vmem_limit_bytes=32 << 20),
    )(scalars, *arrays)


def whole(x):
    return (x, pl.BlockSpec(x.shape, lambda g, p: (0,) * x.ndim))


def sds(shape, dtype):
    return jax.ShapeDtypeStruct(shape, dtype)


def hbm(shape, dtype):
    return pltpu.HBM(shape, dtype)


def vmem(shape, dtype):
    return pltpu.VMEM(shape, dtype)


def dispatch_kernel(sc, tok, cot, routing, router, send, hit0, hit1, stats):
    experts = iota((EXPERTS, TOK), 0)
    picked = [(experts == routing[k : k + 1, :]) for k in range(2)]
    both = (picked[0] | picked[1]).astype(F32)
    logits = dot(router[...], tok[...], 0, 1)
    s = [
        jax.nn.sigmoid(jnp.sum(jnp.where(m, logits, 0.0), axis=0, keepdims=True)) for m in picked
    ]
    total = s[0] + s[1]
    g = [v / total for v in s]
    slope = [v * (1.0 - v) / total for v in s]
    before = (iota((TOK, TOK), 0) < iota((TOK, TOK), 1)).astype(BF16)
    within = dot(both.astype(BF16), before)
    mine = within == sc[0].astype(F32)
    line = iota((128, TOK), 0)
    hits = []
    info = None
    for k, out in ((0, hit0), (1, hit1)):
        hit = jnp.where(picked[k] & mine, 1.0, 0.0)
        out[...] = hit.astype(BF16)
        hits.append(hit)
        own = slope[k] * g[1 - k]
        other = slope[1 - k] * g[k]
        columns = [*pieces(g[k]), *pieces(own), *pieces(other), routing[1 - k : 2 - k, :].astype(F32)]
        table = jnp.zeros((128, TOK), F32)
        for c, v in enumerate(columns):
            table = jnp.where(line == c, v, table)
        part = dot(hit.astype(BF16), table.astype(BF16), 1, 1)
        info = part if info is None else info + part
    any_hit = (hits[0] + hits[1]).astype(BF16)
    toks = dot(any_hit, tok[...]).astype(BF16)
    cots = dot(any_hit, cot[...]).astype(BF16)
    rows = None
    for u in range(8):
        at = slice(CH * u, CH * (u + 1))
        part = dot(spread(u), jnp.concatenate([toks[:, at], cots[:, at]], axis=1))
        rows = part if rows is None else rows + part
    send[:, 0 : 2 * CH] = rows.astype(BF16)
    send[:, 2 * CH :] = dot(every(), info.astype(BF16)).astype(BF16)
    stats[...] = jnp.concatenate(
        [s[0], s[1], total, g[0], g[1], total, total, total], axis=0
    )


def pack_kernel(sc, gate, up, down, out):
    out[0:D, :] = gate[...]
    out[D : 2 * D, :] = up[...]
    for c in range(D // 128):
        out[2 * D + 128 * c : 2 * D + 128 * (c + 1), :] = down[:, 128 * c : 128 * (c + 1)]


def rows_kernel(sc, got, tok_r, cot_r, info_r):
    for u in range(8):
        at = slice(CH * u, CH * (u + 1))
        part = dot(gather(u), got[:, 0 : 2 * CH]).astype(BF16)
        tok_r[:, at] = part[:, 0:CH]
        cot_r[:, at] = part[:, CH:]
    info_r[...] = dot(gather(0), got[:, 2 * CH :]).astype(BF16)


def quarter(tok_r, cot_r, info_r, gate, up, down, grads, back, gg_out):
    toks = tok_r[...]
    pre_gate = dot(toks, gate)
    pre_up = dot(toks, up)
    back_raw = dot(cot_r[...], down, 1, 1)
    about = info_r[...].astype(F32)
    gating = about[:, 0:1] + about[:, 1:2] + about[:, 2:3]
    sig = jax.nn.sigmoid(pre_gate)
    activated = pre_gate * sig
    slope = sig * (1.0 + pre_gate * (1.0 - sig))
    hidden = (activated * pre_up).astype(BF16).astype(F32)
    gg_out[...] = jnp.broadcast_to(jnp.sum(hidden * back_raw, axis=1, keepdims=True), (128, 128))
    scaled = gating * back_raw
    g_gate = (scaled * pre_up * slope).astype(BF16)
    g_up = (scaled * activated).astype(BF16)
    grads[:, 0:FQ] = g_gate
    grads[:, FQ : 2 * FQ] = g_up
    grads[:, 2 * FQ :] = (gating * hidden).astype(BF16)
    back[...] = (dot(g_gate, gate, 1, 1) + dot(g_up, up, 1, 1)).astype(BF16)


def beside(x):
    return jnp.concatenate([x[128 * c : 128 * (c + 1), :] for c in range(D // 128)], axis=1)


def own_kernel(sc, tok_r, cot_r, info_r, gate, up, down, *outs):
    quarter(tok_r, cot_r, info_r, gate[...], up[...], down[...], *outs)


def near_kernel(sc, tok_r, cot_r, info_r, w, *outs):
    quarter(tok_r, cot_r, info_r, w[0:D, :], w[D : 2 * D, :], beside(w[2 * D :, :]), *outs)


def far_kernel(sc, tok_r, cot_r, info_r, wa, wb, *outs):
    half = D // 2
    up = jnp.concatenate([wa[D:, :], wb[0:half, :]], axis=0)
    quarter(tok_r, cot_r, info_r, wa[0:D, :], up, beside(wb[half:, :]), *outs)


def emit_kernel(sc, tok_r, info_r, *refs):
    backs, ggs, send = refs[0:4], refs[4:8], refs[8]
    term = backs[0][...].astype(F32)
    gg = ggs[0][...]
    for d in range(1, TP):
        term = term + backs[d][...].astype(F32)
        gg = gg + ggs[d][...]
    term = term.astype(BF16)
    about = info_r[...].astype(F32)
    own = (about[:, 3:4] + about[:, 4:5] + about[:, 5:6]) * gg
    other = (about[:, 6:7] + about[:, 7:8] + about[:, 8:9]) * gg
    other_expert = about[:, 9:10].astype(jnp.int32)
    lane = iota((128, EXPERTS), 1)
    mix = jnp.where(lane == sc[1], own, 0.0) - jnp.where(lane == other_expert, other, 0.0)
    mix_hi = mix.astype(BF16)
    mix_lo = (mix - mix_hi.astype(F32)).astype(BF16)
    router = dot(tok_r[...], jnp.concatenate([mix_hi, mix_lo], axis=1), 0, 0)
    router = (router[:, 0:EXPERTS] + router[:, EXPERTS:]).reshape(128, 2, 8, EXPERTS)
    rows = None
    for u in range(8):
        part = dot(spread(u), term[:, CH * u : CH * (u + 1)])
        rows = part if rows is None else rows + part
    send[:, 0:CH] = rows.astype(BF16)
    for h in range(2):
        send[:, CH + 128 * h : CH + 128 * (h + 1)] = router[:, h].reshape(SENT, EXPERTS).astype(BF16)
    tail = jnp.zeros((128, 128), F32)
    for c, v in enumerate(pieces(gg)):
        tail = jnp.where(lane == c, v, tail)
    send[:, 2 * CH :] = dot(every(), tail.astype(BF16)).astype(BF16)


def share_kernel(sc, tok_r, cot_r, *refs):
    p = sc[0]
    grads, outs = refs[0:4], refs[4:8]
    for d, out in enumerate(outs):
        at = pl.ds(aligned((p + d) % TP, DQ), DQ)
        out[:, 0:DQ] = tok_r[:, at]
        out[:, DQ : 2 * DQ] = cot_r[:, at]
        for r, g in enumerate(grads):
            f = (p + r) % TP
            for c in range(3):
                out[:, pl.ds(aligned(8 + 4 * c + f, FQ), FQ)] = g[:, FQ * c : FQ * (c + 1)]


def row_sums(x):
    n, width = x.shape
    acc = x[:, 0:128]
    for c in range(1, width // 128):
        acc = acc + x[:, 128 * c : 128 * (c + 1)]
    return jnp.concatenate(
        [jnp.sum(acc[128 * c : 128 * (c + 1), :].T, axis=0, keepdims=True) for c in range(n // 128)],
        axis=0,
    )


def sums_kernel(sc, *refs):
    p = sc[0]
    shared, outs = refs[0:4], refs[4:]
    toks = jnp.concatenate([t[:, 0:DQ] for t in shared], axis=0).T
    cots = jnp.concatenate([t[:, DQ : 2 * DQ] for t in shared], axis=0)
    acc_gate = jnp.zeros((DQ, FQ), F32)
    acc_up = jnp.zeros((DQ, FQ), F32)
    for d, out in enumerate(outs):
        f = (p + d) % TP
        at = [pl.ds(aligned(8 + 4 * c + f, FQ), FQ) for c in range(3)]
        gate_sum = dot(toks, jnp.concatenate([g[:, at[0]] for g in shared], axis=0))
        up_sum = dot(toks, jnp.concatenate([g[:, at[1]] for g in shared], axis=0))
        down_sum = dot(jnp.concatenate([g[:, at[2]] for g in shared], axis=0), cots, 0, 0)
        acc_gate = acc_gate + gate_sum * gate_sum
        acc_up = acc_up + up_sum * up_sum
        out[0:DQ, :] = gate_sum.astype(BF16)
        out[DQ : 2 * DQ, :] = up_sum.astype(BF16)
        for c in range(4):
            out[2 * DQ + 128 * c : 2 * DQ + 128 * (c + 1), :] = down_sum[
                :, 128 * c : 128 * (c + 1)
            ].astype(BF16)
        hi, mid, lo = pieces(row_sums(down_sum * down_sum))
        line = iota((8, 128), 0)
        last = jnp.where(line == 0, hi, jnp.where(line == 1, mid, jnp.where(line == 2, lo, 0.0)))
        out[3 * DQ + 24 : 3 * DQ + 32, :] = last.astype(BF16)
    both = jnp.concatenate([row_sums(acc_gate), row_sums(acc_up)], axis=0)
    norms = jnp.concatenate(pieces(both), axis=0).astype(BF16)
    for out in outs:
        out[3 * DQ : 3 * DQ + 24, :] = norms


def home_kernel(sc, got, hit0, hit1, out):
    hits = [hit0[...], hit1[...]]
    both = (hits[0].astype(F32) + hits[1].astype(F32)).astype(BF16)
    terms = jnp.concatenate(
        [dot(gather(u), got[:, 0:CH]).astype(BF16) for u in range(8)], axis=1
    )
    summed = dot(both, terms, 0, 0).astype(BF16)
    tail = dot(gather(0), got[:, 2 * CH :]).astype(BF16)
    pick = (iota((8, SENT), 0) == iota((8, SENT), 1) % 8).astype(BF16)
    router = dot(pick, got[:, CH : 2 * CH])
    hi, mid, lo = pieces(router)
    lines = [jnp.concatenate([hi, mid + lo], axis=1)]
    flat = []
    for hit in hits:
        flat.append(dot(tail, hit, 0, 0)[0:4, :])
    flat = jnp.concatenate(flat, axis=0)
    lines.append(jnp.concatenate([flat] * 4, axis=1))
    extra = jnp.concatenate(lines, axis=0).astype(BF16)
    for q in range(TP):
        out[q, 0:TOK, :] = summed[:, DQ * q : DQ * (q + 1)]
        out[q, TOK:, :] = extra


def last_kernel(sc, got, stats, routing, router, grad_tokens, grad_gating, grad_router, norms):
    total = got[0].astype(F32)
    for q in range(1, TP):
        total = total + got[q].astype(F32)
    extra = total[TOK:, :]
    rows = [
        extra[8 + 4 * k : 9 + 4 * k, 0:128]
        + extra[9 + 4 * k : 10 + 4 * k, 0:128]
        + extra[10 + 4 * k : 11 + 4 * k, 0:128]
        for k in range(2)
    ]
    grad_gating[...] = jnp.concatenate(rows, axis=0)
    st = stats[...]
    score_sum = st[2:3, :]
    weighted = st[3:4, :] * rows[0] + st[4:5, :] * rows[1]
    experts = iota((EXPERTS, TOK), 0)
    logits = jnp.zeros((EXPERTS, TOK), F32)
    for k in range(2):
        s = st[k : k + 1, :]
        chosen = (rows[k] - weighted) / score_sum * s * (1.0 - s)
        logits = jnp.where(experts == routing[k : k + 1, :], chosen, logits)
    term = dot(logits.astype(BF16), router[...], 0, 1)
    grad_tokens[...] = (total[0:TOK, :] + term).astype(BF16)
    sums = extra[0:8, 0:256] + extra[0:8, 256:512]
    x = jnp.concatenate([sums[:, 0:128], sums[:, 128:256]], axis=0)
    grad_router[...] = x
    squares = lax.dot_general(
        jnp.ones((8, EXPERTS), F32),
        x * x,
        (((1,), (1,)), ((), ())),
        precision=lax.Precision.HIGHEST,
        preferred_element_type=F32,
    )
    norms[...] = squares[0:1, :]


def weights_kernel(sc, own, x1, x2, x3, gate, up, down, in_norms, down_norms):
    p = sc[0]
    total = None
    for d, x in enumerate((own, x1, x2, x3)):
        q = (p + TP - d) % TP
        gate[pl.ds(aligned(q, DQ), DQ), :] = x[0:DQ, :]
        up[pl.ds(aligned(q, DQ), DQ), :] = x[DQ : 2 * DQ, :]
        for c in range(4):
            down[:, pl.ds(aligned(q * 4 + c, 128), 128)] = x[
                2 * DQ + 128 * c : 2 * DQ + 128 * (c + 1), :
            ]
        tail = x[3 * DQ : 3 * DQ + 32, :].astype(F32)
        norms = tail[0:8, :] + tail[8:16, :] + tail[16:24, :]
        for c in range(4):
            at = pl.ds(aligned(q * 4 + c, 128), 128)
            in_norms[0:1, at] = norms[c : c + 1, :]
            in_norms[1:2, at] = norms[4 + c : 5 + c, :]
        part = tail[24:25, :] + tail[25:26, :] + tail[26:27, :]
        total = part if total is None else total + part
    down_norms[...] = total


def layer(tokens, cotangent, routing, router_weight, gate_weight, up_weight, down_weight):
    tp_index = lax.axis_index("tp")
    ep_index = lax.axis_index(EP)
    sc = jnp.stack([tp_index, ep_index]).astype(jnp.int32)
    routing_t = routing.T
    gate_w = gate_weight[0]
    up_w = up_weight[0]
    down_w = down_weight[0]
    far = functools.partial(pltpu.with_memory_space_constraint, memory_space=pltpu.HBM)

    def shift(x, d):
        return lax.ppermute(x, "tp", [(a, (a + d) % TP) for a in range(TP)])

    (packed,) = call(
        pack_kernel,
        sc,
        (whole(far(gate_w)), whole(far(up_w)), whole(far(down_w))),
        (hbm((6 * D // 2, FQ), BF16),),
    )
    from_below = shift(packed, 1)
    from_above = shift(packed, 3)
    far_a = shift(from_below[0 : 3 * D // 2], 1)
    far_b = shift(from_above[3 * D // 2 :], 3)

    send, hit0, hit1, stats = call(
        dispatch_kernel,
        sc,
        (whole(far(tokens)), whole(far(cotangent)), whole(far(routing_t)), whole(far(router_weight))),
        (
            hbm((SENT, 2 * CH + 128), BF16),
            hbm((EXPERTS, TOK), BF16),
            hbm((EXPERTS, TOK), BF16),
            hbm((8, TOK), F32),
        ),
    )
    got = lax.all_to_all(send.reshape(EXPERTS, 8, 2 * CH + 128), EP, 0, 0, tiled=True)
    rows = call(
        rows_kernel,
        sc,
        (got.reshape(SENT, 2 * CH + 128),),
        (sds((128, D), BF16), sds((128, D), BF16), sds((128, 128), BF16)),
    )
    results = (sds((128, 3 * FQ), BF16), sds((128, D), BF16), sds((128, 128), F32))
    inputs = tuple(map(whole, rows))
    quarters = [
        call(own_kernel, sc, (*inputs, whole(gate_w), whole(up_w), whole(down_w)), results),
        call(near_kernel, sc, (*inputs, whole(from_above)), results),
        call(far_kernel, sc, (*inputs, whole(far_a), whole(far_b)), results),
        call(near_kernel, sc, (*inputs, whole(from_below)), results),
    ]
    grads, backs, ggs = zip(*quarters)
    (send_back,) = call(
        emit_kernel,
        sc,
        (inputs[0], inputs[2], *map(whole, backs), *map(whole, ggs)),
        (hbm((SENT, 2 * CH + 128), BF16),),
    )
    home = lax.all_to_all(send_back.reshape(EXPERTS, 8, 2 * CH + 128), EP, 0, 0, tiled=True)
    home = home.reshape(SENT, 2 * CH + 128)
    shared = call(
        share_kernel,
        sc,
        (*inputs[0:2], *map(whole, grads)),
        (hbm((128, 2 * DQ + 3 * F), BF16),) * 4,
    )
    shared = [shared[0]] + [shift(t, d) for d, t in enumerate(shared[1:], 1)]
    blocks = call(sums_kernel, sc, tuple(map(whole, shared)), (hbm((3 * DQ + 32, 128), BF16),) * 4)
    x = [shift(b, d) for d, b in enumerate(blocks[1:], 1)]
    grad_gate, grad_up, grad_down, in_norms, down_norms = call(
        weights_kernel,
        sc,
        (whole(far(blocks[0])), *map(whole, x)),
        (
            sds((D, FQ), BF16),
            sds((D, FQ), BF16),
            sds((FQ, D), BF16),
            sds((2, D), F32),
            sds((1, FQ), F32),
        ),
    )
    (parts,) = call(
        home_kernel, sc, (home, whole(hit0), whole(hit1)), (vmem((TP, TOK + 16, DQ), BF16),)
    )
    parts = lax.all_to_all(parts, "tp", 0, 0, tiled=True)
    grad_tokens, grad_gating, grad_router, router_norms = call(
        last_kernel,
        sc,
        (
            parts,
            whole(stats),
            whole(routing_t),
            (router_weight, pl.BlockSpec((DQ, 128), lambda g, p: (p[0], 0))),
        ),
        (sds((TOK, DQ), BF16), sds((2, TOK), F32), sds((16, EXPERTS), F32), sds((1, 16), F32)),
    )
    return (
        grad_tokens,
        grad_gating.T,
        grad_router,
        grad_gate[None],
        grad_up[None],
        grad_down[None],
        in_norms[None],
        down_norms,
        router_norms[0],
    )


def solution(mesh):
    split = Mesh(mesh.devices.reshape(8, 8, 2, TP), ("ep_0", "ep_1", "ep_2", "tp"))
    in_specs = (
        P(EP, None),
        P(EP, None),
        P(EP, None),
        P(),
        P(EP, None, "tp"),
        P(EP, None, "tp"),
        P(EP, "tp", None),
    )
    out_specs = (
        P(EP, "tp"),
        P(EP, None),
        P(EP, None),
        P(EP, None, "tp"),
        P(EP, None, "tp"),
        P(EP, "tp", None),
        P(EP, None, None),
        P(EP, "tp"),
        P(EP),
    )
    return jax.shard_map(layer, mesh=split, in_specs=in_specs, out_specs=out_specs, check_vma=False)
```

profile of v0, /device:TPU:11, one launch (start us, length us, event | category | flops | bytes accessed | tf_op | source)
XLA Modules:
  0.0 193.5 jit_solution(9163072190616338149)
XLA Ops:
  0.7 6.2 %shard_map.142 = (bf16[1024,640]{1,0:T(8,128)(2,1)}, bf16[128,128]{1,0:T(8,128)(2,1)}, bf16[128,128]{1,0:T(8,128)(2,1)}, f32[8,128]{1,0:T(8,128)}) custom-call(s32[2]{0:T(128)S(1)} %pad_add_fusion.sc, bf16[128,2048]{1,0:T(8,128)(2,1)} %tok.1, bf16[128,2048]{1,0:T(8,128)(2,1)} %cot.1, s32[2,128]{1,0:T(2,128)} %bitcast.24, bf16[2048,128]{1,0:T(8,128)(2,1)} %router.3), custom_call_target="tpu_custom_call" | custom-call | tf_op jit(solution)/shard_map/pallas_call | solution.py:74
  7.0 17.6 %all-to-all-start = ((bf16[128,8,640]{2,1,0:T(8,128)(2,1)}), bf16[128,8,640]{2,1,0:T(8,128)(2,1)S(1)}, u32[]{:S(2)}, u32[]{:S(2)}) async-start(bf16[128,8,640]{2,1,0:T(8,128)(2,1)} %bitcast.27), calls=%async_computation | async-start | bytes 2621440 | tf_op jit(solution)/shard_map/all_to_all | solution.py:405
  24.6 3.2 %shard_map.145 = bf16[6144,128]{1,0:T(8,128)(2,1)} custom-call(s32[2]{0:T(128)S(1)} %pad_add_fusion.sc, bf16[2048,128]{1,0:T(8,128)(2,1)} %bitcast.18, bf16[2048,128]{1,0:T(8,128)(2,1)} %bitcast.20, bf16[128,2048]{1,0:T(8,128)(2,1)} %bitcast.22), custom_call_target="tpu_custom_call" | custom-call | tf_op jit(solution)/shard_map/pallas_call | solution.py:74
  27.8 3.1 %collective-permute-start.1 = (bf16[6144,128]{1,0:T(8,128)(2,1)}, bf16[6144,128]{1,0:T(8,128)(2,1)S(1)}, u32[]{:S(2)}, u32[]{:S(2)}) collective-permute-start(bf16[6144,128]{1,0:T(8,128)(2,1)} %shard_map.145), channel_id=1, source_target_pairs={{0,1},{1,2},{2,3},{3,0},{4,5},{5,6},{6,7},{7,4},{8,9},{9,10},{10,1... | collective-permute-start | bytes 4718600 | tf_op jit(solution)/shard_map/ppermute | solution.py:381
  30.9 2.2 %collective-permute-start = (bf16[6144,128]{1,0:T(8,128)(2,1)}, bf16[6144,128]{1,0:T(8,128)(2,1)S(1)}, u32[]{:S(2)}, u32[]{:S(2)}) collective-permute-start(bf16[6144,128]{1,0:T(8,128)(2,1)} %shard_map.145), channel_id=1, source_target_pairs={{0,3},{1,0},{2,1},{3,2},{4,7},{5,4},{6,5},{7,6},{8,11},{9,8},{10,9... | collective-permute-start | bytes 4718600 | tf_op jit(solution)/shard_map/ppermute | solution.py:381
  33.1 32.4 %collective-permute-done.1.w = bf16[6144,128]{1,0:T(8,128)(2,1)S(1)} collective-permute-done((bf16[6144,128]{1,0:T(8,128)(2,1)}, bf16[6144,128]{1,0:T(8,128)(2,1)S(1)}, u32[]{:S(2)}, u32[]{:S(2)}) %collective-permute-start.1) | collective-permute-done | bytes 1572896 | tf_op jit(solution)/shard_map/ppermute | solution.py:381
  66.5 3.2 %collective-permute-start.2 = (bf16[3072,128]{1,0:T(8,128)(2,1)}, bf16[3072,128]{1,0:T(8,128)(2,1)}, u32[]{:S(2)}, u32[]{:S(2)}) collective-permute-start(bf16[3072,128]{1,0:T(8,128)(2,1)} %slice.8), channel_id=1, source_target_pairs={{0,1},{1,2},{2,3},{3,0},{4,5},{5,6},{6,7},{7,4},{8,9},{9,10},{10,1... | collective-permute-start | bytes 2359304 | tf_op jit(solution)/shard_map/ppermute | solution.py:381
  71.2 2.3 %collective-permute-start.3 = (bf16[3072,128]{1,0:T(8,128)(2,1)}, bf16[3072,128]{1,0:T(8,128)(2,1)}, u32[]{:S(2)}, u32[]{:S(2)}) collective-permute-start(bf16[3072,128]{1,0:T(8,128)(2,1)} %slice.9), channel_id=1, source_target_pairs={{0,3},{1,0},{2,1},{3,2},{4,7},{5,4},{6,5},{7,6},{8,11},{9,8},{10,9... | collective-permute-start | bytes 2359304 | tf_op jit(solution)/shard_map/ppermute | solution.py:381
  73.6 1.9 shard_map.143
  76.5 2.0 %shard_map.144 = (bf16[128,384]{1,0:T(8,128)(2,1)S(1)}, bf16[128,2048]{1,0:T(8,128)(2,1)S(1)}, f32[128,128]{1,0:T(8,128)S(1)}) custom-call(s32[2]{0:T(128)S(1)} %pad_add_fusion.sc, bf16[128,2048]{1,0:T(8,128)(2,1)S(1)} %get-tuple-element.46.tok_r, bf16[128,2048]{1,0:T(8,128)(2,1)S(1)} %get-tuple-element.48.cot_r, ...), custom_call_target="tpu_custom_call" | custom-call | tf_op jit(solution)/shard_map/pallas_call | solution.py:74
  78.5 2.0 %shard_map.148 = (bf16[128,384]{1,0:T(8,128)(2,1)S(1)}, bf16[128,2048]{1,0:T(8,128)(2,1)S(1)}, f32[128,128]{1,0:T(8,128)S(1)}) custom-call(s32[2]{0:T(128)S(1)} %pad_add_fusion.sc, bf16[128,2048]{1,0:T(8,128)(2,1)S(1)} %get-tuple-element.46.tok_r, bf16[128,2048]{1,0:T(8,128)(2,1)S(1)} %get-tuple-element.48.cot_r, ...), custom_call_target="tpu_custom_call" | custom-call | tf_op jit(solution)/shard_map/pallas_call | solution.py:74
  80.5 2.0 %shard_map.146 = (bf16[128,384]{1,0:T(8,128)(2,1)S(1)}, bf16[128,2048]{1,0:T(8,128)(2,1)S(1)}, f32[128,128]{1,0:T(8,128)S(1)}) custom-call(s32[2]{0:T(128)S(1)} %pad_add_fusion.sc, bf16[128,2048]{1,0:T(8,128)(2,1)S(1)} %get-tuple-element.46.tok_r, bf16[128,2048]{1,0:T(8,128)(2,1)S(1)} %get-tuple-element.48.cot_r, ...), custom_call_target="tpu_custom_call" | custom-call | tf_op jit(solution)/shard_map/pallas_call | solution.py:74
  82.5 4.2 %collective-permute-done.2.wa = bf16[3072,128]{1,0:T(8,128)(2,1)} collective-permute-done((bf16[3072,128]{1,0:T(8,128)(2,1)}, bf16[3072,128]{1,0:T(8,128)(2,1)}, u32[]{:S(2)}, u32[]{:S(2)}) %collective-permute-start.2) | collective-permute-done | bytes 786464 | tf_op jit(solution)/shard_map/ppermute | solution.py:381
  86.7 4.2 %collective-permute-done.3.wb = bf16[3072,128]{1,0:T(8,128)(2,1)} collective-permute-done((bf16[3072,128]{1,0:T(8,128)(2,1)}, bf16[3072,128]{1,0:T(8,128)(2,1)}, u32[]{:S(2)}, u32[]{:S(2)}) %collective-permute-start.3) | collective-permute-done | bytes 786464 | tf_op jit(solution)/shard_map/ppermute | solution.py:381
  91.0 3.4 %shard_map.147 = (bf16[128,384]{1,0:T(8,128)(2,1)S(1)}, bf16[128,2048]{1,0:T(8,128)(2,1)S(1)}, f32[128,128]{1,0:T(8,128)S(1)}) custom-call(s32[2]{0:T(128)S(1)} %pad_add_fusion.sc, bf16[128,2048]{1,0:T(8,128)(2,1)S(1)} %get-tuple-element.46.tok_r, bf16[128,2048]{1,0:T(8,128)(2,1)S(1)} %get-tuple-element.48.cot_r, ...), custom_call_target="tpu_custom_call" | custom-call | tf_op jit(solution)/shard_map/pallas_call | solution.py:74
  94.3 3.4 %shard_map.149 = bf16[1024,640]{1,0:T(8,128)(2,1)} custom-call(s32[2]{0:T(128)S(1)} %pad_add_fusion.sc, bf16[128,2048]{1,0:T(8,128)(2,1)S(1)} %get-tuple-element.46.tok_r, bf16[128,128]{1,0:T(8,128)(2,1)S(1)} %get-tuple-element.47.info_r, bf16[128,2048]{1,0:T(8,128)(2,1)S(1)} %get-tuple-element.49.refs_0_, bf16[128,2048]{1,0:T(8,128)(2,1)S(1)} %get-tuple-element.50.refs_1_, ...), custom_call_target="tpu_custom_call" | custom-call | tf_op jit(solution)/shard_map/pallas_call | solution.py:74
  97.7 15.7 %all-to-all-start.1 = ((bf16[128,8,640]{2,1,0:T(8,128)(2,1)}), bf16[128,8,640]{2,1,0:T(8,128)(2,1)S(1)}, u32[]{:S(2)}, u32[]{:S(2)}) async-start(bf16[128,8,640]{2,1,0:T(8,128)(2,1)} %bitcast.26), calls=%async_computation.1 | async-start | bytes 2621440 | tf_op jit(solution)/shard_map/all_to_all | solution.py:427
  113.5 2.4 %shard_map.152 = (bf16[128,2560]{1,0:T(8,128)(2,1)}, bf16[128,2560]{1,0:T(8,128)(2,1)}, bf16[128,2560]{1,0:T(8,128)(2,1)}, bf16[128,2560]{1,0:T(8,128)(2,1)}) custom-call(s32[2]{0:T(128)S(1)} %pad_add_fusion.sc, bf16[128,2048]{1,0:T(8,128)(2,1)S(1)} %get-tuple-element.46.tok_r, bf16[128,2048]{1,0:T(8,128)(2,1)S(1)} %get-tuple-element.48.cot_r, ...), custom_call_target="tpu_custom_call" | custom-call | tf_op jit(solution)/shard_map/pallas_call | solution.py:74
  115.8 2.8 %collective-permute-start.4 = (bf16[128,2560]{1,0:T(8,128)(2,1)}, bf16[128,2560]{1,0:T(8,128)(2,1)}, u32[]{:S(2)}, u32[]{:S(2)}) collective-permute-start(bf16[128,2560]{1,0:T(8,128)(2,1)} %get-tuple-element.68), channel_id=1, source_target_pairs={{0,1},{1,2},{2,3},{3,0},{4,5},{5,6},{6,7},{7,4},{8,9},{9,10},{10,1... | collective-permute-start | bytes 1966088 | tf_op jit(solution)/shard_map/ppermute | solution.py:381
  118.7 4.3 %collective-permute-start.5 = (bf16[128,2560]{1,0:T(8,128)(2,1)}, bf16[128,2560]{1,0:T(8,128)(2,1)}, u32[]{:S(2)}, u32[]{:S(2)}) collective-permute-start(bf16[128,2560]{1,0:T(8,128)(2,1)} %get-tuple-element.69), channel_id=1, source_target_pairs={{0,2},{1,3},{2,0},{3,1},{4,6},{5,7},{6,4},{7,5},{8,10},{9,11},{10,... | collective-permute-start | bytes 1966088 | tf_op jit(solution)/shard_map/ppermute | solution.py:381
  122.9 4.0 %collective-permute-start.6 = (bf16[128,2560]{1,0:T(8,128)(2,1)}, bf16[128,2560]{1,0:T(8,128)(2,1)}, u32[]{:S(2)}, u32[]{:S(2)}) collective-permute-start(bf16[128,2560]{1,0:T(8,128)(2,1)} %get-tuple-element.70), channel_id=1, source_target_pairs={{0,3},{1,0},{2,1},{3,2},{4,7},{5,4},{6,5},{7,6},{8,11},{9,8},{10,9... | collective-permute-start | bytes 1966088 | tf_op jit(solution)/shard_map/ppermute | solution.py:381
  126.9 22.8 %all-to-all-done.1 = bf16[128,8,640]{2,1,0:T(8,128)(2,1)S(1)} async-done(((bf16[128,8,640]{2,1,0:T(8,128)(2,1)}), bf16[128,8,640]{2,1,0:T(8,128)(2,1)S(1)}, u32[]{:S(2)}, u32[]{:S(2)}) %all-to-all-start.1) | async-done | bytes 1310752 | tf_op jit(solution)/shard_map/all_to_all | solution.py:427
  149.7 2.5 %shard_map.150 = bf16[4,144,512]{2,1,0:T(8,128)(2,1)} custom-call(s32[2]{0:T(128)S(1)} %pad_add_fusion.sc, bf16[1024,640]{1,0:T(8,128)(2,1)S(1)} %bitcast.17, bf16[128,128]{1,0:T(8,128)(2,1)S(1)} %copy-done.9, bf16[128,128]{1,0:T(8,128)(2,1)S(1)} %copy-done.10), custom_call_target="tpu_custom_call" | custom-call | tf_op jit(solution)/shard_map/pallas_call | solution.py:74
  152.2 5.4 %all-to-all-start.2 = ((bf16[4,144,512]{2,1,0:T(8,128)(2,1)}), bf16[4,144,512]{2,1,0:T(8,128)(2,1)S(1)}, u32[]{:S(2)}, u32[]{:S(2)}) async-start(bf16[4,144,512]{2,1,0:T(8,128)(2,1)} %shard_map.150), calls=%async_computation.2 | async-start | bytes 1179648 | tf_op jit(solution)/shard_map/all_to_all | solution.py:453
  157.6 4.9 %shard_map.153 = (bf16[1568,128]{1,0:T(8,128)(2,1)}, bf16[1568,128]{1,0:T(8,128)(2,1)}, bf16[1568,128]{1,0:T(8,128)(2,1)}, bf16[1568,128]{1,0:T(8,128)(2,1)}) custom-call(s32[2]{0:T(128)S(1)} %pad_add_fusion.sc, bf16[128,2560]{1,0:T(8,128)(2,1)S(1)} %copy-done.8, bf16[128,2560]{1,0:T(8,128)(2,1)} %collective-permute-done.4.refs_1_, ...), custom_call_target="tpu_custom_call" | custom-call | tf_op jit(solution)/shard_map/pallas_call | solution.py:74
  162.5 3.2 %collective-permute-start.7 = (bf16[1568,128]{1,0:T(8,128)(2,1)}, bf16[1568,128]{1,0:T(8,128)(2,1)S(1)}, u32[]{:S(2)}, u32[]{:S(2)}) collective-permute-start(bf16[1568,128]{1,0:T(8,128)(2,1)} %get-tuple-element.72), channel_id=1, source_target_pairs={{0,1},{1,2},{2,3},{3,0},{4,5},{5,6},{6,7},{7,4},{8,9},{9,10},{10,1... | collective-permute-start | bytes 1204232 | tf_op jit(solution)/shard_map/ppermute | solution.py:381
  165.8 2.5 %collective-permute-start.8 = (bf16[1568,128]{1,0:T(8,128)(2,1)}, bf16[1568,128]{1,0:T(8,128)(2,1)S(1)}, u32[]{:S(2)}, u32[]{:S(2)}) collective-permute-start(bf16[1568,128]{1,0:T(8,128)(2,1)} %get-tuple-element.73), channel_id=1, source_target_pairs={{0,2},{1,3},{2,0},{3,1},{4,6},{5,7},{6,4},{7,5},{8,10},{9,11},{10,... | collective-permute-start | bytes 1204232 | tf_op jit(solution)/shard_map/ppermute | solution.py:381
  168.3 4.0 %collective-permute-start.9 = (bf16[1568,128]{1,0:T(8,128)(2,1)}, bf16[1568,128]{1,0:T(8,128)(2,1)S(1)}, u32[]{:S(2)}, u32[]{:S(2)}) collective-permute-start(bf16[1568,128]{1,0:T(8,128)(2,1)} %get-tuple-element.74), channel_id=1, source_target_pairs={{0,3},{1,0},{2,1},{3,2},{4,7},{5,4},{6,5},{7,6},{8,11},{9,8},{10,9... | collective-permute-start | bytes 1204232 | tf_op jit(solution)/shard_map/ppermute | solution.py:381
  172.3 1.7 collective-permute-done.7.x1
  173.9 4.4 %collective-permute-done.8.x2 = bf16[1568,128]{1,0:T(8,128)(2,1)S(1)} collective-permute-done((bf16[1568,128]{1,0:T(8,128)(2,1)}, bf16[1568,128]{1,0:T(8,128)(2,1)S(1)}, u32[]{:S(2)}, u32[]{:S(2)}) %collective-permute-start.8) | collective-permute-done | bytes 401440 | tf_op jit(solution)/shard_map/ppermute | solution.py:381
  178.3 10.9 %collective-permute-done.9.x3 = bf16[1568,128]{1,0:T(8,128)(2,1)S(1)} collective-permute-done((bf16[1568,128]{1,0:T(8,128)(2,1)}, bf16[1568,128]{1,0:T(8,128)(2,1)S(1)}, u32[]{:S(2)}, u32[]{:S(2)}) %collective-permute-start.9) | collective-permute-done | bytes 401440 | tf_op jit(solution)/shard_map/ppermute | solution.py:381
  189.2 2.9 %shard_map.154 = (bf16[2048,128]{1,0:T(8,128)(2,1)}, bf16[2048,128]{1,0:T(8,128)(2,1)}, bf16[128,2048]{1,0:T(8,128)(2,1)}, f32[2,2048]{1,0:T(2,128)}, f32[1,128]{1,0:T(1,128)}) custom-call(s32[2]{0:T(128)S(1)} %pad_add_fusion.sc, bf16[1568,128]{1,0:T(8,128)(2,1)} %get-tuple-element.71.own, bf16[1568,128]{1,0:T(8,128)(2,1)S(1)} %collective-permute-done.7.x1, ...), custom_call_target="tpu_custom_call" | custom-call | tf_op jit(solution)/shard_map/pallas_call | solution.py:74
  (36 shorter events, 5.0 us)
Async XLA Ops:
  7.0 66.6 %all-to-all-start = ((bf16[128,8,640]{2,1,0:T(8,128)(2,1)}), bf16[128,8,640]{2,1,0:T(8,128)(2,1)S(1)}, u32[]{:S(2)}, u32[]{:S(2)}) async-start(bf16[128,8,640]{2,1,0:T(8,128)(2,1)} %bitcast.27), calls=%async_computation | async-start | bytes 2621440 | tf_op jit(solution)/shard_map/all_to_all | solution.py:405
  27.8 37.7 %collective-permute-start.1 = (bf16[6144,128]{1,0:T(8,128)(2,1)}, bf16[6144,128]{1,0:T(8,128)(2,1)S(1)}, u32[]{:S(2)}, u32[]{:S(2)}) collective-permute-start(bf16[6144,128]{1,0:T(8,128)(2,1)} %shard_map.145), channel_id=1, source_target_pairs={{0,1},{1,2},{2,3},{3,0},{4,5},{5,6},{6,7},{7,4},{8,9},{9,10},{10,1... | collective-permute-start | bytes 4718600 | tf_op jit(solution)/shard_map/ppermute | solution.py:381
  30.9 38.8 %collective-permute-start = (bf16[6144,128]{1,0:T(8,128)(2,1)}, bf16[6144,128]{1,0:T(8,128)(2,1)S(1)}, u32[]{:S(2)}, u32[]{:S(2)}) collective-permute-start(bf16[6144,128]{1,0:T(8,128)(2,1)} %shard_map.145), channel_id=1, source_target_pairs={{0,3},{1,0},{2,1},{3,2},{4,7},{5,4},{6,5},{7,6},{8,11},{9,8},{10,9... | collective-permute-start | bytes 4718600 | tf_op jit(solution)/shard_map/ppermute | solution.py:381
  65.5 5.3 %copy-start.2 = (bf16[6144,128]{1,0:T(8,128)(2,1)}, bf16[6144,128]{1,0:T(8,128)(2,1)S(1)}, u32[]{:S(2)}) copy-start(bf16[6144,128]{1,0:T(8,128)(2,1)S(1)} %collective-permute-done.1.w) | copy-start | bytes 4718596
  66.5 8.9 %copy-start.5 = (bf16[1,2048,128]{2,1,0:T(8,128)(2,1)S(1)}, bf16[1,2048,128]{2,1,0:T(8,128)(2,1)}, u32[]{:S(2)}) copy-start(bf16[1,2048,128]{2,1,0:T(8,128)(2,1)} %param.11) | copy-start | bytes 1572868
  66.5 8.9 %copy-start.6 = (bf16[1,2048,128]{2,1,0:T(8,128)(2,1)S(1)}, bf16[1,2048,128]{2,1,0:T(8,128)(2,1)}, u32[]{:S(2)}) copy-start(bf16[1,2048,128]{2,1,0:T(8,128)(2,1)} %param.12) | copy-start | bytes 1572868
  66.5 20.2 %collective-permute-start.2 = (bf16[3072,128]{1,0:T(8,128)(2,1)}, bf16[3072,128]{1,0:T(8,128)(2,1)}, u32[]{:S(2)}, u32[]{:S(2)}) collective-permute-start(bf16[3072,128]{1,0:T(8,128)(2,1)} %slice.8), channel_id=1, source_target_pairs={{0,1},{1,2},{2,3},{3,0},{4,5},{5,6},{6,7},{7,4},{8,9},{9,10},{10,1... | collective-permute-start | bytes 2359304 | tf_op jit(solution)/shard_map/ppermute | solution.py:381
  69.8 1.4 copy-start
  71.2 19.8 %collective-permute-start.3 = (bf16[3072,128]{1,0:T(8,128)(2,1)}, bf16[3072,128]{1,0:T(8,128)(2,1)}, u32[]{:S(2)}, u32[]{:S(2)}) collective-permute-start(bf16[3072,128]{1,0:T(8,128)(2,1)} %slice.9), channel_id=1, source_target_pairs={{0,3},{1,0},{2,1},{3,2},{4,7},{5,4},{6,5},{7,6},{8,11},{9,8},{10,9... | collective-permute-start | bytes 2359304 | tf_op jit(solution)/shard_map/ppermute | solution.py:381
  75.5 1.0 copy-start.7
  76.5 2.0 %copy-start.3 = (bf16[6144,128]{1,0:T(8,128)(2,1)S(1)}, bf16[6144,128]{1,0:T(8,128)(2,1)}, u32[]{:S(2)}) copy-start(bf16[6144,128]{1,0:T(8,128)(2,1)} %copy-done.2) | copy-start | bytes 4718596
  78.5 2.0 %copy-start.1 = (bf16[6144,128]{1,0:T(8,128)(2,1)S(1)}, bf16[6144,128]{1,0:T(8,128)(2,1)}, u32[]{:S(2)}) copy-start(bf16[6144,128]{1,0:T(8,128)(2,1)} %copy-done) | copy-start | bytes 4718596
  97.7 52.0 %all-to-all-start.1 = ((bf16[128,8,640]{2,1,0:T(8,128)(2,1)}), bf16[128,8,640]{2,1,0:T(8,128)(2,1)S(1)}, u32[]{:S(2)}, u32[]{:S(2)}) async-start(bf16[128,8,640]{2,1,0:T(8,128)(2,1)} %bitcast.26), calls=%async_computation.1 | async-start | bytes 2621440 | tf_op jit(solution)/shard_map/all_to_all | solution.py:427
  113.5 36.3 %copy-start.9 = (bf16[128,128]{1,0:T(8,128)(2,1)S(1)}, bf16[128,128]{1,0:T(8,128)(2,1)}, u32[]{:S(2)}) copy-start(bf16[128,128]{1,0:T(8,128)(2,1)} %get-tuple-element.57.hit0) | copy-start | bytes 98308
  113.5 36.2 %copy-start.10 = (bf16[128,128]{1,0:T(8,128)(2,1)S(1)}, bf16[128,128]{1,0:T(8,128)(2,1)}, u32[]{:S(2)}) copy-start(bf16[128,128]{1,0:T(8,128)(2,1)} %get-tuple-element.58.hit1) | copy-start | bytes 98308
  115.8 41.8 %collective-permute-start.4 = (bf16[128,2560]{1,0:T(8,128)(2,1)}, bf16[128,2560]{1,0:T(8,128)(2,1)}, u32[]{:S(2)}, u32[]{:S(2)}) collective-permute-start(bf16[128,2560]{1,0:T(8,128)(2,1)} %get-tuple-element.68), channel_id=1, source_target_pairs={{0,1},{1,2},{2,3},{3,0},{4,5},{5,6},{6,7},{7,4},{8,9},{9,10},{10,1... | collective-permute-start | bytes 1966088 | tf_op jit(solution)/shard_map/ppermute | solution.py:381
  118.7 39.0 %collective-permute-start.5 = (bf16[128,2560]{1,0:T(8,128)(2,1)}, bf16[128,2560]{1,0:T(8,128)(2,1)}, u32[]{:S(2)}, u32[]{:S(2)}) collective-permute-start(bf16[128,2560]{1,0:T(8,128)(2,1)} %get-tuple-element.69), channel_id=1, source_target_pairs={{0,2},{1,3},{2,0},{3,1},{4,6},{5,7},{6,4},{7,5},{8,10},{9,11},{10,... | collective-permute-start | bytes 1966088 | tf_op jit(solution)/shard_map/ppermute | solution.py:381
  122.9 34.7 %collective-permute-start.6 = (bf16[128,2560]{1,0:T(8,128)(2,1)}, bf16[128,2560]{1,0:T(8,128)(2,1)}, u32[]{:S(2)}, u32[]{:S(2)}) collective-permute-start(bf16[128,2560]{1,0:T(8,128)(2,1)} %get-tuple-element.70), channel_id=1, source_target_pairs={{0,3},{1,0},{2,1},{3,2},{4,7},{5,4},{6,5},{7,6},{8,11},{9,8},{10,9... | collective-permute-start | bytes 1966088 | tf_op jit(solution)/shard_map/ppermute | solution.py:381
  149.7 7.9 %copy-start.8 = (bf16[128,2560]{1,0:T(8,128)(2,1)S(1)}, bf16[128,2560]{1,0:T(8,128)(2,1)}, u32[]{:S(2)}) copy-start(bf16[128,2560]{1,0:T(8,128)(2,1)} %get-tuple-element.67.refs_0_) | copy-start | bytes 1966084
  152.2 39.9 %all-to-all-start.2 = ((bf16[4,144,512]{2,1,0:T(8,128)(2,1)}), bf16[4,144,512]{2,1,0:T(8,128)(2,1)S(1)}, u32[]{:S(2)}, u32[]{:S(2)}) async-start(bf16[4,144,512]{2,1,0:T(8,128)(2,1)} %shard_map.150), calls=%async_computation.2 | async-start | bytes 1179648 | tf_op jit(solution)/shard_map/all_to_all | solution.py:453
  162.5 29.6 %copy-start.4 = (bf16[2048,128]{1,0:T(8,128)(2,1)S(1)}, bf16[2048,128]{1,0:T(8,128)(2,1)}, u32[]{:S(2)}) copy-start(bf16[2048,128]{1,0:T(8,128)(2,1)} %router.3) | copy-start | bytes 1572868
  162.5 29.6 %copy-start.11 = (f32[8,128]{1,0:T(8,128)S(1)}, f32[8,128]{1,0:T(8,128)}, u32[]{:S(2)}) copy-start(f32[8,128]{1,0:T(8,128)} %get-tuple-element.59.stats) | copy-start | bytes 12292
  162.5 29.6 %copy-start.12 = (s32[128,2]{0,1:T(2,128)S(1)}, s32[128,2]{0,1:T(2,128)}, u32[]{:S(2)}) copy-start(s32[128,2]{0,1:T(2,128)} %param.9) | copy-start | bytes 3076
  162.5 11.4 %collective-permute-start.7 = (bf16[1568,128]{1,0:T(8,128)(2,1)}, bf16[1568,128]{1,0:T(8,128)(2,1)S(1)}, u32[]{:S(2)}, u32[]{:S(2)}) collective-permute-start(bf16[1568,128]{1,0:T(8,128)(2,1)} %get-tuple-element.72), channel_id=1, source_target_pairs={{0,1},{1,2},{2,3},{3,0},{4,5},{5,6},{6,7},{7,4},{8,9},{9,10},{10,1... | collective-permute-start | bytes 1204232 | tf_op jit(solution)/shard_map/ppermute | solution.py:381
  165.8 12.5 %collective-permute-start.8 = (bf16[1568,128]{1,0:T(8,128)(2,1)}, bf16[1568,128]{1,0:T(8,128)(2,1)S(1)}, u32[]{:S(2)}, u32[]{:S(2)}) collective-permute-start(bf16[1568,128]{1,0:T(8,128)(2,1)} %get-tuple-element.73), channel_id=1, source_target_pairs={{0,2},{1,3},{2,0},{3,1},{4,6},{5,7},{6,4},{7,5},{8,10},{9,11},{10,... | collective-permute-start | bytes 1204232 | tf_op jit(solution)/shard_map/ppermute | solution.py:381
  168.3 20.9 %collective-permute-start.9 = (bf16[1568,128]{1,0:T(8,128)(2,1)}, bf16[1568,128]{1,0:T(8,128)(2,1)S(1)}, u32[]{:S(2)}, u32[]{:S(2)}) collective-permute-start(bf16[1568,128]{1,0:T(8,128)(2,1)} %get-tuple-element.74), channel_id=1, source_target_pairs={{0,3},{1,0},{2,1},{3,2},{4,7},{5,4},{6,5},{7,6},{8,11},{9,8},{10,9... | collective-permute-start | bytes 1204232 | tf_op jit(solution)/shard_map/ppermute | solution.py:381
where the time goes:
time: 194 us
  waiting for transfers between devices  80.5 us (41%)
  starting transfers between devices  70.4 us (36%)
  Pallas kernels  38.1 us (20%)
  local copies, waits for them, and re-layouts  3.51 us (2%)
    ppermute x10, waiting for transfers between devices, shift(): return lax.ppermute(x, 'tp', [(a, (a + d) % TP) for a in range(TP)])  57.7 us
    pallas_call x13, Pallas kernels, call(): pl.pallas_call(kernel, grid_spec=pltpu.PrefetchScalarGridSpec(num_scalar_...  38.1 us
    ppermute x10, starting transfers between devices, shift(): return lax.ppermute(x, 'tp', [(a, (a + d) % TP) for a in range(TP)])  31.6 us
    all_to_all x1, waiting for transfers between devices, layer(): lax.all_to_all(send_back.reshape(EXPERTS, 8, 2 * CH + 128), EP, 0, 0, til...  22.8 us
    all_to_all x1, starting transfers between devices, layer(): lax.all_to_all(send.reshape(EXPERTS, 8, 2 * CH + 128), EP, 0, 0, tiled=True)  17.6 us
    all_to_all x1, starting transfers between devices, layer(): lax.all_to_all(send_back.reshape(EXPERTS, 8, 2 * CH + 128), EP, 0, 0, til...  15.7 us
    all_to_all x1, starting transfers between devices, layer(): parts = lax.all_to_all(parts, 'tp', 0, 0, tiled=True)  5.41 us
  transfers between devices with their start and end apart: 13, of which 7 were waited for; matrix products, arithmetic and copies ran while one was open for 1% of the time, Pallas kernels for 12%

commit v1 on v0

v1 whole, which is shorter than its diff:
```python
import functools

import jax
import jax.numpy as jnp
from jax import lax
from jax.experimental import pallas as pl
from jax.experimental.pallas import tpu as pltpu
from jax.sharding import Mesh
from jax.sharding import PartitionSpec as P


EP = ("ep_0", "ep_1", "ep_2")
F32 = jnp.float32
BF16 = jnp.bfloat16


TOK = 128
D = 2048
EXPERTS = 128
TP = 4
DQ = D // TP
F = 512
FQ = F // TP
SENT = EXPERTS * 8
CH = D // 8


def dot(a, b, ca=1, cb=0):
    return lax.dot_general(a, b, (((ca,), (cb,)), ((), ())), preferred_element_type=F32)


def iota(shape, dim):
    return lax.broadcasted_iota(jnp.int32, shape, dim)


def pieces(x):
    hi = x.astype(BF16).astype(F32)
    rest = x - hi
    mid = rest.astype(BF16).astype(F32)
    return hi, mid, rest - mid


def spread(chunks):
    row = iota((SENT, SENT), 0)
    col = iota((SENT, SENT), 1)
    place = ((row // 8 == col % 128) & (row % 8 == col // 128)).astype(BF16)
    return dot(place, jnp.concatenate(chunks, axis=0)).astype(BF16)


def gather(u):
    row = iota((128, SENT), 1)
    return ((row // 8 == iota((128, SENT), 0)) & (row % 8 == u)).astype(BF16)


def every():
    return (iota((SENT, 128), 0) // 8 == iota((SENT, 128), 1)).astype(BF16)


ON_CHIP = pl.BlockSpec(memory_space=pltpu.VMEM)


def call(kernel, scalars, ins, outs, scratch=()):
    arrays = []
    specs = []
    for x in ins:
        if isinstance(x, tuple):
            arrays.append(x[0])
            specs.append(x[1])
        else:
            arrays.append(pltpu.with_memory_space_constraint(x, pltpu.VMEM))
            specs.append(ON_CHIP)
    return pl.pallas_call(
        kernel,
        grid_spec=pltpu.PrefetchScalarGridSpec(
            num_scalar_prefetch=1,
            grid=(1,),
            in_specs=tuple(specs),
            out_specs=(ON_CHIP,) * len(outs),
            scratch_shapes=scratch,
        ),
        out_shape=tuple(outs),
        compiler_params=pltpu.CompilerParams(vmem_limit_bytes=32 << 20),
    )(scalars, *arrays)


def whole(x):
    return (x, pl.BlockSpec(x.shape, lambda g, p: (0,) * x.ndim))


def sds(shape, dtype):
    return jax.ShapeDtypeStruct(shape, dtype)


def hbm(shape, dtype):
    return pltpu.HBM(shape, dtype)


def vmem(shape, dtype):
    return pltpu.VMEM(shape, dtype)


def dispatch_kernel(sc, tok, cot, routing, router, send, hit0, hit1, stats):
    experts = iota((EXPERTS, TOK), 0)
    picked = [(experts == routing[k : k + 1, :]) for k in range(2)]
    both = (picked[0] | picked[1]).astype(F32)
    logits = dot(router[...], tok[...], 0, 1)
    s = [
        jax.nn.sigmoid(jnp.sum(jnp.where(m, logits, 0.0), axis=0, keepdims=True)) for m in picked
    ]
    total = s[0] + s[1]
    g = [v / total for v in s]
    slope = [v * (1.0 - v) / total for v in s]
    before = (iota((TOK, TOK), 0) < iota((TOK, TOK), 1)).astype(BF16)
    within = dot(both.astype(BF16), before)
    mine = within == sc[0].astype(F32)
    line = iota((128, TOK), 0)
    hits = []
    info = None
    for k, out in ((0, hit0), (1, hit1)):
        hit = jnp.where(picked[k] & mine, 1.0, 0.0)
        out[...] = hit.astype(BF16)
        hits.append(hit)
        own = slope[k] * g[1 - k]
        other = slope[1 - k] * g[k]
        columns = [*pieces(g[k]), *pieces(own), *pieces(other), routing[1 - k : 2 - k, :].astype(F32)]
        table = jnp.zeros((128, TOK), F32)
        for c, v in enumerate(columns):
            table = jnp.where(line == c, v, table)
        part = dot(hit.astype(BF16), table.astype(BF16), 1, 1)
        info = part if info is None else info + part
    any_hit = (hits[0] + hits[1]).astype(BF16)
    toks = dot(any_hit, tok[...]).astype(BF16)
    cots = dot(any_hit, cot[...]).astype(BF16)
    send[:, 0 : 2 * CH] = spread(
        [
            jnp.concatenate([x[:, CH * u : CH * (u + 1)] for x in (toks, cots)], axis=1)
            for u in range(8)
        ]
    )
    send[:, 2 * CH :] = dot(every(), info.astype(BF16)).astype(BF16)
    stats[...] = jnp.concatenate(
        [s[0], s[1], total, g[0], g[1], total, total, total], axis=0
    )


def pack_kernel(sc, gate, up, down, out):
    out[:, 0:FQ] = gate[...]
    out[:, FQ : 2 * FQ] = up[...]
    out[:, 2 * FQ :] = down[...].T


def rows_kernel(sc, got, pair, info):
    for u in range(8):
        part = dot(gather(u), got[:, 0 : 2 * CH]).astype(BF16)
        pair[:, CH * u : CH * (u + 1)] = part[:, 0:CH]
        pair[:, D + CH * u : D + CH * (u + 1)] = part[:, CH:]
    info[...] = dot(gather(0), got[:, 2 * CH :]).astype(BF16)


def quarter(pair, about, parts, grads):
    pre = None
    back_raw = None
    at = 0
    for w in parts:
        n = w.shape[0]
        x = dot(pair[:, at : at + n], w[:, 0 : 2 * FQ])
        y = dot(pair[:, D + at : D + at + n], w[:, 2 * FQ :])
        pre = x if pre is None else pre + x
        back_raw = y if back_raw is None else back_raw + y
        at += n
    pre_gate = pre[:, 0:FQ]
    pre_up = pre[:, FQ:]
    gating = about[:, 0:1] + about[:, 1:2] + about[:, 2:3]
    sig = jax.nn.sigmoid(pre_gate)
    activated = pre_gate * sig
    slope = sig * (1.0 + pre_gate * (1.0 - sig))
    hidden = (activated * pre_up).astype(BF16).astype(F32)
    gg = jnp.sum(hidden * back_raw, axis=1, keepdims=True)
    scaled = gating * back_raw
    g_in = jnp.concatenate([scaled * pre_up * slope, scaled * activated], axis=1).astype(BF16)
    grads[:, 0 : 2 * FQ] = g_in
    grads[:, 2 * FQ :] = (gating * hidden).astype(BF16)
    backs = [dot(g_in, w[:, 0 : 2 * FQ], 1, 1) for w in parts]
    return gg, backs


def three_kernel(sc, pair, info, own, above, below, grads0, grads1, grads3, back, gg_out):
    about = info[...].astype(F32)
    gg = None
    for w, grads in ((own, grads0), (above, grads1), (below, grads3)):
        part, backs = quarter(pair, about, (w,), grads)
        if gg is None:
            gg = part
            back[...] = backs[0]
        else:
            gg = gg + part
            back[...] += backs[0]
    gg_out[...] = jnp.broadcast_to(gg, (128, 128))


def emit_kernel(sc, pair, info, wa, wb, back, gg_in, grads, send):
    about = info[...].astype(F32)
    gg, backs = quarter(pair, about, (wa, wb), grads)
    gg = gg + gg_in[:, 0:1]
    term = (back[...] + jnp.concatenate(backs, axis=1)).astype(BF16)
    own = (about[:, 3:4] + about[:, 4:5] + about[:, 5:6]) * gg
    other = (about[:, 6:7] + about[:, 7:8] + about[:, 8:9]) * gg
    other_expert = about[:, 9:10].astype(jnp.int32)
    lane = iota((128, EXPERTS), 1)
    mix = jnp.where(lane == sc[1], own, 0.0) - jnp.where(lane == other_expert, other, 0.0)
    mix_hi = mix.astype(BF16)
    mix_lo = (mix - mix_hi.astype(F32)).astype(BF16)
    router = dot(pair[:, 0:D], jnp.concatenate([mix_hi, mix_lo], axis=1), 0, 0)
    router = (router[:, 0:EXPERTS] + router[:, EXPERTS:]).reshape(128, 2, 8, EXPERTS)
    send[:, 0:CH] = spread([term[:, CH * u : CH * (u + 1)] for u in range(8)])
    for h in range(2):
        send[:, CH + 128 * h : CH + 128 * (h + 1)] = router[:, h].reshape(SENT, EXPERTS).astype(BF16)
    tail = jnp.zeros((128, 128), F32)
    for c, v in enumerate(pieces(gg)):
        tail = jnp.where(lane == c, v, tail)
    send[:, 2 * CH :] = dot(every(), tail.astype(BF16)).astype(BF16)


def row_sums(x):
    n, width = x.shape
    acc = x[:, 0:128]
    for c in range(1, width // 128):
        acc = acc + x[:, 128 * c : 128 * (c + 1)]
    return jnp.concatenate(
        [jnp.sum(acc[128 * c : 128 * (c + 1), :].T, axis=0, keepdims=True) for c in range(n // 128)],
        axis=0,
    )


def sums_kernel(sc, *refs):
    pairs, grads = refs[0:4], refs[4:8]
    gate, up, down, down_norms, norms = refs[8:]
    toks = jnp.concatenate([x[:, 0:D] for x in pairs], axis=0)
    cots = jnp.concatenate([x[:, D:] for x in pairs], axis=0)
    g_in = jnp.concatenate([g[:, 0 : 2 * FQ] for g in grads], axis=0)
    scaled = jnp.concatenate([g[:, 2 * FQ :] for g in grads], axis=0)
    in_sums = dot(toks, g_in, 0, 0)
    gate[...] = in_sums[:, 0:FQ].astype(BF16)
    up[...] = in_sums[:, FQ:].astype(BF16)
    squares = in_sums * in_sums
    lines = []
    for x in (squares[:, 0:FQ], squares[:, FQ:]):
        hi, mid, lo = pieces(row_sums(x))
        lines += [hi, mid + lo]
    norms[...] = jnp.concatenate(lines, axis=1).astype(BF16)
    down_sum = dot(scaled, cots, 0, 0)
    down[...] = down_sum.astype(BF16)
    down_norms[...] = row_sums(down_sum * down_sum)


def home_kernel(sc, got, hit0, hit1, norms, out):
    hits = [hit0[...], hit1[...]]
    both = (hits[0].astype(F32) + hits[1].astype(F32)).astype(BF16)
    terms = jnp.concatenate(
        [dot(gather(u), got[:, 0:CH]).astype(BF16) for u in range(8)], axis=1
    )
    summed = dot(both, terms, 0, 0).astype(BF16)
    tail = dot(gather(0), got[:, 2 * CH :]).astype(BF16)
    pick = (iota((8, SENT), 0) == iota((8, SENT), 1) % 8).astype(BF16)
    router = dot(pick, got[:, CH : 2 * CH])
    hi, mid, lo = pieces(router)
    lines = [jnp.concatenate([hi, mid + lo], axis=1)]
    flat = []
    for hit in hits:
        flat.append(dot(tail, hit, 0, 0)[0:4, :])
    flat = jnp.concatenate(flat, axis=0)
    lines.append(jnp.concatenate([flat] * 4, axis=1))
    extra = jnp.concatenate(lines, axis=0).astype(BF16)
    for q in range(TP):
        out[q, 0:TOK, :] = summed[:, DQ * q : DQ * (q + 1)]
        out[q, TOK : TOK + 16, :] = extra
        out[q, TOK + 16 :, :] = norms[...]


def last_kernel(
    sc, got, stats, routing, router, grad_tokens, grad_gating, grad_router, norms, in_norms
):
    total = got[0].astype(F32)
    for q in range(1, TP):
        total = total + got[q].astype(F32)
    extra = total[TOK:, :]
    rows = [
        extra[8 + 4 * k : 9 + 4 * k, 0:128]
        + extra[9 + 4 * k : 10 + 4 * k, 0:128]
        + extra[10 + 4 * k : 11 + 4 * k, 0:128]
        for k in range(2)
    ]
    grad_gating[...] = jnp.concatenate(rows, axis=0)
    st = stats[...]
    score_sum = st[2:3, :]
    weighted = st[3:4, :] * rows[0] + st[4:5, :] * rows[1]
    experts = iota((EXPERTS, TOK), 0)
    logits = jnp.zeros((EXPERTS, TOK), F32)
    for k in range(2):
        s = st[k : k + 1, :]
        chosen = (rows[k] - weighted) / score_sum * s * (1.0 - s)
        logits = jnp.where(experts == routing[k : k + 1, :], chosen, logits)
    term = dot(logits.astype(BF16), router[...], 0, 1)
    grad_tokens[...] = (total[0:TOK, :] + term).astype(BF16)
    sums = extra[0:8, 0:256] + extra[0:8, 256:512]
    x = jnp.concatenate([sums[:, 0:128], sums[:, 128:256]], axis=0)
    grad_router[...] = x
    squares = lax.dot_general(
        jnp.ones((8, EXPERTS), F32),
        x * x,
        (((1,), (1,)), ((), ())),
        precision=lax.Precision.HIGHEST,
        preferred_element_type=F32,
    )
    norms[...] = squares[0:1, :]
    for k in range(2):
        sums = extra[16:32, 256 * k : 256 * k + 128] + extra[16:32, 256 * k + 128 : 256 * (k + 1)]
        for c in range(D // 128):
            in_norms[k : k + 1, 128 * c : 128 * (c + 1)] = sums[c : c + 1, :]


def layer(tokens, cotangent, routing, router_weight, gate_weight, up_weight, down_weight):
    tp_index = lax.axis_index("tp")
    ep_index = lax.axis_index(EP)
    sc = jnp.stack([tp_index, ep_index]).astype(jnp.int32)
    routing_t = routing.T
    gate_w = gate_weight[0]
    up_w = up_weight[0]
    down_w = down_weight[0]
    far = functools.partial(pltpu.with_memory_space_constraint, memory_space=pltpu.HBM)

    def shift(x, d):
        return lax.ppermute(x, "tp", [(a, (a + d) % TP) for a in range(TP)])

    (packed,) = call(
        pack_kernel,
        sc,
        (whole(far(gate_w)), whole(far(up_w)), whole(far(down_w))),
        (hbm((D, 3 * FQ), BF16),),
    )
    from_below = shift(packed, 1)
    from_above = shift(packed, 3)
    far_a = shift(from_below[0 : D // 2], 1)
    far_b = shift(from_above[D // 2 :], 3)

    send, hit0, hit1, stats = call(
        dispatch_kernel,
        sc,
        (whole(far(tokens)), whole(far(cotangent)), whole(far(routing_t)), whole(far(router_weight))),
        (
            hbm((SENT, 2 * CH + 128), BF16),
            hbm((EXPERTS, TOK), BF16),
            hbm((EXPERTS, TOK), BF16),
            hbm((8, TOK), F32),
        ),
    )
    got = lax.all_to_all(send.reshape(EXPERTS, 8, 2 * CH + 128), EP, 0, 0, tiled=True)
    pair, info = call(
        rows_kernel,
        sc,
        (got.reshape(SENT, 2 * CH + 128),),
        (hbm((128, 2 * D), BF16), hbm((128, 128), BF16)),
    )
    pairs = [pair]
    for d in (1, 2, 3):
        pairs.append(shift(pair, d))
    quarter_grads = hbm((128, 3 * FQ), BF16)
    grads = [None] * TP
    grads[0], grads[1], grads[3], back, gg = call(
        three_kernel,
        sc,
        tuple(whole(far(x)) for x in (pair, info, packed, from_above, from_below)),
        (quarter_grads,) * 3 + (vmem((128, D), F32), vmem((128, 128), F32)),
    )
    grads[2], send_back = call(
        emit_kernel,
        sc,
        (*(whole(far(x)) for x in (pair, info, far_a, far_b)), back, gg),
        (quarter_grads, hbm((SENT, 2 * CH + 128), BF16)),
    )
    home = lax.all_to_all(send_back.reshape(EXPERTS, 8, 2 * CH + 128), EP, 0, 0, tiled=True)
    home = home.reshape(SENT, 2 * CH + 128)
    grads = [grads[0]] + [shift(grads[d], d) for d in (1, 2, 3)]
    grad_gate, grad_up, grad_down, down_norms, norms = call(
        sums_kernel,
        sc,
        tuple(whole(far(x)) for x in (*pairs, *grads)),
        (
            sds((D, FQ), BF16),
            sds((D, FQ), BF16),
            sds((FQ, D), BF16),
            sds((1, FQ), F32),
            hbm((16, 4 * 128), BF16),
        ),
    )
    (parts,) = call(
        home_kernel,
        sc,
        (home, whole(hit0), whole(hit1), whole(norms)),
        (vmem((TP, TOK + 32, DQ), BF16),),
    )
    parts = lax.all_to_all(parts, "tp", 0, 0, tiled=True)
    grad_tokens, grad_gating, grad_router, router_norms, in_norms = call(
        last_kernel,
        sc,
        (
            parts,
            whole(stats),
            whole(routing_t),
            (router_weight, pl.BlockSpec((DQ, 128), lambda g, p: (p[0], 0))),
        ),
        (
            sds((TOK, DQ), BF16),
            sds((2, TOK), F32),
            sds((16, EXPERTS), F32),
            sds((1, 16), F32),
            sds((2, D), F32),
        ),
    )
    return (
        grad_tokens,
        grad_gating.T,
        grad_router,
        grad_gate[None],
        grad_up[None],
        grad_down[None],
        in_norms[None],
        down_norms,
        router_norms[0],
    )


def solution(mesh):
    split = Mesh(mesh.devices.reshape(8, 8, 2, TP), ("ep_0", "ep_1", "ep_2", "tp"))
    in_specs = (
        P(EP, None),
        P(EP, None),
        P(EP, None),
        P(),
        P(EP, None, "tp"),
        P(EP, None, "tp"),
        P(EP, "tp", None),
    )
    out_specs = (
        P(EP, "tp"),
        P(EP, None),
        P(EP, None),
        P(EP, None, "tp"),
        P(EP, None, "tp"),
        P(EP, "tp", None),
        P(EP, None, None),
        P(EP, "tp"),
        P(EP),
    )
    return jax.shard_map(layer, mesh=split, in_specs=in_specs, out_specs=out_specs, check_vma=False)
```

time: 194 us -> 198 us (1.021)
  the two profiles are of different devices: /device:TPU:11 before, /device:TPU:8 now
where the time goes in v1:
time: 198 us; the launch traced here: 197 us
  waiting for transfers between devices  80.9 us (41%)
  starting transfers between devices  67.4 us (34%)
  Pallas kernels  30.5 us (15%)
  blocking collectives  13.8 us (7%)
  local copies, waits for them, and re-layouts  3.6 us (2%)
    ppermute x10, waiting for transfers between devices, shift(): return lax.ppermute(x, 'tp', [(a, (a + d) % TP) for a in range(TP)])  80.9 us
    ppermute x10, starting transfers between devices, shift(): return lax.ppermute(x, 'tp', [(a, (a + d) % TP) for a in range(TP)])  36.1 us
    pallas_call x8, Pallas kernels, call(): pl.pallas_call(kernel, grid_spec=pltpu.PrefetchScalarGridSpec(num_scalar_...  30.5 us
    all_to_all x1, starting transfers between devices, layer(): lax.all_to_all(send.reshape(EXPERTS, 8, 2 * CH + 128), EP, 0, 0, tiled=True)  17.4 us
    all_to_all x1, starting transfers between devices, layer(): lax.all_to_all(send_back.reshape(EXPERTS, 8, 2 * CH + 128), EP, 0, 0, til...  13.9 us
    all_to_all x1, blocking collectives, layer(): parts = lax.all_to_all(parts, 'tp', 0, 0, tiled=True)  13.8 us
  transfers between devices with their start and end apart: 12, of which 5 were waited for; matrix products, arithmetic and copies ran while one was open for 0% of the time, Pallas kernels for 9%

profile of v1, /device:TPU:8, one launch (start us, length us, event | category | flops | bytes accessed | tf_op | source)
XLA Modules:
  0.0 197.3 jit_solution(15214251806104297085)
XLA Ops:
  0.7 5.2 %shard_map.142 = (bf16[1024,640]{1,0:T(8,128)(2,1)}, bf16[128,128]{1,0:T(8,128)(2,1)}, bf16[128,128]{1,0:T(8,128)(2,1)}, f32[8,128]{1,0:T(8,128)}) custom-call(s32[2]{0:T(128)S(1)} %pad_add_fusion.sc, bf16[128,2048]{1,0:T(8,128)(2,1)} %tok.1, bf16[128,2048]{1,0:T(8,128)(2,1)} %cot.1, s32[2,128]{1,0:T(2,128)} %bitcast.18, bf16[2048,128]{1,0:T(8,128)(2,1)} %router.3), custom_call_target="tpu_custom_call" | custom-call | tf_op jit(solution)/shard_map/pallas_call | solution.py:72
  5.9 17.4 %all-to-all-start = ((bf16[128,8,640]{2,1,0:T(8,128)(2,1)}), bf16[128,8,640]{2,1,0:T(8,128)(2,1)S(1)}, u32[]{:S(2)}, u32[]{:S(2)}) async-start(bf16[128,8,640]{2,1,0:T(8,128)(2,1)} %bitcast.21), calls=%async_computation | async-start | bytes 2621440 | tf_op jit(solution)/shard_map/all_to_all | solution.py:357
  23.3 3.4 %shard_map.144.own = bf16[2048,384]{1,0:T(8,128)(2,1)} custom-call(s32[2]{0:T(128)S(1)} %pad_add_fusion.sc, bf16[2048,128]{1,0:T(8,128)(2,1)} %bitcast.22, bf16[2048,128]{1,0:T(8,128)(2,1)} %bitcast.23, bf16[128,2048]{1,0:T(8,128)(2,1)} %bitcast.24), custom_call_target="tpu_custom_call" | custom-call | tf_op jit(solution)/shard_map/pallas_call | solution.py:72
  26.7 3.4 %collective-permute-start = (bf16[2048,384]{1,0:T(8,128)(2,1)}, bf16[2048,384]{1,0:T(8,128)(2,1)S(1)}, u32[]{:S(2)}, u32[]{:S(2)}) collective-permute-start(bf16[2048,384]{1,0:T(8,128)(2,1)} %shard_map.144.own), channel_id=1, source_target_pairs={{0,1},{1,2},{2,3},{3,0},{4,5},{5,6},{6,7},{7,4},{8,9},{9,10},{10,1... | collective-permute-start | bytes 4718600 | tf_op jit(solution)/shard_map/ppermute | solution.py:333
  30.1 3.7 %collective-permute-start.2 = (bf16[2048,384]{1,0:T(8,128)(2,1)}, bf16[2048,384]{1,0:T(8,128)(2,1)S(1)}, u32[]{:S(2)}, u32[]{:S(2)}) collective-permute-start(bf16[2048,384]{1,0:T(8,128)(2,1)} %shard_map.144.own), channel_id=1, source_target_pairs={{0,3},{1,0},{2,1},{3,2},{4,7},{5,4},{6,5},{7,6},{8,11},{9,8},{10,9... | collective-permute-start | bytes 4718600 | tf_op jit(solution)/shard_map/ppermute | solution.py:333
  33.8 32.7 %collective-permute-done.below = bf16[2048,384]{1,0:T(8,128)(2,1)S(1)} collective-permute-done((bf16[2048,384]{1,0:T(8,128)(2,1)}, bf16[2048,384]{1,0:T(8,128)(2,1)S(1)}, u32[]{:S(2)}, u32[]{:S(2)}) %collective-permute-start) | collective-permute-done | bytes 1572896 | tf_op jit(solution)/shard_map/ppermute | solution.py:333
  66.5 2.2 %collective-permute-start.1 = (bf16[1024,384]{1,0:T(8,128)(2,1)S(1)}, bf16[1024,384]{1,0:T(8,128)(2,1)}, u32[]{:S(2)}, u32[]{:S(2)}) collective-permute-start(bf16[1024,384]{1,0:T(8,128)(2,1)S(1)} %slice.8), channel_id=1, source_target_pairs={{0,1},{1,2},{2,3},{3,0},{4,5},{5,6},{6,7},{7,4},{8,9},{9,10},{10,1... | collective-permute-start | bytes 2359304 | tf_op jit(solution)/shard_map/ppermute | solution.py:333
  68.8 1.0 copy-done.8
  69.9 4.9 %collective-permute-start.3 = (bf16[1024,384]{1,0:T(8,128)(2,1)S(1)}, bf16[1024,384]{1,0:T(8,128)(2,1)}, u32[]{:S(2)}, u32[]{:S(2)}) collective-permute-start(bf16[1024,384]{1,0:T(8,128)(2,1)S(1)} %slice.9), channel_id=1, source_target_pairs={{0,3},{1,0},{2,1},{3,2},{4,7},{5,4},{6,5},{7,6},{8,11},{9,8},{10,9... | collective-permute-start | bytes 2359304 | tf_op jit(solution)/shard_map/ppermute | solution.py:333
  74.7 2.8 %shard_map.143 = (bf16[128,4096]{1,0:T(8,128)(2,1)}, bf16[128,128]{1,0:T(8,128)(2,1)}) custom-call(s32[2]{0:T(128)S(1)} %pad_add_fusion.sc, bf16[1024,640]{1,0:T(8,128)(2,1)S(1)} %bitcast.17), custom_call_target="tpu_custom_call" | custom-call | tf_op jit(solution)/shard_map/pallas_call | solution.py:72
  77.6 5.7 %shard_map.145 = (bf16[128,384]{1,0:T(8,128)(2,1)}, bf16[128,384]{1,0:T(8,128)(2,1)}, bf16[128,384]{1,0:T(8,128)(2,1)}, f32[128,2048]{1,0:T(8,128)S(1)}, f32[128,128]{1,0:T(8,128)S(1)}) custom-call(s32[2]{0:T(128)S(1)} %pad_add_fusion.sc, bf16[128,4096]{1,0:T(8,128)(2,1)} %get-tuple-element.33.pair.refs_0_, bf16[128,128]{1,0:T(8,128)(2,1)} %get-tuple-element.34.info, ...), custom_call_target="tpu_custom_call" | custom-call | tf_op jit(solution)/shard_map/pallas_call | solution.py:72
  83.3 5.1 %collective-permute-done.1.wa = bf16[1024,384]{1,0:T(8,128)(2,1)} collective-permute-done((bf16[1024,384]{1,0:T(8,128)(2,1)S(1)}, bf16[1024,384]{1,0:T(8,128)(2,1)}, u32[]{:S(2)}, u32[]{:S(2)}) %collective-permute-start.1) | collective-permute-done | bytes 786464 | tf_op jit(solution)/shard_map/ppermute | solution.py:333
  88.4 2.2 %collective-permute-done.3.wb = bf16[1024,384]{1,0:T(8,128)(2,1)} collective-permute-done((bf16[1024,384]{1,0:T(8,128)(2,1)S(1)}, bf16[1024,384]{1,0:T(8,128)(2,1)}, u32[]{:S(2)}, u32[]{:S(2)}) %collective-permute-start.3) | collective-permute-done | bytes 786464 | tf_op jit(solution)/shard_map/ppermute | solution.py:333
  90.6 5.1 %shard_map.146 = (bf16[128,384]{1,0:T(8,128)(2,1)}, bf16[1024,640]{1,0:T(8,128)(2,1)}) custom-call(s32[2]{0:T(128)S(1)} %pad_add_fusion.sc, bf16[128,4096]{1,0:T(8,128)(2,1)} %get-tuple-element.33.pair.refs_0_, bf16[128,128]{1,0:T(8,128)(2,1)} %get-tuple-element.34.info, bf16[1024,384]{1,0:T(8,128)(2,1)} %collective-permute-done.1.wa, ...), custom_call_target="tpu_custom_call" | custom-call | tf_op jit(solution)/shard_map/pallas_call | solution.py:72
  95.8 13.9 %all-to-all-start.1 = ((bf16[128,8,640]{2,1,0:T(8,128)(2,1)}), bf16[128,8,640]{2,1,0:T(8,128)(2,1)S(1)}, u32[]{:S(2)}, u32[]{:S(2)}) async-start(bf16[128,8,640]{2,1,0:T(8,128)(2,1)} %bitcast.20), calls=%async_computation.1 | async-start | bytes 2621440 | tf_op jit(solution)/shard_map/all_to_all | solution.py:381
  109.7 3.0 %collective-permute-start.4 = (bf16[128,4096]{1,0:T(8,128)(2,1)S(1)}, bf16[128,4096]{1,0:T(8,128)(2,1)S(1)}, u32[]{:S(2)}, u32[]{:S(2)}) collective-permute-start(bf16[128,4096]{1,0:T(8,128)(2,1)S(1)} %copy-done.6), channel_id=1, source_target_pairs={{0,1},{1,2},{2,3},{3,0},{4,5},{5,6},{6,7},{7,4},{8,9},{9,10},{10,1... | collective-permute-start | bytes 3145736 | tf_op jit(solution)/shard_map/ppermute | solution.py:333
  112.8 6.2 %collective-permute-start.5 = (bf16[128,4096]{1,0:T(8,128)(2,1)S(1)}, bf16[128,4096]{1,0:T(8,128)(2,1)S(1)}, u32[]{:S(2)}, u32[]{:S(2)}) collective-permute-start(bf16[128,4096]{1,0:T(8,128)(2,1)S(1)} %copy-done.6), channel_id=1, source_target_pairs={{0,2},{1,3},{2,0},{3,1},{4,6},{5,7},{6,4},{7,5},{8,10},{9,11},{10,... | collective-permute-start | bytes 3145736 | tf_op jit(solution)/shard_map/ppermute | solution.py:333
  119.0 1.9 collective-permute-start.6
  120.9 3.4 %collective-permute-start.8 = (bf16[128,384]{1,0:T(8,128)(2,1)S(1)}, bf16[128,384]{1,0:T(8,128)(2,1)S(1)}, u32[]{:S(2)}, u32[]{:S(2)}) collective-permute-start(bf16[128,384]{1,0:T(8,128)(2,1)S(1)} %copy-done.17), channel_id=1, source_target_pairs={{0,2},{1,3},{2,0},{3,1},{4,6},{5,7},{6,4},{7,5},{8,10},{9,11},{10,... | collective-permute-start | bytes 294920 | tf_op jit(solution)/shard_map/ppermute | solution.py:333
  124.3 2.5 %collective-permute-start.7 = (bf16[128,384]{1,0:T(8,128)(2,1)S(1)}, bf16[128,384]{1,0:T(8,128)(2,1)S(1)}, u32[]{:S(2)}, u32[]{:S(2)}) collective-permute-start(bf16[128,384]{1,0:T(8,128)(2,1)S(1)} %copy-done.16), channel_id=1, source_target_pairs={{0,1},{1,2},{2,3},{3,0},{4,5},{5,6},{6,7},{7,4},{8,9},{9,10},{10,1... | collective-permute-start | bytes 294920 | tf_op jit(solution)/shard_map/ppermute | solution.py:333
  126.8 38.7 %collective-permute-done.8.refs_6_ = bf16[128,384]{1,0:T(8,128)(2,1)S(1)} collective-permute-done((bf16[128,384]{1,0:T(8,128)(2,1)S(1)}, bf16[128,384]{1,0:T(8,128)(2,1)S(1)}, u32[]{:S(2)}, u32[]{:S(2)}) %collective-permute-start.8) | collective-permute-done | bytes 98336 | tf_op jit(solution)/shard_map/ppermute | solution.py:333
  165.5 5.0 %collective-permute-start.9 = (bf16[128,384]{1,0:T(8,128)(2,1)S(1)}, bf16[128,384]{1,0:T(8,128)(2,1)S(1)}, u32[]{:S(2)}, u32[]{:S(2)}) collective-permute-start(bf16[128,384]{1,0:T(8,128)(2,1)S(1)} %copy-done.15), channel_id=1, source_target_pairs={{0,3},{1,0},{2,1},{3,2},{4,7},{5,4},{6,5},{7,6},{8,11},{9,8},{10,9... | collective-permute-start | bytes 294920 | tf_op jit(solution)/shard_map/ppermute | solution.py:333
  170.6 2.2 %collective-permute-done.9.refs_7_ = bf16[128,384]{1,0:T(8,128)(2,1)S(1)} collective-permute-done((bf16[128,384]{1,0:T(8,128)(2,1)S(1)}, bf16[128,384]{1,0:T(8,128)(2,1)S(1)}, u32[]{:S(2)}, u32[]{:S(2)}) %collective-permute-start.9) | collective-permute-done | bytes 98336 | tf_op jit(solution)/shard_map/ppermute | solution.py:333
  172.8 0.6 copy-done.14
  173.4 0.4 copy-done.9
  173.8 0.3 copy-done.10
  174.1 0.4 copy-done.11
  174.4 5.1 %shard_map.147 = (bf16[2048,128]{1,0:T(8,128)(2,1)}, bf16[2048,128]{1,0:T(8,128)(2,1)}, bf16[128,2048]{1,0:T(8,128)(2,1)}, f32[1,128]{1,0:T(1,128)}, bf16[16,512]{1,0:T(8,128)(2,1)}) custom-call(s32[2]{0:T(128)S(1)} %pad_add_fusion.sc, bf16[128,4096]{1,0:T(8,128)(2,1)} %get-tuple-element.33.pair.refs_0_, bf16[128,4096]{1,0:T(8,128)(2,1)} %copy-done.9, ...), custom_call_target="tpu_custom_call" | custom-call | tf_op jit(solution)/shard_map/pallas_call | solution.py:72
  179.5 0.7 copy-done.3
  180.3 1.7 shard_map.148
  182.0 13.8 %all_to_all.15.got = bf16[4,160,512]{2,1,0:T(8,128)(2,1)S(1)} all-to-all(bf16[4,160,512]{2,1,0:T(8,128)(2,1)S(1)} %shard_map.148), channel_id=1, replica_groups=mesh['ep_0'=8,'ep_1'=8,'ep_2'=2,'tp'=4] {'tp'}, dimensions={0} | all-to-all | bytes 1310720 | tf_op jit(solution)/shard_map/all_to_all | solution.py:402
  195.8 1.4 shard_map.149
  (40 shorter events, 0.3 us)
Async XLA Ops:
  5.9 68.8 %all-to-all-start = ((bf16[128,8,640]{2,1,0:T(8,128)(2,1)}), bf16[128,8,640]{2,1,0:T(8,128)(2,1)S(1)}, u32[]{:S(2)}, u32[]{:S(2)}) async-start(bf16[128,8,640]{2,1,0:T(8,128)(2,1)} %bitcast.21), calls=%async_computation | async-start | bytes 2621440 | tf_op jit(solution)/shard_map/all_to_all | solution.py:357
  26.7 39.7 %collective-permute-start = (bf16[2048,384]{1,0:T(8,128)(2,1)}, bf16[2048,384]{1,0:T(8,128)(2,1)S(1)}, u32[]{:S(2)}, u32[]{:S(2)}) collective-permute-start(bf16[2048,384]{1,0:T(8,128)(2,1)} %shard_map.144.own), channel_id=1, source_target_pairs={{0,1},{1,2},{2,3},{3,0},{4,5},{5,6},{6,7},{7,4},{8,9},{9,10},{10,1... | collective-permute-start | bytes 4718600 | tf_op jit(solution)/shard_map/ppermute | solution.py:333
  30.1 38.6 %collective-permute-start.2 = (bf16[2048,384]{1,0:T(8,128)(2,1)}, bf16[2048,384]{1,0:T(8,128)(2,1)S(1)}, u32[]{:S(2)}, u32[]{:S(2)}) collective-permute-start(bf16[2048,384]{1,0:T(8,128)(2,1)} %shard_map.144.own), channel_id=1, source_target_pairs={{0,3},{1,0},{2,1},{3,2},{4,7},{5,4},{6,5},{7,6},{8,11},{9,8},{10,9... | collective-permute-start | bytes 4718600 | tf_op jit(solution)/shard_map/ppermute | solution.py:333
  66.4 2.4 %copy-start.7 = (bf16[2048,384]{1,0:T(8,128)(2,1)}, bf16[2048,384]{1,0:T(8,128)(2,1)S(1)}, u32[]{:S(2)}) copy-start(bf16[2048,384]{1,0:T(8,128)(2,1)S(1)} %collective-permute-done.below) | copy-start | bytes 4718596
  66.5 21.9 %collective-permute-start.1 = (bf16[1024,384]{1,0:T(8,128)(2,1)S(1)}, bf16[1024,384]{1,0:T(8,128)(2,1)}, u32[]{:S(2)}, u32[]{:S(2)}) collective-permute-start(bf16[1024,384]{1,0:T(8,128)(2,1)S(1)} %slice.8), channel_id=1, source_target_pairs={{0,1},{1,2},{2,3},{3,0},{4,5},{5,6},{6,7},{7,4},{8,9},{9,10},{10,1... | collective-permute-start | bytes 2359304 | tf_op jit(solution)/shard_map/ppermute | solution.py:333
  68.7 1.1 copy-start.8
  69.9 20.8 %collective-permute-start.3 = (bf16[1024,384]{1,0:T(8,128)(2,1)S(1)}, bf16[1024,384]{1,0:T(8,128)(2,1)}, u32[]{:S(2)}, u32[]{:S(2)}) collective-permute-start(bf16[1024,384]{1,0:T(8,128)(2,1)S(1)} %slice.9), channel_id=1, source_target_pairs={{0,3},{1,0},{2,1},{3,2},{4,7},{5,4},{6,5},{7,6},{8,11},{9,8},{10,9... | collective-permute-start | bytes 2359304 | tf_op jit(solution)/shard_map/ppermute | solution.py:333
  95.8 13.9 %copy-start.6 = (bf16[128,4096]{1,0:T(8,128)(2,1)S(1)}, bf16[128,4096]{1,0:T(8,128)(2,1)}, u32[]{:S(2)}) copy-start(bf16[128,4096]{1,0:T(8,128)(2,1)} %get-tuple-element.33.pair.refs_0_) | copy-start | bytes 3145732
  95.8 25.1 %copy-start.17 = (bf16[128,384]{1,0:T(8,128)(2,1)S(1)}, bf16[128,384]{1,0:T(8,128)(2,1)}, u32[]{:S(2)}) copy-start(bf16[128,384]{1,0:T(8,128)(2,1)} %get-tuple-element.42) | copy-start | bytes 294916
  95.8 28.5 %copy-start.16 = (bf16[128,384]{1,0:T(8,128)(2,1)S(1)}, bf16[128,384]{1,0:T(8,128)(2,1)}, u32[]{:S(2)}) copy-start(bf16[128,384]{1,0:T(8,128)(2,1)} %get-tuple-element.41) | copy-start | bytes 294916
  95.8 69.7 %copy-start.15 = (bf16[128,384]{1,0:T(8,128)(2,1)S(1)}, bf16[128,384]{1,0:T(8,128)(2,1)}, u32[]{:S(2)}) copy-start(bf16[128,384]{1,0:T(8,128)(2,1)} %get-tuple-element.43) | copy-start | bytes 294916
  95.8 83.7 %all-to-all-start.1 = ((bf16[128,8,640]{2,1,0:T(8,128)(2,1)}), bf16[128,8,640]{2,1,0:T(8,128)(2,1)S(1)}, u32[]{:S(2)}, u32[]{:S(2)}) async-start(bf16[128,8,640]{2,1,0:T(8,128)(2,1)} %bitcast.20), calls=%async_computation.1 | async-start | bytes 2621440 | tf_op jit(solution)/shard_map/all_to_all | solution.py:381
  109.7 63.0 %collective-permute-start.4 = (bf16[128,4096]{1,0:T(8,128)(2,1)S(1)}, bf16[128,4096]{1,0:T(8,128)(2,1)S(1)}, u32[]{:S(2)}, u32[]{:S(2)}) collective-permute-start(bf16[128,4096]{1,0:T(8,128)(2,1)S(1)} %copy-done.6), channel_id=1, source_target_pairs={{0,1},{1,2},{2,3},{3,0},{4,5},{5,6},{6,7},{7,4},{8,9},{9,10},{10,1... | collective-permute-start | bytes 3145736 | tf_op jit(solution)/shard_map/ppermute | solution.py:333
  112.8 60.0 %collective-permute-start.5 = (bf16[128,4096]{1,0:T(8,128)(2,1)S(1)}, bf16[128,4096]{1,0:T(8,128)(2,1)S(1)}, u32[]{:S(2)}, u32[]{:S(2)}) collective-permute-start(bf16[128,4096]{1,0:T(8,128)(2,1)S(1)} %copy-done.6), channel_id=1, source_target_pairs={{0,2},{1,3},{2,0},{3,1},{4,6},{5,7},{6,4},{7,5},{8,10},{9,11},{10,... | collective-permute-start | bytes 3145736 | tf_op jit(solution)/shard_map/ppermute | solution.py:333
  119.0 53.8 %collective-permute-start.6 = (bf16[128,4096]{1,0:T(8,128)(2,1)S(1)}, bf16[128,4096]{1,0:T(8,128)(2,1)S(1)}, u32[]{:S(2)}, u32[]{:S(2)}) collective-permute-start(bf16[128,4096]{1,0:T(8,128)(2,1)S(1)} %copy-done.6), channel_id=1, source_target_pairs={{0,3},{1,0},{2,1},{3,2},{4,7},{5,4},{6,5},{7,6},{8,11},{9,8},{10,9... | collective-permute-start | bytes 3145736 | tf_op jit(solution)/shard_map/ppermute | solution.py:333
  120.9 44.6 %collective-permute-start.8 = (bf16[128,384]{1,0:T(8,128)(2,1)S(1)}, bf16[128,384]{1,0:T(8,128)(2,1)S(1)}, u32[]{:S(2)}, u32[]{:S(2)}) collective-permute-start(bf16[128,384]{1,0:T(8,128)(2,1)S(1)} %copy-done.17), channel_id=1, source_target_pairs={{0,2},{1,3},{2,0},{3,1},{4,6},{5,7},{6,4},{7,5},{8,10},{9,11},{10,... | collective-permute-start | bytes 294920 | tf_op jit(solution)/shard_map/ppermute | solution.py:333
  124.3 46.2 %collective-permute-start.7 = (bf16[128,384]{1,0:T(8,128)(2,1)S(1)}, bf16[128,384]{1,0:T(8,128)(2,1)S(1)}, u32[]{:S(2)}, u32[]{:S(2)}) collective-permute-start(bf16[128,384]{1,0:T(8,128)(2,1)S(1)} %copy-done.16), channel_id=1, source_target_pairs={{0,1},{1,2},{2,3},{3,0},{4,5},{5,6},{6,7},{7,4},{8,9},{9,10},{10,1... | collective-permute-start | bytes 294920 | tf_op jit(solution)/shard_map/ppermute | solution.py:333
  165.5 7.3 %copy-start.12 = (bf16[128,384]{1,0:T(8,128)(2,1)}, bf16[128,384]{1,0:T(8,128)(2,1)S(1)}, u32[]{:S(2)}) copy-start(bf16[128,384]{1,0:T(8,128)(2,1)S(1)} %collective-permute-done.8.refs_6_) | copy-start | bytes 294916
  165.5 7.2 %collective-permute-start.9 = (bf16[128,384]{1,0:T(8,128)(2,1)S(1)}, bf16[128,384]{1,0:T(8,128)(2,1)S(1)}, u32[]{:S(2)}, u32[]{:S(2)}) collective-permute-start(bf16[128,384]{1,0:T(8,128)(2,1)S(1)} %copy-done.15), channel_id=1, source_target_pairs={{0,3},{1,0},{2,1},{3,2},{4,7},{5,4},{6,5},{7,6},{8,11},{9,8},{10,9... | collective-permute-start | bytes 294920 | tf_op jit(solution)/shard_map/ppermute | solution.py:333
  170.6 2.2 %copy-start.13 = (bf16[128,384]{1,0:T(8,128)(2,1)}, bf16[128,384]{1,0:T(8,128)(2,1)S(1)}, u32[]{:S(2)}) copy-start(bf16[128,384]{1,0:T(8,128)(2,1)S(1)} %collective-permute-done.7.refs_5_) | copy-start | bytes 294916
  172.7 0.6 copy-start.14
  172.8 1.0 copy-start.9
  172.8 1.3 copy-start.10
  172.8 1.7 copy-start.11
  174.4 5.1 %copy-start.1 = (bf16[128,128]{1,0:T(8,128)(2,1)S(1)}, bf16[128,128]{1,0:T(8,128)(2,1)}, u32[]{:S(2)}) copy-start(bf16[128,128]{1,0:T(8,128)(2,1)} %get-tuple-element.38.hit0) | copy-start | bytes 98308
  174.4 5.1 %copy-start.2 = (bf16[128,128]{1,0:T(8,128)(2,1)S(1)}, bf16[128,128]{1,0:T(8,128)(2,1)}, u32[]{:S(2)}) copy-start(bf16[128,128]{1,0:T(8,128)(2,1)} %get-tuple-element.39.hit1) | copy-start | bytes 98308
  179.5 0.7 copy-start.3
  180.3 15.6 %copy-start = (bf16[2048,128]{1,0:T(8,128)(2,1)S(1)}, bf16[2048,128]{1,0:T(8,128)(2,1)}, u32[]{:S(2)}) copy-start(bf16[2048,128]{1,0:T(8,128)(2,1)} %router.3) | copy-start | bytes 1572868
  180.3 15.6 %copy-start.4 = (f32[8,128]{1,0:T(8,128)S(1)}, f32[8,128]{1,0:T(8,128)}, u32[]{:S(2)}) copy-start(f32[8,128]{1,0:T(8,128)} %get-tuple-element.45.stats) | copy-start | bytes 12292
  180.3 15.6 %copy-start.5 = (s32[128,2]{0,1:T(2,128)S(1)}, s32[128,2]{0,1:T(2,128)}, u32[]{:S(2)}) copy-start(s32[128,2]{0,1:T(2,128)} %param.9) | copy-start | bytes 3076

commit v2 on v1

--- a/solution.py
+++ b/solution.py
@@ -40,16 +40,23 @@
     return hi, mid, rest - mid
 
 
-def spread(chunks):
-    row = iota((SENT, SENT), 0)
-    col = iota((SENT, SENT), 1)
-    place = ((row // 8 == col % 128) & (row % 8 == col // 128)).astype(BF16)
-    return dot(place, jnp.concatenate(chunks, axis=0)).astype(BF16)
-
-
-def gather(u):
-    row = iota((128, SENT), 1)
-    return ((row // 8 == iota((128, SENT), 0)) & (row % 8 == u)).astype(BF16)
+def spread(scratch, chunks):
+    width = scratch.shape[0]
+    for u, chunk in enumerate(chunks):
+        for c in range(width):
+            scratch[c, pl.ds(u, 128, stride=8), :] = chunk[:, 128 * c : 128 * (c + 1)].astype(F32)
+    return jnp.concatenate([scratch[c].astype(BF16) for c in range(width)], axis=1)
+
+
+def fill(scratch, got):
+    for c in range(scratch.shape[0]):
+        scratch[c] = got[:, 128 * c : 128 * (c + 1)].astype(F32)
+
+
+def gather(scratch, u):
+    return jnp.concatenate(
+        [scratch[c, pl.ds(u, 128, stride=8), :].astype(BF16) for c in range(scratch.shape[0])], axis=1
+    )
 
 
 def every():
@@ -99,7 +106,7 @@
     return pltpu.VMEM(shape, dtype)
 
 
-def dispatch_kernel(sc, tok, cot, routing, router, send, hit0, hit1, stats):
+def dispatch_kernel(sc, tok, cot, routing, router, send, hit0, hit1, stats, scratch):
     experts = iota((EXPERTS, TOK), 0)
     picked = [(experts == routing[k : k + 1, :]) for k in range(2)]
     both = (picked[0] | picked[1]).astype(F32)
@@ -129,13 +136,14 @@
         part = dot(hit.astype(BF16), table.astype(BF16), 1, 1)
         info = part if info is None else info + part
     any_hit = (hits[0] + hits[1]).astype(BF16)
-    toks = dot(any_hit, tok[...]).astype(BF16)
-    cots = dot(any_hit, cot[...]).astype(BF16)
+    toks = dot(any_hit, tok[...])
+    cots = dot(any_hit, cot[...])
     send[:, 0 : 2 * CH] = spread(
+        scratch,
         [
             jnp.concatenate([x[:, CH * u : CH * (u + 1)] for x in (toks, cots)], axis=1)
             for u in range(8)
-        ]
+        ],
     )
     send[:, 2 * CH :] = dot(every(), info.astype(BF16)).astype(BF16)
     stats[...] = jnp.concatenate(
@@ -149,12 +157,14 @@
     out[:, 2 * FQ :] = down[...].T
 
 
-def rows_kernel(sc, got, pair, info):
+def rows_kernel(sc, got, pair, info, scratch):
+    fill(scratch, got)
     for u in range(8):
-        part = dot(gather(u), got[:, 0 : 2 * CH]).astype(BF16)
+        part = gather(scratch, u)
         pair[:, CH * u : CH * (u + 1)] = part[:, 0:CH]
-        pair[:, D + CH * u : D + CH * (u + 1)] = part[:, CH:]
-    info[...] = dot(gather(0), got[:, 2 * CH :]).astype(BF16)
+        pair[:, D + CH * u : D + CH * (u + 1)] = part[:, CH : 2 * CH]
+        if u == 0:
+            info[...] = part[:, 2 * CH :]
 
 
 def quarter(pair, about, parts, grads):
@@ -184,11 +194,17 @@
     return gg, backs
 
 
-def three_kernel(sc, pair, info, own, above, below, grads0, grads1, grads3, back, gg_out):
+def three_kernel(sc, pair, info, own, above, below, grads0, grads1, grads3, back, gg_out, held, sems):
+    copies = [
+        pltpu.make_async_copy(w, held.at[k], sems.at[k]) for k, w in enumerate((own, above, below))
+    ]
+    for c in copies:
+        c.start()
     about = info[...].astype(F32)
     gg = None
-    for w, grads in ((own, grads0), (above, grads1), (below, grads3)):
-        part, backs = quarter(pair, about, (w,), grads)
+    for k, grads in enumerate((grads0, grads1, grads3)):
+        copies[k].wait()
+        part, backs = quarter(pair, about, (held.at[k],), grads)
         if gg is None:
             gg = part
             back[...] = backs[0]
@@ -198,11 +214,11 @@
     gg_out[...] = jnp.broadcast_to(gg, (128, 128))
 
 
-def emit_kernel(sc, pair, info, wa, wb, back, gg_in, grads, send):
+def emit_kernel(sc, pair, info, wa, wb, back, gg_in, grads, send, scratch):
     about = info[...].astype(F32)
     gg, backs = quarter(pair, about, (wa, wb), grads)
     gg = gg + gg_in[:, 0:1]
-    term = (back[...] + jnp.concatenate(backs, axis=1)).astype(BF16)
+    term = back[...] + jnp.concatenate(backs, axis=1)
     own = (about[:, 3:4] + about[:, 4:5] + about[:, 5:6]) * gg
     other = (about[:, 6:7] + about[:, 7:8] + about[:, 8:9]) * gg
     other_expert = about[:, 9:10].astype(jnp.int32)
@@ -212,7 +228,7 @@
     mix_lo = (mix - mix_hi.astype(F32)).astype(BF16)
     router = dot(pair[:, 0:D], jnp.concatenate([mix_hi, mix_lo], axis=1), 0, 0)
     router = (router[:, 0:EXPERTS] + router[:, EXPERTS:]).reshape(128, 2, 8, EXPERTS)
-    send[:, 0:CH] = spread([term[:, CH * u : CH * (u + 1)] for u in range(8)])
+    send[:, 0:CH] = spread(scratch, [term[:, CH * u : CH * (u + 1)] for u in range(8)])
     for h in range(2):
         send[:, CH + 128 * h : CH + 128 * (h + 1)] = router[:, h].reshape(SENT, EXPERTS).astype(BF16)
     tail = jnp.zeros((128, 128), F32)
@@ -233,8 +249,8 @@
 
 
 def sums_kernel(sc, *refs):
-    pairs, grads = refs[0:4], refs[4:8]
-    gate, up, down, down_norms, norms = refs[8:]
+    pairs, grads = refs[0:5], refs[5:9]
+    gate, up, down, down_norms, norms = refs[9:]
     toks = jnp.concatenate([x[:, 0:D] for x in pairs], axis=0)
     cots = jnp.concatenate([x[:, D:] for x in pairs], axis=0)
     g_in = jnp.concatenate([g[:, 0 : 2 * FQ] for g in grads], axis=0)
@@ -253,14 +269,14 @@
     down_norms[...] = row_sums(down_sum * down_sum)
 
 
-def home_kernel(sc, got, hit0, hit1, norms, out):
+def home_kernel(sc, got, hit0, hit1, norms, out, scratch):
+    fill(scratch, got)
     hits = [hit0[...], hit1[...]]
     both = (hits[0].astype(F32) + hits[1].astype(F32)).astype(BF16)
-    terms = jnp.concatenate(
-        [dot(gather(u), got[:, 0:CH]).astype(BF16) for u in range(8)], axis=1
-    )
+    lines = [gather(scratch, u) for u in range(8)]
+    terms = jnp.concatenate([x[:, 0:CH] for x in lines], axis=1)
     summed = dot(both, terms, 0, 0).astype(BF16)
-    tail = dot(gather(0), got[:, 2 * CH :]).astype(BF16)
+    tail = lines[0][:, 2 * CH :]
     pick = (iota((8, SENT), 0) == iota((8, SENT), 1) % 8).astype(BF16)
     router = dot(pick, got[:, CH : 2 * CH])
     hi, mid, lo = pieces(router)
@@ -353,6 +369,7 @@
             hbm((EXPERTS, TOK), BF16),
             hbm((8, TOK), F32),
         ),
+        (pltpu.VMEM((2 * CH // 128, SENT, 128), F32),),
     )
     got = lax.all_to_all(send.reshape(EXPERTS, 8, 2 * CH + 128), EP, 0, 0, tiled=True)
     pair, info = call(
@@ -360,23 +377,31 @@
         sc,
         (got.reshape(SENT, 2 * CH + 128),),
         (hbm((128, 2 * D), BF16), hbm((128, 128), BF16)),
-    )
-    pairs = [pair]
-    for d in (1, 2, 3):
-        pairs.append(shift(pair, d))
+        (pltpu.VMEM((2 * CH // 128 + 1, SENT, 128), F32),),
+    )
+    pair_1 = shift(pair, 1)
+    pair_3 = shift(pair, 3)
+    top = shift(pair_1[0:64], 1)
+    bottom = shift(pair_3[64:], 3)
+    pairs = [pair, pair_1, top, bottom, pair_3]
     quarter_grads = hbm((128, 3 * FQ), BF16)
     grads = [None] * TP
     grads[0], grads[1], grads[3], back, gg = call(
         three_kernel,
         sc,
-        tuple(whole(far(x)) for x in (pair, info, packed, from_above, from_below)),
+        (
+            *(whole(far(x)) for x in (pair, info)),
+            *((far(x), pl.BlockSpec(memory_space=pltpu.HBM)) for x in (packed, from_above, from_below)),
+        ),
         (quarter_grads,) * 3 + (vmem((128, D), F32), vmem((128, 128), F32)),
+        (pltpu.VMEM((3, D, 3 * FQ), BF16), pltpu.SemaphoreType.DMA((3,))),
     )
     grads[2], send_back = call(
         emit_kernel,
         sc,
         (*(whole(far(x)) for x in (pair, info, far_a, far_b)), back, gg),
         (quarter_grads, hbm((SENT, 2 * CH + 128), BF16)),
+        (pltpu.VMEM((CH // 128, SENT, 128), F32),),
     )
     home = lax.all_to_all(send_back.reshape(EXPERTS, 8, 2 * CH + 128), EP, 0, 0, tiled=True)
     home = home.reshape(SENT, 2 * CH + 128)
@@ -398,6 +423,7 @@
         sc,
         (home, whole(hit0), whole(hit1), whole(norms)),
         (vmem((TP, TOK + 32, DQ), BF16),),
+        (pltpu.VMEM((2 * CH // 128 + 1, SENT, 128), F32),),
     )
     parts = lax.all_to_all(parts, "tp", 0, 0, tiled=True)
     grad_tokens, grad_gating, grad_router, router_norms, in_norms = call(

time: 198 us -> 184 us (0.929)
  waiting for transfers between devices: 80.9 us -> 69.1 us
  Pallas kernels: 30.5 us -> 27.8 us
    ppermute x10 -> x11, waiting for transfers between devices: 80.9 us -> 69.1 us  [shift(): return lax.ppermute(x, 'tp', [(a, (a + d) % TP) for a in range(TP)])]
    pallas_call x8, Pallas kernels: 30.5 us -> 27.8 us  [call(): pl.pallas_call(kernel, grid_spec=pltpu.PrefetchScalarGridSpec(num_scalar_...]
    ppermute x10 -> x11, starting transfers between devices: 36.1 us -> 36.7 us  [shift(): return lax.ppermute(x, 'tp', [(a, (a + d) % TP) for a in range(TP)])]
  transfers between devices with their start and end apart: 12 -> 13, of which waited for: 5 -> 6; matrix products, arithmetic and copies ran while one was open for 0% -> 0% of each run, Pallas kernels for 9% -> 9%
where the time goes in v2:
time: 184 us; the launch traced here: 183 us
  waiting for transfers between devices  69.1 us (38%)
  starting transfers between devices  67.9 us (37%)
  Pallas kernels  27.8 us (15%)
  blocking collectives  14.2 us (8%)
  local copies, waits for them, and re-layouts  3.02 us (2%)
    ppermute x11, waiting for transfers between devices, shift(): return lax.ppermute(x, 'tp', [(a, (a + d) % TP) for a in range(TP)])  69.1 us
    ppermute x11, starting transfers between devices, shift(): return lax.ppermute(x, 'tp', [(a, (a + d) % TP) for a in range(TP)])  36.7 us
    pallas_call x8, Pallas kernels, call(): pl.pallas_call(kernel, grid_spec=pltpu.PrefetchScalarGridSpec(num_scalar_...  27.8 us
    all_to_all x1, starting transfers between devices, layer(): lax.all_to_all(send.reshape(EXPERTS, 8, 2 * CH + 128), EP, 0, 0, tiled=True)  17.4 us
    all_to_all x1, blocking collectives, layer(): parts = lax.all_to_all(parts, 'tp', 0, 0, tiled=True)  14.2 us
    all_to_all x1, starting transfers between devices, layer(): lax.all_to_all(send_back.reshape(EXPERTS, 8, 2 * CH + 128), EP, 0, 0, til...  13.9 us
  transfers between devices with their start and end apart: 13, of which 6 were waited for; matrix products, arithmetic and copies ran while one was open for 0% of the time, Pallas kernels for 9%

profile of v2, /device:TPU:8, one launch (start us, length us, event | category | flops | bytes accessed | tf_op | source)
XLA Modules:
  0.0 183.1 jit_solution(5281155364908655982)
XLA Ops:
  0.7 4.2 %shard_map.142 = (bf16[1024,640]{1,0:T(8,128)(2,1)}, bf16[128,128]{1,0:T(8,128)(2,1)}, bf16[128,128]{1,0:T(8,128)(2,1)}, f32[8,128]{1,0:T(8,128)}) custom-call(s32[2]{0:T(128)S(1)} %pad_add_fusion.sc, bf16[128,2048]{1,0:T(8,128)(2,1)} %tok.1, bf16[128,2048]{1,0:T(8,128)(2,1)} %cot.1, s32[2,128]{1,0:T(2,128)} %bitcast.18, bf16[2048,128]{1,0:T(8,128)(2,1)} %router.3), custom_call_target="tpu_custom_call" | custom-call | tf_op jit(solution)/shard_map/pallas_call | solution.py:79
  4.9 17.4 %all-to-all-start = ((bf16[128,8,640]{2,1,0:T(8,128)(2,1)}), bf16[128,8,640]{2,1,0:T(8,128)(2,1)S(1)}, u32[]{:S(2)}, u32[]{:S(2)}) async-start(bf16[128,8,640]{2,1,0:T(8,128)(2,1)} %bitcast.21), calls=%async_computation | async-start | bytes 2621440 | tf_op jit(solution)/shard_map/all_to_all | solution.py:374
  22.3 3.4 %shard_map.144.own = bf16[2048,384]{1,0:T(8,128)(2,1)} custom-call(s32[2]{0:T(128)S(1)} %pad_add_fusion.sc, bf16[2048,128]{1,0:T(8,128)(2,1)} %bitcast.22, bf16[2048,128]{1,0:T(8,128)(2,1)} %bitcast.23, bf16[128,2048]{1,0:T(8,128)(2,1)} %bitcast.24), custom_call_target="tpu_custom_call" | custom-call | tf_op jit(solution)/shard_map/pallas_call | solution.py:79
  25.7 3.4 %collective-permute-start = (bf16[2048,384]{1,0:T(8,128)(2,1)}, bf16[2048,384]{1,0:T(8,128)(2,1)S(1)}, u32[]{:S(2)}, u32[]{:S(2)}) collective-permute-start(bf16[2048,384]{1,0:T(8,128)(2,1)} %shard_map.144.own), channel_id=1, source_target_pairs={{0,1},{1,2},{2,3},{3,0},{4,5},{5,6},{6,7},{7,4},{8,9},{9,10},{10,1... | collective-permute-start | bytes 4718600 | tf_op jit(solution)/shard_map/ppermute | solution.py:349
  29.1 3.7 %collective-permute-start.2 = (bf16[2048,384]{1,0:T(8,128)(2,1)}, bf16[2048,384]{1,0:T(8,128)(2,1)S(1)}, u32[]{:S(2)}, u32[]{:S(2)}) collective-permute-start(bf16[2048,384]{1,0:T(8,128)(2,1)} %shard_map.144.own), channel_id=1, source_target_pairs={{0,3},{1,0},{2,1},{3,2},{4,7},{5,4},{6,5},{7,6},{8,11},{9,8},{10,9... | collective-permute-start | bytes 4718600 | tf_op jit(solution)/shard_map/ppermute | solution.py:349
  32.8 32.7 %collective-permute-done.below = bf16[2048,384]{1,0:T(8,128)(2,1)S(1)} collective-permute-done((bf16[2048,384]{1,0:T(8,128)(2,1)}, bf16[2048,384]{1,0:T(8,128)(2,1)S(1)}, u32[]{:S(2)}, u32[]{:S(2)}) %collective-permute-start) | collective-permute-done | bytes 1572896 | tf_op jit(solution)/shard_map/ppermute | solution.py:349
  65.5 2.2 %collective-permute-start.1 = (bf16[1024,384]{1,0:T(8,128)(2,1)S(1)}, bf16[1024,384]{1,0:T(8,128)(2,1)}, u32[]{:S(2)}, u32[]{:S(2)}) collective-permute-start(bf16[1024,384]{1,0:T(8,128)(2,1)S(1)} %slice.16), channel_id=1, source_target_pairs={{0,1},{1,2},{2,3},{3,0},{4,5},{5,6},{6,7},{7,4},{8,9},{9,10},{10,1... | collective-permute-start | bytes 2359304 | tf_op jit(solution)/shard_map/ppermute | solution.py:349
  67.8 1.0 copy-done.8
  68.9 4.9 %collective-permute-start.3 = (bf16[1024,384]{1,0:T(8,128)(2,1)S(1)}, bf16[1024,384]{1,0:T(8,128)(2,1)}, u32[]{:S(2)}, u32[]{:S(2)}) collective-permute-start(bf16[1024,384]{1,0:T(8,128)(2,1)S(1)} %slice.17), channel_id=1, source_target_pairs={{0,3},{1,0},{2,1},{3,2},{4,7},{5,4},{6,5},{7,6},{8,11},{9,8},{10,9... | collective-permute-start | bytes 2359304 | tf_op jit(solution)/shard_map/ppermute | solution.py:349
  73.7 2.2 %shard_map.143 = (bf16[128,4096]{1,0:T(8,128)(2,1)}, bf16[128,128]{1,0:T(8,128)(2,1)}) custom-call(s32[2]{0:T(128)S(1)} %pad_add_fusion.sc, bf16[1024,640]{1,0:T(8,128)(2,1)S(1)} %bitcast.17), custom_call_target="tpu_custom_call" | custom-call | tf_op jit(solution)/shard_map/pallas_call | solution.py:79
  76.0 5.8 %shard_map.145 = (bf16[128,384]{1,0:T(8,128)(2,1)}, bf16[128,384]{1,0:T(8,128)(2,1)}, bf16[128,384]{1,0:T(8,128)(2,1)}, f32[128,2048]{1,0:T(8,128)S(1)}, f32[128,128]{1,0:T(8,128)S(1)}) custom-call(s32[2]{0:T(128)S(1)} %pad_add_fusion.sc, bf16[128,4096]{1,0:T(8,128)(2,1)} %get-tuple-element.33.pair.refs_0_, bf16[128,128]{1,0:T(8,128)(2,1)} %get-tuple-element.34.info, ...), custom_call_target="tpu_custom_call" | custom-call | tf_op jit(solution)/shard_map/pallas_call | solution.py:79
  81.7 5.7 %collective-permute-done.1.wa = bf16[1024,384]{1,0:T(8,128)(2,1)} collective-permute-done((bf16[1024,384]{1,0:T(8,128)(2,1)S(1)}, bf16[1024,384]{1,0:T(8,128)(2,1)}, u32[]{:S(2)}, u32[]{:S(2)}) %collective-permute-start.1) | collective-permute-done | bytes 786464 | tf_op jit(solution)/shard_map/ppermute | solution.py:349
  87.4 2.2 %collective-permute-done.3.wb = bf16[1024,384]{1,0:T(8,128)(2,1)} collective-permute-done((bf16[1024,384]{1,0:T(8,128)(2,1)S(1)}, bf16[1024,384]{1,0:T(8,128)(2,1)}, u32[]{:S(2)}, u32[]{:S(2)}) %collective-permute-start.3) | collective-permute-done | bytes 786464 | tf_op jit(solution)/shard_map/ppermute | solution.py:349
  89.6 4.7 %shard_map.146 = (bf16[128,384]{1,0:T(8,128)(2,1)}, bf16[1024,640]{1,0:T(8,128)(2,1)}) custom-call(s32[2]{0:T(128)S(1)} %pad_add_fusion.sc, bf16[128,4096]{1,0:T(8,128)(2,1)} %get-tuple-element.33.pair.refs_0_, bf16[128,128]{1,0:T(8,128)(2,1)} %get-tuple-element.34.info, bf16[1024,384]{1,0:T(8,128)(2,1)} %collective-permute-done.1.wa, ...), custom_call_target="tpu_custom_call" | custom-call | tf_op jit(solution)/shard_map/pallas_call | solution.py:79
  94.3 13.9 %all-to-all-start.1 = ((bf16[128,8,640]{2,1,0:T(8,128)(2,1)}), bf16[128,8,640]{2,1,0:T(8,128)(2,1)S(1)}, u32[]{:S(2)}, u32[]{:S(2)}) async-start(bf16[128,8,640]{2,1,0:T(8,128)(2,1)} %bitcast.20), calls=%async_computation.1 | async-start | bytes 2621440 | tf_op jit(solution)/shard_map/all_to_all | solution.py:406
  108.3 3.2 %collective-permute-start.4 = (bf16[128,4096]{1,0:T(8,128)(2,1)S(1)}, bf16[128,4096]{1,0:T(8,128)(2,1)S(1)}, u32[]{:S(2)}, u32[]{:S(2)}) collective-permute-start(bf16[128,4096]{1,0:T(8,128)(2,1)S(1)} %copy-done.6), channel_id=1, source_target_pairs={{0,1},{1,2},{2,3},{3,0},{4,5},{5,6},{6,7},{7,4},{8,9},{9,10},{10,1... | collective-permute-start | bytes 3145736 | tf_op jit(solution)/shard_map/ppermute | solution.py:349
  111.4 4.6 %collective-permute-start.6 = (bf16[128,4096]{1,0:T(8,128)(2,1)S(1)}, bf16[128,4096]{1,0:T(8,128)(2,1)S(1)}, u32[]{:S(2)}, u32[]{:S(2)}) collective-permute-start(bf16[128,4096]{1,0:T(8,128)(2,1)S(1)} %copy-done.6), channel_id=1, source_target_pairs={{0,3},{1,0},{2,1},{3,2},{4,7},{5,4},{6,5},{7,6},{8,11},{9,8},{10,9... | collective-permute-start | bytes 3145736 | tf_op jit(solution)/shard_map/ppermute | solution.py:349
  116.0 21.5 %collective-permute-done.4.refs_1_ = bf16[128,4096]{1,0:T(8,128)(2,1)S(1)} collective-permute-done((bf16[128,4096]{1,0:T(8,128)(2,1)S(1)}, bf16[128,4096]{1,0:T(8,128)(2,1)S(1)}, u32[]{:S(2)}, u32[]{:S(2)}) %collective-permute-start.4) | collective-permute-done | bytes 1048608 | tf_op jit(solution)/shard_map/ppermute | solution.py:349
  137.6 1.9 %collective-permute-start.5 = (bf16[64,4096]{1,0:T(8,128)(2,1)S(1)}, bf16[64,4096]{1,0:T(8,128)(2,1)S(1)}, u32[]{:S(2)}, u32[]{:S(2)}) collective-permute-start(bf16[64,4096]{1,0:T(8,128)(2,1)S(1)} %slice.18), channel_id=1, source_target_pairs={{0,1},{1,2},{2,3},{3,0},{4,5},{5,6},{6,7},{7,4},{8,9},{9,10},{10,1... | collective-permute-start | bytes 1572872 | tf_op jit(solution)/shard_map/ppermute | solution.py:349
  139.6 5.1 %collective-permute-start.7 = (bf16[64,4096]{1,0:T(8,128)(2,1)S(1)}, bf16[64,4096]{1,0:T(8,128)(2,1)S(1)}, u32[]{:S(2)}, u32[]{:S(2)}) collective-permute-start(bf16[64,4096]{1,0:T(8,128)(2,1)S(1)} %slice.19), channel_id=1, source_target_pairs={{0,3},{1,0},{2,1},{3,2},{4,7},{5,4},{6,5},{7,6},{8,11},{9,8},{10,9... | collective-permute-start | bytes 1572872 | tf_op jit(solution)/shard_map/ppermute | solution.py:349
  144.7 1.9 %collective-permute-start.9 = (bf16[128,384]{1,0:T(8,128)(2,1)S(1)}, bf16[128,384]{1,0:T(8,128)(2,1)S(1)}, u32[]{:S(2)}, u32[]{:S(2)}) collective-permute-start(bf16[128,384]{1,0:T(8,128)(2,1)S(1)} %copy-done.18), channel_id=1, source_target_pairs={{0,2},{1,3},{2,0},{3,1},{4,6},{5,7},{6,4},{7,5},{8,10},{9,11},{10,... | collective-permute-start | bytes 294920 | tf_op jit(solution)/shard_map/ppermute | solution.py:349
  146.7 3.4 %collective-permute-start.10 = (bf16[128,384]{1,0:T(8,128)(2,1)S(1)}, bf16[128,384]{1,0:T(8,128)(2,1)S(1)}, u32[]{:S(2)}, u32[]{:S(2)}) collective-permute-start(bf16[128,384]{1,0:T(8,128)(2,1)S(1)} %copy-done.17), channel_id=1, source_target_pairs={{0,3},{1,0},{2,1},{3,2},{4,7},{5,4},{6,5},{7,6},{8,11},{9,8},{10,9... | collective-permute-start | bytes 294920 | tf_op jit(solution)/shard_map/ppermute | solution.py:349
  150.1 2.5 %collective-permute-start.8 = (bf16[128,384]{1,0:T(8,128)(2,1)S(1)}, bf16[128,384]{1,0:T(8,128)(2,1)S(1)}, u32[]{:S(2)}, u32[]{:S(2)}) collective-permute-start(bf16[128,384]{1,0:T(8,128)(2,1)S(1)} %copy-done.16), channel_id=1, source_target_pairs={{0,1},{1,2},{2,3},{3,0},{4,5},{5,6},{6,7},{7,4},{8,9},{9,10},{10,1... | collective-permute-start | bytes 294920 | tf_op jit(solution)/shard_map/ppermute | solution.py:349
  152.5 4.1 %collective-permute-done.9.refs_7_ = bf16[128,384]{1,0:T(8,128)(2,1)S(1)} collective-permute-done((bf16[128,384]{1,0:T(8,128)(2,1)S(1)}, bf16[128,384]{1,0:T(8,128)(2,1)S(1)}, u32[]{:S(2)}, u32[]{:S(2)}) %collective-permute-start.9) | collective-permute-done | bytes 98336 | tf_op jit(solution)/shard_map/ppermute | solution.py:349
  156.7 2.8 %collective-permute-done.10.refs_8_ = bf16[128,384]{1,0:T(8,128)(2,1)S(1)} collective-permute-done((bf16[128,384]{1,0:T(8,128)(2,1)S(1)}, bf16[128,384]{1,0:T(8,128)(2,1)S(1)}, u32[]{:S(2)}, u32[]{:S(2)}) %collective-permute-start.10) | collective-permute-done | bytes 98336 | tf_op jit(solution)/shard_map/ppermute | solution.py:349
  159.6 0.6 copy-done.14
  160.4 0.2 copy-done.12
  160.6 5.1 %shard_map.147 = (bf16[2048,128]{1,0:T(8,128)(2,1)}, bf16[2048,128]{1,0:T(8,128)(2,1)}, bf16[128,2048]{1,0:T(8,128)(2,1)}, f32[1,128]{1,0:T(1,128)}, bf16[16,512]{1,0:T(8,128)(2,1)}) custom-call(s32[2]{0:T(128)S(1)} %pad_add_fusion.sc, bf16[128,4096]{1,0:T(8,128)(2,1)} %get-tuple-element.33.pair.refs_0_, bf16[128,4096]{1,0:T(8,128)(2,1)} %copy-done.9, ...), custom_call_target="tpu_custom_call" | custom-call | tf_op jit(solution)/shard_map/pallas_call | solution.py:79
  165.7 0.7 copy-done.3
  166.4 1.0 shard_map.148
  167.4 14.2 %all_to_all.15.got = bf16[4,160,512]{2,1,0:T(8,128)(2,1)S(1)} all-to-all(bf16[4,160,512]{2,1,0:T(8,128)(2,1)S(1)} %shard_map.148), channel_id=1, replica_groups=mesh['ep_0'=8,'ep_1'=8,'ep_2'=2,'tp'=4] {'tp'}, dimensions={0} | all-to-all | bytes 1310720 | tf_op jit(solution)/shard_map/all_to_all | solution.py:428
  181.7 1.4 shard_map.149
  (46 shorter events, 0.6 us)
Async XLA Ops:
  4.9 68.8 %all-to-all-start = ((bf16[128,8,640]{2,1,0:T(8,128)(2,1)}), bf16[128,8,640]{2,1,0:T(8,128)(2,1)S(1)}, u32[]{:S(2)}, u32[]{:S(2)}) async-start(bf16[128,8,640]{2,1,0:T(8,128)(2,1)} %bitcast.21), calls=%async_computation | async-start | bytes 2621440 | tf_op jit(solution)/shard_map/all_to_all | solution.py:374
  25.7 39.7 %collective-permute-start = (bf16[2048,384]{1,0:T(8,128)(2,1)}, bf16[2048,384]{1,0:T(8,128)(2,1)S(1)}, u32[]{:S(2)}, u32[]{:S(2)}) collective-permute-start(bf16[2048,384]{1,0:T(8,128)(2,1)} %shard_map.144.own), channel_id=1, source_target_pairs={{0,1},{1,2},{2,3},{3,0},{4,5},{5,6},{6,7},{7,4},{8,9},{9,10},{10,1... | collective-permute-start | bytes 4718600 | tf_op jit(solution)/shard_map/ppermute | solution.py:349
  29.1 38.6 %collective-permute-start.2 = (bf16[2048,384]{1,0:T(8,128)(2,1)}, bf16[2048,384]{1,0:T(8,128)(2,1)S(1)}, u32[]{:S(2)}, u32[]{:S(2)}) collective-permute-start(bf16[2048,384]{1,0:T(8,128)(2,1)} %shard_map.144.own), channel_id=1, source_target_pairs={{0,3},{1,0},{2,1},{3,2},{4,7},{5,4},{6,5},{7,6},{8,11},{9,8},{10,9... | collective-permute-start | bytes 4718600 | tf_op jit(solution)/shard_map/ppermute | solution.py:349
  65.4 2.4 %copy-start.7 = (bf16[2048,384]{1,0:T(8,128)(2,1)}, bf16[2048,384]{1,0:T(8,128)(2,1)S(1)}, u32[]{:S(2)}) copy-start(bf16[2048,384]{1,0:T(8,128)(2,1)S(1)} %collective-permute-done.below) | copy-start | bytes 4718596
  65.5 21.9 %collective-permute-start.1 = (bf16[1024,384]{1,0:T(8,128)(2,1)S(1)}, bf16[1024,384]{1,0:T(8,128)(2,1)}, u32[]{:S(2)}, u32[]{:S(2)}) collective-permute-start(bf16[1024,384]{1,0:T(8,128)(2,1)S(1)} %slice.16), channel_id=1, source_target_pairs={{0,1},{1,2},{2,3},{3,0},{4,5},{5,6},{6,7},{7,4},{8,9},{9,10},{10,1... | collective-permute-start | bytes 2359304 | tf_op jit(solution)/shard_map/ppermute | solution.py:349
  67.7 1.1 copy-start.8
  68.9 20.8 %collective-permute-start.3 = (bf16[1024,384]{1,0:T(8,128)(2,1)S(1)}, bf16[1024,384]{1,0:T(8,128)(2,1)}, u32[]{:S(2)}, u32[]{:S(2)}) collective-permute-start(bf16[1024,384]{1,0:T(8,128)(2,1)S(1)} %slice.17), channel_id=1, source_target_pairs={{0,3},{1,0},{2,1},{3,2},{4,7},{5,4},{6,5},{7,6},{8,11},{9,8},{10,9... | collective-permute-start | bytes 2359304 | tf_op jit(solution)/shard_map/ppermute | solution.py:349
  94.3 13.9 %copy-start.6 = (bf16[128,4096]{1,0:T(8,128)(2,1)S(1)}, bf16[128,4096]{1,0:T(8,128)(2,1)}, u32[]{:S(2)}) copy-start(bf16[128,4096]{1,0:T(8,128)(2,1)} %get-tuple-element.33.pair.refs_0_) | copy-start | bytes 3145732
  94.3 71.3 %all-to-all-start.1 = ((bf16[128,8,640]{2,1,0:T(8,128)(2,1)}), bf16[128,8,640]{2,1,0:T(8,128)(2,1)S(1)}, u32[]{:S(2)}, u32[]{:S(2)}) async-start(bf16[128,8,640]{2,1,0:T(8,128)(2,1)} %bitcast.20), calls=%async_computation.1 | async-start | bytes 2621440 | tf_op jit(solution)/shard_map/all_to_all | solution.py:406
  108.2 36.5 %copy-start.18 = (bf16[128,384]{1,0:T(8,128)(2,1)S(1)}, bf16[128,384]{1,0:T(8,128)(2,1)}, u32[]{:S(2)}) copy-start(bf16[128,384]{1,0:T(8,128)(2,1)} %get-tuple-element.42) | copy-start | bytes 294916
  108.2 38.4 %copy-start.17 = (bf16[128,384]{1,0:T(8,128)(2,1)S(1)}, bf16[128,384]{1,0:T(8,128)(2,1)}, u32[]{:S(2)}) copy-start(bf16[128,384]{1,0:T(8,128)(2,1)} %get-tuple-element.43) | copy-start | bytes 294916
  108.3 41.8 %copy-start.16 = (bf16[128,384]{1,0:T(8,128)(2,1)S(1)}, bf16[128,384]{1,0:T(8,128)(2,1)}, u32[]{:S(2)}) copy-start(bf16[128,384]{1,0:T(8,128)(2,1)} %get-tuple-element.41) | copy-start | bytes 294916
  108.3 29.3 %collective-permute-start.4 = (bf16[128,4096]{1,0:T(8,128)(2,1)S(1)}, bf16[128,4096]{1,0:T(8,128)(2,1)S(1)}, u32[]{:S(2)}, u32[]{:S(2)}) collective-permute-start(bf16[128,4096]{1,0:T(8,128)(2,1)S(1)} %copy-done.6), channel_id=1, source_target_pairs={{0,1},{1,2},{2,3},{3,0},{4,5},{5,6},{6,7},{7,4},{8,9},{9,10},{10,1... | collective-permute-start | bytes 3145736 | tf_op jit(solution)/shard_map/ppermute | solution.py:349
  111.4 28.1 %collective-permute-start.6 = (bf16[128,4096]{1,0:T(8,128)(2,1)S(1)}, bf16[128,4096]{1,0:T(8,128)(2,1)S(1)}, u32[]{:S(2)}, u32[]{:S(2)}) collective-permute-start(bf16[128,4096]{1,0:T(8,128)(2,1)S(1)} %copy-done.6), channel_id=1, source_target_pairs={{0,3},{1,0},{2,1},{3,2},{4,7},{5,4},{6,5},{7,6},{8,11},{9,8},{10,9... | collective-permute-start | bytes 3145736 | tf_op jit(solution)/shard_map/ppermute | solution.py:349
  137.5 22.0 %copy-start.9 = (bf16[128,4096]{1,0:T(8,128)(2,1)}, bf16[128,4096]{1,0:T(8,128)(2,1)S(1)}, u32[]{:S(2)}) copy-start(bf16[128,4096]{1,0:T(8,128)(2,1)S(1)} %collective-permute-done.4.refs_1_) | copy-start | bytes 3145732
  137.6 21.9 %collective-permute-start.5 = (bf16[64,4096]{1,0:T(8,128)(2,1)S(1)}, bf16[64,4096]{1,0:T(8,128)(2,1)S(1)}, u32[]{:S(2)}, u32[]{:S(2)}) collective-permute-start(bf16[64,4096]{1,0:T(8,128)(2,1)S(1)} %slice.18), channel_id=1, source_target_pairs={{0,1},{1,2},{2,3},{3,0},{4,5},{5,6},{6,7},{7,4},{8,9},{9,10},{10,1... | collective-permute-start | bytes 1572872 | tf_op jit(solution)/shard_map/ppermute | solution.py:349
  139.5 20.0 %copy-start.10 = (bf16[128,4096]{1,0:T(8,128)(2,1)}, bf16[128,4096]{1,0:T(8,128)(2,1)S(1)}, u32[]{:S(2)}) copy-start(bf16[128,4096]{1,0:T(8,128)(2,1)S(1)} %collective-permute-done.6.refs_4_) | copy-start | bytes 3145732
  139.6 20.0 %collective-permute-start.7 = (bf16[64,4096]{1,0:T(8,128)(2,1)S(1)}, bf16[64,4096]{1,0:T(8,128)(2,1)S(1)}, u32[]{:S(2)}, u32[]{:S(2)}) collective-permute-start(bf16[64,4096]{1,0:T(8,128)(2,1)S(1)} %slice.19), channel_id=1, source_target_pairs={{0,3},{1,0},{2,1},{3,2},{4,7},{5,4},{6,5},{7,6},{8,11},{9,8},{10,9... | collective-permute-start | bytes 1572872 | tf_op jit(solution)/shard_map/ppermute | solution.py:349
  144.7 11.9 %collective-permute-start.9 = (bf16[128,384]{1,0:T(8,128)(2,1)S(1)}, bf16[128,384]{1,0:T(8,128)(2,1)S(1)}, u32[]{:S(2)}, u32[]{:S(2)}) collective-permute-start(bf16[128,384]{1,0:T(8,128)(2,1)S(1)} %copy-done.18), channel_id=1, source_target_pairs={{0,2},{1,3},{2,0},{3,1},{4,6},{5,7},{6,4},{7,5},{8,10},{9,11},{10,... | collective-permute-start | bytes 294920 | tf_op jit(solution)/shard_map/ppermute | solution.py:349
  146.7 12.8 %collective-permute-start.10 = (bf16[128,384]{1,0:T(8,128)(2,1)S(1)}, bf16[128,384]{1,0:T(8,128)(2,1)S(1)}, u32[]{:S(2)}, u32[]{:S(2)}) collective-permute-start(bf16[128,384]{1,0:T(8,128)(2,1)S(1)} %copy-done.17), channel_id=1, source_target_pairs={{0,3},{1,0},{2,1},{3,2},{4,7},{5,4},{6,5},{7,6},{8,11},{9,8},{10,9... | collective-permute-start | bytes 294920 | tf_op jit(solution)/shard_map/ppermute | solution.py:349
  150.1 9.5 %collective-permute-start.8 = (bf16[128,384]{1,0:T(8,128)(2,1)S(1)}, bf16[128,384]{1,0:T(8,128)(2,1)S(1)}, u32[]{:S(2)}, u32[]{:S(2)}) collective-permute-start(bf16[128,384]{1,0:T(8,128)(2,1)S(1)} %copy-done.16), channel_id=1, source_target_pairs={{0,1},{1,2},{2,3},{3,0},{4,5},{5,6},{6,7},{7,4},{8,9},{9,10},{10,1... | collective-permute-start | bytes 294920 | tf_op jit(solution)/shard_map/ppermute | solution.py:349
  156.7 2.9 %copy-start.13 = (bf16[128,384]{1,0:T(8,128)(2,1)}, bf16[128,384]{1,0:T(8,128)(2,1)S(1)}, u32[]{:S(2)}) copy-start(bf16[128,384]{1,0:T(8,128)(2,1)S(1)} %collective-permute-done.9.refs_7_) | copy-start | bytes 294916
  159.5 0.6 copy-start.14
  159.5 0.7 copy-start.15
  159.5 0.8 copy-start.11
  159.5 1.0 copy-start.12
  160.6 5.1 %copy-start.1 = (bf16[128,128]{1,0:T(8,128)(2,1)S(1)}, bf16[128,128]{1,0:T(8,128)(2,1)}, u32[]{:S(2)}) copy-start(bf16[128,128]{1,0:T(8,128)(2,1)} %get-tuple-element.38.hit0) | copy-start | bytes 98308
  160.6 5.1 %copy-start.2 = (bf16[128,128]{1,0:T(8,128)(2,1)S(1)}, bf16[128,128]{1,0:T(8,128)(2,1)}, u32[]{:S(2)}) copy-start(bf16[128,128]{1,0:T(8,128)(2,1)} %get-tuple-element.39.hit1) | copy-start | bytes 98308
  165.7 0.7 copy-start.3
  166.4 15.3 %copy-start = (bf16[2048,128]{1,0:T(8,128)(2,1)S(1)}, bf16[2048,128]{1,0:T(8,128)(2,1)}, u32[]{:S(2)}) copy-start(bf16[2048,128]{1,0:T(8,128)(2,1)} %router.3) | copy-start | bytes 1572868
  166.4 15.3 %copy-start.4 = (f32[8,128]{1,0:T(8,128)S(1)}, f32[8,128]{1,0:T(8,128)}, u32[]{:S(2)}) copy-start(f32[8,128]{1,0:T(8,128)} %get-tuple-element.45.stats) | copy-start | bytes 12292
  166.4 15.3 %copy-start.5 = (s32[128,2]{0,1:T(2,128)S(1)}, s32[128,2]{0,1:T(2,128)}, u32[]{:S(2)}) copy-start(s32[128,2]{0,1:T(2,128)} %param.9) | copy-start | bytes 3076

commit v3 on v2

--- a/solution.py
+++ b/solution.py
@@ -151,12 +151,6 @@
     )
 
 
-def pack_kernel(sc, gate, up, down, out):
-    out[:, 0:FQ] = gate[...]
-    out[:, FQ : 2 * FQ] = up[...]
-    out[:, 2 * FQ :] = down[...].T
-
-
 def rows_kernel(sc, got, pair, info, scratch):
     fill(scratch, got)
     for u in range(8):
@@ -167,17 +161,9 @@
             info[...] = part[:, 2 * CH :]
 
 
-def quarter(pair, about, parts, grads):
-    pre = None
-    back_raw = None
-    at = 0
-    for w in parts:
-        n = w.shape[0]
-        x = dot(pair[:, at : at + n], w[:, 0 : 2 * FQ])
-        y = dot(pair[:, D + at : D + at + n], w[:, 2 * FQ :])
-        pre = x if pre is None else pre + x
-        back_raw = y if back_raw is None else back_raw + y
-        at += n
+def quarter(pair, about, both, down, grads):
+    pre = dot(pair[:, 0:D], both)
+    back_raw = dot(pair[:, D:], down, 1, 1)
     pre_gate = pre[:, 0:FQ]
     pre_up = pre[:, FQ:]
     gating = about[:, 0:1] + about[:, 1:2] + about[:, 2:3]
@@ -190,35 +176,46 @@
     g_in = jnp.concatenate([scaled * pre_up * slope, scaled * activated], axis=1).astype(BF16)
     grads[:, 0 : 2 * FQ] = g_in
     grads[:, 2 * FQ :] = (gating * hidden).astype(BF16)
-    backs = [dot(g_in, w[:, 0 : 2 * FQ], 1, 1) for w in parts]
-    return gg, backs
-
-
-def three_kernel(sc, pair, info, own, above, below, grads0, grads1, grads3, back, gg_out, held, sems):
-    copies = [
-        pltpu.make_async_copy(w, held.at[k], sems.at[k]) for k, w in enumerate((own, above, below))
-    ]
-    for c in copies:
-        c.start()
+    return gg, dot(g_in, both, 1, 1)
+
+
+def three_kernel(sc, pair, info, *refs):
+    weights, outs = refs[0:9], refs[9:12]
+    back, gg_out, held, held_down, sems = refs[12:]
+    copies = []
+    for k in range(3):
+        gate, up, down = weights[3 * k : 3 * k + 3]
+        targets = (held.at[k, :, 0:FQ], held.at[k, :, FQ : 2 * FQ], held_down.at[k])
+        copies.append(
+            [
+                pltpu.make_async_copy(x, t, sems.at[3 * k + c])
+                for c, (x, t) in enumerate(zip((gate, up, down), targets))
+            ]
+        )
+        for c in copies[k]:
+            c.start()
     about = info[...].astype(F32)
     gg = None
-    for k, grads in enumerate((grads0, grads1, grads3)):
-        copies[k].wait()
-        part, backs = quarter(pair, about, (held.at[k],), grads)
+    for k, grads in enumerate(outs):
+        for c in copies[k]:
+            c.wait()
+        part, term = quarter(pair, about, held[k], held_down[k], grads)
         if gg is None:
             gg = part
-            back[...] = backs[0]
+            back[...] = term
         else:
             gg = gg + part
-            back[...] += backs[0]
+            back[...] += term
     gg_out[...] = jnp.broadcast_to(gg, (128, 128))
 
 
-def emit_kernel(sc, pair, info, wa, wb, back, gg_in, grads, send, scratch):
+def emit_kernel(sc, pair, info, gate, up_a, up_b, down, back, gg_in, grads, send, scratch):
     about = info[...].astype(F32)
-    gg, backs = quarter(pair, about, (wa, wb), grads)
+    up = jnp.concatenate([up_a[...], up_b[...]], axis=0)
+    both = jnp.concatenate([gate[...], up], axis=1)
+    gg, term = quarter(pair, about, both, down[...], grads)
     gg = gg + gg_in[:, 0:1]
-    term = back[...] + jnp.concatenate(backs, axis=1)
+    term = back[...] + term
     own = (about[:, 3:4] + about[:, 4:5] + about[:, 5:6]) * gg
     other = (about[:, 6:7] + about[:, 7:8] + about[:, 8:9]) * gg
     other_expert = about[:, 9:10].astype(jnp.int32)
@@ -248,9 +245,20 @@
     )
 
 
-def sums_kernel(sc, *refs):
-    pairs, grads = refs[0:5], refs[5:9]
-    gate, up, down, down_norms, norms = refs[9:]
+def hop_kernel(sc, pair_1, pair_3, grads_1, grads_3, out_1, out_3):
+    for out, rows, grads in ((out_1, pair_1[0:64, :], grads_1), (out_3, pair_3[64:, :], grads_3)):
+        out[:, 0 : 2 * D] = rows
+        for h in range(2):
+            at = 2 * D + 3 * FQ * h
+            out[:, at : at + 3 * FQ] = grads[64 * h : 64 * (h + 1), :]
+
+
+def sums_kernel(sc, pair, pair_1, pair_3, hop_1, hop_3, grads_0, grads_2, *outs):
+    gate, up, down, down_norms, norms = outs
+    pairs = [pair[...], pair_1[...], hop_1[:, 0 : 2 * D], hop_3[:, 0 : 2 * D], pair_3[...]]
+    grads = [grads_0[...]]
+    halves = [slice(2 * D + 3 * FQ * h, 2 * D + 3 * FQ * (h + 1)) for h in range(2)]
+    grads += [hop_1[:, at] for at in halves] + [grads_2[...]] + [hop_3[:, at] for at in halves]
     toks = jnp.concatenate([x[:, 0:D] for x in pairs], axis=0)
     cots = jnp.concatenate([x[:, D:] for x in pairs], axis=0)
     g_in = jnp.concatenate([g[:, 0 : 2 * FQ] for g in grads], axis=0)
@@ -348,16 +356,16 @@
     def shift(x, d):
         return lax.ppermute(x, "tp", [(a, (a + d) % TP) for a in range(TP)])
 
-    (packed,) = call(
-        pack_kernel,
-        sc,
-        (whole(far(gate_w)), whole(far(up_w)), whole(far(down_w))),
-        (hbm((D, 3 * FQ), BF16),),
-    )
-    from_below = shift(packed, 1)
-    from_above = shift(packed, 3)
-    far_a = shift(from_below[0 : D // 2], 1)
-    far_b = shift(from_above[D // 2 :], 3)
+    gate_1 = shift(gate_w, 1)
+    down_3 = shift(down_w, 3)
+    up_1 = shift(up_w, 1)
+    up_3 = shift(up_w, 3)
+    gate_2 = shift(gate_1, 1)
+    down_2 = shift(down_3, 3)
+    down_1 = shift(down_w, 1)
+    gate_3 = shift(gate_w, 3)
+    up_2a = shift(up_1[0 : D // 2], 1)
+    up_2b = shift(up_3[D // 2 :], 3)
 
     send, hit0, hit1, stats = call(
         dispatch_kernel,
@@ -376,52 +384,60 @@
         rows_kernel,
         sc,
         (got.reshape(SENT, 2 * CH + 128),),
-        (hbm((128, 2 * D), BF16), hbm((128, 128), BF16)),
+        (vmem((128, 2 * D), BF16), hbm((128, 128), BF16)),
         (pltpu.VMEM((2 * CH // 128 + 1, SENT, 128), F32),),
     )
     pair_1 = shift(pair, 1)
     pair_3 = shift(pair, 3)
-    top = shift(pair_1[0:64], 1)
-    bottom = shift(pair_3[64:], 3)
-    pairs = [pair, pair_1, top, bottom, pair_3]
     quarter_grads = hbm((128, 3 * FQ), BF16)
     grads = [None] * TP
+    in_place = pl.BlockSpec(memory_space=pltpu.HBM)
+    weights = (gate_w, up_w, down_w, gate_3, up_3, down_3, gate_1, up_1, down_1)
     grads[0], grads[1], grads[3], back, gg = call(
         three_kernel,
         sc,
+        (pair, whole(far(info)), *((far(x), in_place) for x in weights)),
+        (quarter_grads,) * 3 + (vmem((128, D), F32), vmem((128, 128), F32)),
         (
-            *(whole(far(x)) for x in (pair, info)),
-            *((far(x), pl.BlockSpec(memory_space=pltpu.HBM)) for x in (packed, from_above, from_below)),
-        ),
-        (quarter_grads,) * 3 + (vmem((128, D), F32), vmem((128, 128), F32)),
-        (pltpu.VMEM((3, D, 3 * FQ), BF16), pltpu.SemaphoreType.DMA((3,))),
+            pltpu.VMEM((3, D, 2 * FQ), BF16),
+            pltpu.VMEM((3, FQ, D), BF16),
+            pltpu.SemaphoreType.DMA((9,)),
+        ),
     )
     grads[2], send_back = call(
         emit_kernel,
         sc,
-        (*(whole(far(x)) for x in (pair, info, far_a, far_b)), back, gg),
+        (pair, *(whole(far(x)) for x in (info, gate_2, up_2a, up_2b, down_2)), back, gg),
         (quarter_grads, hbm((SENT, 2 * CH + 128), BF16)),
         (pltpu.VMEM((CH // 128, SENT, 128), F32),),
     )
     home = lax.all_to_all(send_back.reshape(EXPERTS, 8, 2 * CH + 128), EP, 0, 0, tiled=True)
     home = home.reshape(SENT, 2 * CH + 128)
-    grads = [grads[0]] + [shift(grads[d], d) for d in (1, 2, 3)]
+    hops = call(
+        hop_kernel,
+        sc,
+        tuple(whole(far(x)) for x in (pair_1, pair_3, grads[1], grads[3])),
+        (hbm((64, 2 * D + 6 * FQ), BF16),) * 2,
+    )
+    hop_1 = shift(hops[0], 1)
+    hop_3 = shift(hops[1], 3)
+    grads_2 = shift(grads[2], 2)
     grad_gate, grad_up, grad_down, down_norms, norms = call(
         sums_kernel,
         sc,
-        tuple(whole(far(x)) for x in (*pairs, *grads)),
+        tuple(whole(far(x)) for x in (pair, pair_1, pair_3, hop_1, hop_3, grads[0], grads_2)),
         (
             sds((D, FQ), BF16),
             sds((D, FQ), BF16),
             sds((FQ, D), BF16),
             sds((1, FQ), F32),
-            hbm((16, 4 * 128), BF16),
+            vmem((16, 4 * 128), BF16),
         ),
     )
     (parts,) = call(
         home_kernel,
         sc,
-        (home, whole(hit0), whole(hit1), whole(norms)),
+        (home, whole(hit0), whole(hit1), norms),
         (vmem((TP, TOK + 32, DQ), BF16),),
         (pltpu.VMEM((2 * CH // 128 + 1, SENT, 128), F32),),
     )

time: 184 us -> 181 us (0.984)
  waiting for transfers between devices: 69.1 us -> 54.2 us
  starting transfers between devices: 67.9 us -> 80.7 us
    ppermute x11 -> x15, waiting for transfers between devices: 69.1 us -> 54.2 us  [shift(): return lax.ppermute(x, 'tp', [(a, (a + d) % TP) for a in range(TP)])]
    ppermute x11 -> x15, starting transfers between devices: 36.7 us -> 49.5 us  [shift(): return lax.ppermute(x, 'tp', [(a, (a + d) % TP) for a in range(TP)])]
  transfers between devices with their start and end apart: 13 -> 17, of which waited for: 6 -> 9; matrix products, arithmetic and copies ran while one was open for 0% -> 1% of each run, Pallas kernels for 9% -> 8%
where the time goes in v3:
time: 181 us; the launch traced here: 180 us
  starting transfers between devices  80.7 us (45%)
  waiting for transfers between devices  54.2 us (30%)
  Pallas kernels  26.3 us (15%)
  blocking collectives  13.4 us (7%)
  local copies, waits for them, and re-layouts  4.11 us (2%)
    ppermute x15, waiting for transfers between devices, shift(): return lax.ppermute(x, 'tp', [(a, (a + d) % TP) for a in range(TP)])  54.2 us
    ppermute x15, starting transfers between devices, shift(): return lax.ppermute(x, 'tp', [(a, (a + d) % TP) for a in range(TP)])  49.5 us
    pallas_call x8, Pallas kernels, call(): pl.pallas_call(kernel, grid_spec=pltpu.PrefetchScalarGridSpec(num_scalar_...  26.3 us
    all_to_all x1, starting transfers between devices, layer(): lax.all_to_all(send.reshape(EXPERTS, 8, 2 * CH + 128), EP, 0, 0, tiled=True)  17.5 us
    all_to_all x1, starting transfers between devices, layer(): lax.all_to_all(send_back.reshape(EXPERTS, 8, 2 * CH + 128), EP, 0, 0, til...  13.7 us
    all_to_all x1, blocking collectives, layer(): parts = lax.all_to_all(parts, 'tp', 0, 0, tiled=True)  13.4 us
  transfers between devices with their start and end apart: 17, of which 9 were waited for; matrix products, arithmetic and copies ran while one was open for 1% of the time, Pallas kernels for 8%

profile of v3, /device:TPU:8, one launch (start us, length us, event | category | flops | bytes accessed | tf_op | source)
XLA Modules:
  0.0 179.7 jit_solution(12699894502789086651)
XLA Ops:
  0.7 4.2 %shard_map.142 = (bf16[1024,640]{1,0:T(8,128)(2,1)}, bf16[128,128]{1,0:T(8,128)(2,1)}, bf16[128,128]{1,0:T(8,128)(2,1)}, f32[8,128]{1,0:T(8,128)}) custom-call(s32[2]{0:T(128)S(1)} %pad_add_fusion.sc, bf16[128,2048]{1,0:T(8,128)(2,1)} %tok.1, bf16[128,2048]{1,0:T(8,128)(2,1)} %cot.1, s32[2,128]{1,0:T(2,128)} %bitcast.18, bf16[2048,128]{1,0:T(8,128)(2,1)} %router.3), custom_call_target="tpu_custom_call" | custom-call | tf_op jit(solution)/shard_map/pallas_call | solution.py:79
  4.9 17.5 %all-to-all-start = ((bf16[128,8,640]{2,1,0:T(8,128)(2,1)}), bf16[128,8,640]{2,1,0:T(8,128)(2,1)S(1)}, u32[]{:S(2)}, u32[]{:S(2)}) async-start(bf16[128,8,640]{2,1,0:T(8,128)(2,1)} %bitcast.21), calls=%async_computation | async-start | bytes 2621440 | tf_op jit(solution)/shard_map/all_to_all | solution.py:382
  22.4 3.4 %collective-permute-start = (bf16[2048,128]{1,0:T(8,128)(2,1)S(1)}, bf16[2048,128]{1,0:T(8,128)(2,1)}, u32[]{:S(2)}, u32[]{:S(2)}) collective-permute-start(bf16[2048,128]{1,0:T(8,128)(2,1)S(1)} %bitcast.23), channel_id=1, source_target_pairs={{0,1},{1,2},{2,3},{3,0},{4,5},{5,6},{6,7},{7,4},{8,9},{9,10},{10,1... | collective-permute-start | bytes 1572872 | tf_op jit(solution)/shard_map/ppermute | solution.py:357
  25.9 3.7 %collective-permute-start.4 = (bf16[2048,128]{1,0:T(8,128)(2,1)S(1)}, bf16[2048,128]{1,0:T(8,128)(2,1)S(1)}, u32[]{:S(2)}, u32[]{:S(2)}) collective-permute-start(bf16[2048,128]{1,0:T(8,128)(2,1)S(1)} %bitcast.26), channel_id=1, source_target_pairs={{0,3},{1,0},{2,1},{3,2},{4,7},{5,4},{6,5},{7,6},{8,11},{9,8},{10,9... | collective-permute-start | bytes 1572872 | tf_op jit(solution)/shard_map/ppermute | solution.py:357
  29.5 3.5 %collective-permute-start.6 = (bf16[128,2048]{1,0:T(8,128)(2,1)}, bf16[128,2048]{1,0:T(8,128)(2,1)}, u32[]{:S(2)}, u32[]{:S(2)}) collective-permute-start(bf16[128,2048]{1,0:T(8,128)(2,1)} %bitcast.7.refs_2_), channel_id=1, source_target_pairs={{0,3},{1,0},{2,1},{3,2},{4,7},{5,4},{6,5},{7,6},{8,11},{9,8},{10,9... | collective-permute-start | bytes 1572872 | tf_op jit(solution)/shard_map/ppermute | solution.py:357
  33.0 2.4 %collective-permute-start.2 = (bf16[2048,128]{1,0:T(8,128)(2,1)S(1)}, bf16[2048,128]{1,0:T(8,128)(2,1)S(1)}, u32[]{:S(2)}, u32[]{:S(2)}) collective-permute-start(bf16[2048,128]{1,0:T(8,128)(2,1)S(1)} %bitcast.27), channel_id=1, source_target_pairs={{0,1},{1,2},{2,3},{3,0},{4,5},{5,6},{6,7},{7,4},{8,9},{9,10},{10,1... | collective-permute-start | bytes 1572872 | tf_op jit(solution)/shard_map/ppermute | solution.py:357
  35.4 4.7 %collective-permute-start.8 = (bf16[2048,128]{1,0:T(8,128)(2,1)S(1)}, bf16[2048,128]{1,0:T(8,128)(2,1)S(1)}, u32[]{:S(2)}, u32[]{:S(2)}) collective-permute-start(bf16[2048,128]{1,0:T(8,128)(2,1)S(1)} %bitcast.24), channel_id=1, source_target_pairs={{0,3},{1,0},{2,1},{3,2},{4,7},{5,4},{6,5},{7,6},{8,11},{9,8},{10,9... | collective-permute-start | bytes 1572872 | tf_op jit(solution)/shard_map/ppermute | solution.py:357
  40.5 2.2 %collective-permute-start.9 = (bf16[128,2048]{1,0:T(8,128)(2,1)}, bf16[128,2048]{1,0:T(8,128)(2,1)}, u32[]{:S(2)}, u32[]{:S(2)}) collective-permute-start(bf16[128,2048]{1,0:T(8,128)(2,1)} %bitcast.7.refs_2_), channel_id=1, source_target_pairs={{0,1},{1,2},{2,3},{3,0},{4,5},{5,6},{6,7},{7,4},{8,9},{9,10},{10,1... | collective-permute-start | bytes 1572872 | tf_op jit(solution)/shard_map/ppermute | solution.py:357
  42.7 3.4 %collective-permute-start.1 = (bf16[2048,128]{1,0:T(8,128)(2,1)}, bf16[2048,128]{1,0:T(8,128)(2,1)}, u32[]{:S(2)}, u32[]{:S(2)}) collective-permute-start(bf16[2048,128]{1,0:T(8,128)(2,1)} %collective-permute-done.refs_6_), channel_id=1, source_target_pairs={{0,1},{1,2},{2,3},{3,0},{4,5},{5,6},{6,7},{7,4},{8,9},{9,10},{10,1... | collective-permute-start | bytes 1572872 | tf_op jit(solution)/shard_map/ppermute | solution.py:357
  46.1 7.8 %collective-permute-done.6.refs_5_ = bf16[128,2048]{1,0:T(8,128)(2,1)} collective-permute-done((bf16[128,2048]{1,0:T(8,128)(2,1)}, bf16[128,2048]{1,0:T(8,128)(2,1)}, u32[]{:S(2)}, u32[]{:S(2)}) %collective-permute-start.6) | collective-permute-done | bytes 524320 | tf_op jit(solution)/shard_map/ppermute | solution.py:357
  53.9 4.9 %collective-permute-start.7 = (bf16[128,2048]{1,0:T(8,128)(2,1)}, bf16[128,2048]{1,0:T(8,128)(2,1)}, u32[]{:S(2)}, u32[]{:S(2)}) collective-permute-start(bf16[128,2048]{1,0:T(8,128)(2,1)} %collective-permute-done.6.refs_5_), channel_id=1, source_target_pairs={{0,3},{1,0},{2,1},{3,2},{4,7},{5,4},{6,5},{7,6},{8,11},{9,8},{10,9... | collective-permute-start | bytes 1572872 | tf_op jit(solution)/shard_map/ppermute | solution.py:357
  59.5 2.2 %collective-permute-start.5 = (bf16[1024,128]{1,0:T(8,128)(2,1)}, bf16[1024,128]{1,0:T(8,128)(2,1)}, u32[]{:S(2)}, u32[]{:S(2)}) collective-permute-start(bf16[1024,128]{1,0:T(8,128)(2,1)} %slice.9), channel_id=1, source_target_pairs={{0,3},{1,0},{2,1},{3,2},{4,7},{5,4},{6,5},{7,6},{8,11},{9,8},{10,9... | collective-permute-start | bytes 786440 | tf_op jit(solution)/shard_map/ppermute | solution.py:357
  62.5 2.6 %collective-permute-done.8.refs_3_ = bf16[2048,128]{1,0:T(8,128)(2,1)S(1)} collective-permute-done((bf16[2048,128]{1,0:T(8,128)(2,1)S(1)}, bf16[2048,128]{1,0:T(8,128)(2,1)S(1)}, u32[]{:S(2)}, u32[]{:S(2)}) %collective-permute-start.8) | collective-permute-done | bytes 524320 | tf_op jit(solution)/shard_map/ppermute | solution.py:357
  65.8 3.4 %collective-permute-start.3 = (bf16[1024,128]{1,0:T(8,128)(2,1)}, bf16[1024,128]{1,0:T(8,128)(2,1)}, u32[]{:S(2)}, u32[]{:S(2)}) collective-permute-start(bf16[1024,128]{1,0:T(8,128)(2,1)} %slice.8), channel_id=1, source_target_pairs={{0,1},{1,2},{2,3},{3,0},{4,5},{5,6},{6,7},{7,4},{8,9},{9,10},{10,1... | collective-permute-start | bytes 786440 | tf_op jit(solution)/shard_map/ppermute | solution.py:357
  69.2 1.4 shard_map.143
  70.6 5.5 %shard_map.144 = (bf16[128,384]{1,0:T(8,128)(2,1)}, bf16[128,384]{1,0:T(8,128)(2,1)}, bf16[128,384]{1,0:T(8,128)(2,1)}, f32[128,2048]{1,0:T(8,128)S(1)}, f32[128,128]{1,0:T(8,128)S(1)}) custom-call(s32[2]{0:T(128)S(1)} %pad_add_fusion.sc, bf16[128,4096]{1,0:T(8,128)(2,1)S(1)} %get-tuple-element.35.pair, bf16[128,128]{1,0:T(8,128)(2,1)} %get-tuple-element.36.info, ...), custom_call_target="tpu_custom_call" | custom-call | tf_op jit(solution)/shard_map/pallas_call | solution.py:79
  76.2 4.7 %collective-permute-done.5.up_b = bf16[1024,128]{1,0:T(8,128)(2,1)} collective-permute-done((bf16[1024,128]{1,0:T(8,128)(2,1)}, bf16[1024,128]{1,0:T(8,128)(2,1)}, u32[]{:S(2)}, u32[]{:S(2)}) %collective-permute-start.5) | collective-permute-done | bytes 262176 | tf_op jit(solution)/shard_map/ppermute | solution.py:357
  80.9 4.4 %shard_map.145 = (bf16[128,384]{1,0:T(8,128)(2,1)}, bf16[1024,640]{1,0:T(8,128)(2,1)}) custom-call(s32[2]{0:T(128)S(1)} %pad_add_fusion.sc, bf16[128,4096]{1,0:T(8,128)(2,1)S(1)} %get-tuple-element.35.pair, bf16[128,128]{1,0:T(8,128)(2,1)} %get-tuple-element.36.info, bf16[2048,128]{1,0:T(8,128)(2,1)} %collective-permute-done.1.gate, ...), custom_call_target="tpu_custom_call" | custom-call | tf_op jit(solution)/shard_map/pallas_call | solution.py:79
  85.3 13.7 %all-to-all-start.1 = ((bf16[128,8,640]{2,1,0:T(8,128)(2,1)}), bf16[128,8,640]{2,1,0:T(8,128)(2,1)S(1)}, u32[]{:S(2)}, u32[]{:S(2)}) async-start(bf16[128,8,640]{2,1,0:T(8,128)(2,1)} %bitcast.20), calls=%async_computation.1 | async-start | bytes 2621440 | tf_op jit(solution)/shard_map/all_to_all | solution.py:414
  99.0 5.0 %collective-permute-start.11 = (bf16[128,4096]{1,0:T(8,128)(2,1)S(1)}, bf16[128,4096]{1,0:T(8,128)(2,1)S(1)}, u32[]{:S(2)}, u32[]{:S(2)}) collective-permute-start(bf16[128,4096]{1,0:T(8,128)(2,1)S(1)} %get-tuple-element.35.pair), channel_id=1, source_target_pairs={{0,3},{1,0},{2,1},{3,2},{4,7},{5,4},{6,5},{7,6},{8,11},{9,8},{10,9... | collective-permute-start | bytes 3145736 | tf_op jit(solution)/shard_map/ppermute | solution.py:357
  104.0 1.9 %collective-permute-start.10 = (bf16[128,4096]{1,0:T(8,128)(2,1)S(1)}, bf16[128,4096]{1,0:T(8,128)(2,1)S(1)}, u32[]{:S(2)}, u32[]{:S(2)}) collective-permute-start(bf16[128,4096]{1,0:T(8,128)(2,1)S(1)} %get-tuple-element.35.pair), channel_id=1, source_target_pairs={{0,1},{1,2},{2,3},{3,0},{4,5},{5,6},{6,7},{7,4},{8,9},{9,10},{10,1... | collective-permute-start | bytes 3145736 | tf_op jit(solution)/shard_map/ppermute | solution.py:357
  105.9 20.7 %collective-permute-done.11.pair_3 = bf16[128,4096]{1,0:T(8,128)(2,1)S(1)} collective-permute-done((bf16[128,4096]{1,0:T(8,128)(2,1)S(1)}, bf16[128,4096]{1,0:T(8,128)(2,1)S(1)}, u32[]{:S(2)}, u32[]{:S(2)}) %collective-permute-start.11) | collective-permute-done | bytes 1048608 | tf_op jit(solution)/shard_map/ppermute | solution.py:357
  126.7 5.3 %collective-permute-done.10.pair_1 = bf16[128,4096]{1,0:T(8,128)(2,1)S(1)} collective-permute-done((bf16[128,4096]{1,0:T(8,128)(2,1)S(1)}, bf16[128,4096]{1,0:T(8,128)(2,1)S(1)}, u32[]{:S(2)}, u32[]{:S(2)}) %collective-permute-start.10) | collective-permute-done | bytes 1048608 | tf_op jit(solution)/shard_map/ppermute | solution.py:357
  133.0 3.2 %shard_map.146 = (bf16[64,4864]{1,0:T(8,128)(2,1)}, bf16[64,4864]{1,0:T(8,128)(2,1)}) custom-call(s32[2]{0:T(128)S(1)} %pad_add_fusion.sc, bf16[128,4096]{1,0:T(8,128)(2,1)} %copy-done.7, bf16[128,4096]{1,0:T(8,128)(2,1)} %copy-done.6, bf16[128,384]{1,0:T(8,128)(2,1)} %get-tuple-element.42.grads_1, bf16[128,384]{1,0:T(8,128)(2,1)} %get-tuple-element.43.grads_3), custom_call_target="tpu_custom_call" | custom-call | tf_op jit(solution)/shard_map/pallas_call | solution.py:79
  136.2 1.9 %collective-permute-start.12 = (bf16[64,4864]{1,0:T(8,128)(2,1)}, bf16[64,4864]{1,0:T(8,128)(2,1)S(1)}, u32[]{:S(2)}, u32[]{:S(2)}) collective-permute-start(bf16[64,4864]{1,0:T(8,128)(2,1)} %get-tuple-element.44), channel_id=1, source_target_pairs={{0,1},{1,2},{2,3},{3,0},{4,5},{5,6},{6,7},{7,4},{8,9},{9,10},{10,1... | collective-permute-start | bytes 1867784 | tf_op jit(solution)/shard_map/ppermute | solution.py:357
  138.1 5.1 %collective-permute-start.13 = (bf16[64,4864]{1,0:T(8,128)(2,1)}, bf16[64,4864]{1,0:T(8,128)(2,1)S(1)}, u32[]{:S(2)}, u32[]{:S(2)}) collective-permute-start(bf16[64,4864]{1,0:T(8,128)(2,1)} %get-tuple-element.45), channel_id=1, source_target_pairs={{0,3},{1,0},{2,1},{3,2},{4,7},{5,4},{6,5},{7,6},{8,11},{9,8},{10,9... | collective-permute-start | bytes 1867784 | tf_op jit(solution)/shard_map/ppermute | solution.py:357
  143.3 1.9 %collective-permute-start.14 = (bf16[128,384]{1,0:T(8,128)(2,1)S(1)}, bf16[128,384]{1,0:T(8,128)(2,1)S(1)}, u32[]{:S(2)}, u32[]{:S(2)}) collective-permute-start(bf16[128,384]{1,0:T(8,128)(2,1)S(1)} %copy-done.16), channel_id=1, source_target_pairs={{0,2},{1,3},{2,0},{3,1},{4,6},{5,7},{6,4},{7,5},{8,10},{9,11},{10,... | collective-permute-start | bytes 294920 | tf_op jit(solution)/shard_map/ppermute | solution.py:357
  145.2 9.2 %collective-permute-done.14.grads_2 = bf16[128,384]{1,0:T(8,128)(2,1)S(1)} collective-permute-done((bf16[128,384]{1,0:T(8,128)(2,1)S(1)}, bf16[128,384]{1,0:T(8,128)(2,1)S(1)}, u32[]{:S(2)}, u32[]{:S(2)}) %collective-permute-start.14) | collective-permute-done | bytes 98336 | tf_op jit(solution)/shard_map/ppermute | solution.py:357
  154.4 2.1 %collective-permute-done.12.hop_1 = bf16[64,4864]{1,0:T(8,128)(2,1)S(1)} collective-permute-done((bf16[64,4864]{1,0:T(8,128)(2,1)}, bf16[64,4864]{1,0:T(8,128)(2,1)S(1)}, u32[]{:S(2)}, u32[]{:S(2)}) %collective-permute-start.12) | collective-permute-done | bytes 622624 | tf_op jit(solution)/shard_map/ppermute | solution.py:357
  158.7 5.1 %shard_map.147 = (bf16[2048,128]{1,0:T(8,128)(2,1)}, bf16[2048,128]{1,0:T(8,128)(2,1)}, bf16[128,2048]{1,0:T(8,128)(2,1)}, f32[1,128]{1,0:T(1,128)}, bf16[16,512]{1,0:T(8,128)(2,1)S(1)}) custom-call(s32[2]{0:T(128)S(1)} %pad_add_fusion.sc, bf16[128,4096]{1,0:T(8,128)(2,1)} %copy-done, bf16[128,4096]{1,0:T(8,128)(2,1)} %copy-done.7, ...), custom_call_target="tpu_custom_call" | custom-call | tf_op jit(solution)/shard_map/pallas_call | solution.py:79
  164.8 13.4 %all_to_all.15.got = bf16[4,160,512]{2,1,0:T(8,128)(2,1)S(1)} all-to-all(bf16[4,160,512]{2,1,0:T(8,128)(2,1)S(1)} %shard_map.148), channel_id=1, replica_groups=mesh['ep_0'=8,'ep_1'=8,'ep_2'=2,'tp'=4] {'tp'}, dimensions={0} | all-to-all | bytes 1310720 | tf_op jit(solution)/shard_map/all_to_all | solution.py:444
  178.3 1.4 shard_map.149
  (48 shorter events, 6.9 us)
Async XLA Ops:
  4.9 17.5 %copy-start.12 = (bf16[1,2048,128]{2,1,0:T(8,128)(2,1)S(1)}, bf16[1,2048,128]{2,1,0:T(8,128)(2,1)}, u32[]{:S(2)}) copy-start(bf16[1,2048,128]{2,1,0:T(8,128)(2,1)} %param.11) | copy-start | bytes 1572868
  4.9 20.9 %copy-start.13 = (bf16[1,2048,128]{2,1,0:T(8,128)(2,1)S(1)}, bf16[1,2048,128]{2,1,0:T(8,128)(2,1)}, u32[]{:S(2)}) copy-start(bf16[1,2048,128]{2,1,0:T(8,128)(2,1)} %param.12) | copy-start | bytes 1572868
  4.9 64.3 %all-to-all-start = ((bf16[128,8,640]{2,1,0:T(8,128)(2,1)}), bf16[128,8,640]{2,1,0:T(8,128)(2,1)S(1)}, u32[]{:S(2)}, u32[]{:S(2)}) async-start(bf16[128,8,640]{2,1,0:T(8,128)(2,1)} %bitcast.21), calls=%async_computation | async-start | bytes 2621440 | tf_op jit(solution)/shard_map/all_to_all | solution.py:382
  22.4 18.0 %collective-permute-start = (bf16[2048,128]{1,0:T(8,128)(2,1)S(1)}, bf16[2048,128]{1,0:T(8,128)(2,1)}, u32[]{:S(2)}, u32[]{:S(2)}) collective-permute-start(bf16[2048,128]{1,0:T(8,128)(2,1)S(1)} %bitcast.23), channel_id=1, source_target_pairs={{0,1},{1,2},{2,3},{3,0},{4,5},{5,6},{6,7},{7,4},{8,9},{9,10},{10,1... | collective-permute-start | bytes 1572872 | tf_op jit(solution)/shard_map/ppermute | solution.py:357
  25.9 16.8 %collective-permute-start.4 = (bf16[2048,128]{1,0:T(8,128)(2,1)S(1)}, bf16[2048,128]{1,0:T(8,128)(2,1)S(1)}, u32[]{:S(2)}, u32[]{:S(2)}) collective-permute-start(bf16[2048,128]{1,0:T(8,128)(2,1)S(1)} %bitcast.26), channel_id=1, source_target_pairs={{0,3},{1,0},{2,1},{3,2},{4,7},{5,4},{6,5},{7,6},{8,11},{9,8},{10,9... | collective-permute-start | bytes 1572872 | tf_op jit(solution)/shard_map/ppermute | solution.py:357
  29.5 24.4 %collective-permute-start.6 = (bf16[128,2048]{1,0:T(8,128)(2,1)}, bf16[128,2048]{1,0:T(8,128)(2,1)}, u32[]{:S(2)}, u32[]{:S(2)}) collective-permute-start(bf16[128,2048]{1,0:T(8,128)(2,1)} %bitcast.7.refs_2_), channel_id=1, source_target_pairs={{0,3},{1,0},{2,1},{3,2},{4,7},{5,4},{6,5},{7,6},{8,11},{9,8},{10,9... | collective-permute-start | bytes 1572872 | tf_op jit(solution)/shard_map/ppermute | solution.py:357
  33.0 26.5 %collective-permute-start.2 = (bf16[2048,128]{1,0:T(8,128)(2,1)S(1)}, bf16[2048,128]{1,0:T(8,128)(2,1)S(1)}, u32[]{:S(2)}, u32[]{:S(2)}) collective-permute-start(bf16[2048,128]{1,0:T(8,128)(2,1)S(1)} %bitcast.27), channel_id=1, source_target_pairs={{0,1},{1,2},{2,3},{3,0},{4,5},{5,6},{6,7},{7,4},{8,9},{9,10},{10,1... | collective-permute-start | bytes 1572872 | tf_op jit(solution)/shard_map/ppermute | solution.py:357
  35.4 29.6 %collective-permute-start.8 = (bf16[2048,128]{1,0:T(8,128)(2,1)S(1)}, bf16[2048,128]{1,0:T(8,128)(2,1)S(1)}, u32[]{:S(2)}, u32[]{:S(2)}) collective-permute-start(bf16[2048,128]{1,0:T(8,128)(2,1)S(1)} %bitcast.24), channel_id=1, source_target_pairs={{0,3},{1,0},{2,1},{3,2},{4,7},{5,4},{6,5},{7,6},{8,11},{9,8},{10,9... | collective-permute-start | bytes 1572872 | tf_op jit(solution)/shard_map/ppermute | solution.py:357
  40.5 30.2 %collective-permute-start.9 = (bf16[128,2048]{1,0:T(8,128)(2,1)}, bf16[128,2048]{1,0:T(8,128)(2,1)}, u32[]{:S(2)}, u32[]{:S(2)}) collective-permute-start(bf16[128,2048]{1,0:T(8,128)(2,1)} %bitcast.7.refs_2_), channel_id=1, source_target_pairs={{0,1},{1,2},{2,3},{3,0},{4,5},{5,6},{6,7},{7,4},{8,9},{9,10},{10,1... | collective-permute-start | bytes 1572872 | tf_op jit(solution)/shard_map/ppermute | solution.py:357
  42.7 28.0 %copy-start.8 = (bf16[2048,128]{1,0:T(8,128)(2,1)}, bf16[2048,128]{1,0:T(8,128)(2,1)S(1)}, u32[]{:S(2)}) copy-start(bf16[2048,128]{1,0:T(8,128)(2,1)S(1)} %collective-permute-done.4.refs_4_) | copy-start | bytes 1572868
  42.7 38.2 %collective-permute-start.1 = (bf16[2048,128]{1,0:T(8,128)(2,1)}, bf16[2048,128]{1,0:T(8,128)(2,1)}, u32[]{:S(2)}, u32[]{:S(2)}) collective-permute-start(bf16[2048,128]{1,0:T(8,128)(2,1)} %collective-permute-done.refs_6_), channel_id=1, source_target_pairs={{0,1},{1,2},{2,3},{3,0},{4,5},{5,6},{6,7},{7,4},{8,9},{9,10},{10,1... | collective-permute-start | bytes 1572872 | tf_op jit(solution)/shard_map/ppermute | solution.py:357
  53.9 27.0 %collective-permute-start.7 = (bf16[128,2048]{1,0:T(8,128)(2,1)}, bf16[128,2048]{1,0:T(8,128)(2,1)}, u32[]{:S(2)}, u32[]{:S(2)}) collective-permute-start(bf16[128,2048]{1,0:T(8,128)(2,1)} %collective-permute-done.6.refs_5_), channel_id=1, source_target_pairs={{0,3},{1,0},{2,1},{3,2},{4,7},{5,4},{6,5},{7,6},{8,11},{9,8},{10,9... | collective-permute-start | bytes 1572872 | tf_op jit(solution)/shard_map/ppermute | solution.py:357
  59.5 11.2 %copy-start.9 = (bf16[2048,128]{1,0:T(8,128)(2,1)}, bf16[2048,128]{1,0:T(8,128)(2,1)S(1)}, u32[]{:S(2)}) copy-start(bf16[2048,128]{1,0:T(8,128)(2,1)S(1)} %collective-permute-done.2.refs_7_) | copy-start | bytes 1572868
  59.5 21.4 %collective-permute-start.5 = (bf16[1024,128]{1,0:T(8,128)(2,1)}, bf16[1024,128]{1,0:T(8,128)(2,1)}, u32[]{:S(2)}, u32[]{:S(2)}) collective-permute-start(bf16[1024,128]{1,0:T(8,128)(2,1)} %slice.9), channel_id=1, source_target_pairs={{0,3},{1,0},{2,1},{3,2},{4,7},{5,4},{6,5},{7,6},{8,11},{9,8},{10,9... | collective-permute-start | bytes 786440 | tf_op jit(solution)/shard_map/ppermute | solution.py:357
  65.8 15.0 %collective-permute-start.3 = (bf16[1024,128]{1,0:T(8,128)(2,1)}, bf16[1024,128]{1,0:T(8,128)(2,1)}, u32[]{:S(2)}, u32[]{:S(2)}) collective-permute-start(bf16[1024,128]{1,0:T(8,128)(2,1)} %slice.8), channel_id=1, source_target_pairs={{0,1},{1,2},{2,3},{3,0},{4,5},{5,6},{6,7},{7,4},{8,9},{9,10},{10,1... | collective-permute-start | bytes 786440 | tf_op jit(solution)/shard_map/ppermute | solution.py:357
  70.6 33.4 %copy-start = (bf16[128,4096]{1,0:T(8,128)(2,1)}, bf16[128,4096]{1,0:T(8,128)(2,1)S(1)}, u32[]{:S(2)}) copy-start(bf16[128,4096]{1,0:T(8,128)(2,1)S(1)} %get-tuple-element.35.pair) | copy-start | bytes 3145732
  85.3 78.5 %all-to-all-start.1 = ((bf16[128,8,640]{2,1,0:T(8,128)(2,1)}), bf16[128,8,640]{2,1,0:T(8,128)(2,1)S(1)}, u32[]{:S(2)}, u32[]{:S(2)}) async-start(bf16[128,8,640]{2,1,0:T(8,128)(2,1)} %bitcast.20), calls=%async_computation.1 | async-start | bytes 2621440 | tf_op jit(solution)/shard_map/all_to_all | solution.py:414
  99.0 44.3 %copy-start.16 = (bf16[128,384]{1,0:T(8,128)(2,1)S(1)}, bf16[128,384]{1,0:T(8,128)(2,1)}, u32[]{:S(2)}) copy-start(bf16[128,384]{1,0:T(8,128)(2,1)} %get-tuple-element.47) | copy-start | bytes 294916
  99.0 27.7 %collective-permute-start.11 = (bf16[128,4096]{1,0:T(8,128)(2,1)S(1)}, bf16[128,4096]{1,0:T(8,128)(2,1)S(1)}, u32[]{:S(2)}, u32[]{:S(2)}) collective-permute-start(bf16[128,4096]{1,0:T(8,128)(2,1)S(1)} %get-tuple-element.35.pair), channel_id=1, source_target_pairs={{0,3},{1,0},{2,1},{3,2},{4,7},{5,4},{6,5},{7,6},{8,11},{9,8},{10,9... | collective-permute-start | bytes 3145736 | tf_op jit(solution)/shard_map/ppermute | solution.py:357
  104.0 28.0 %collective-permute-start.10 = (bf16[128,4096]{1,0:T(8,128)(2,1)S(1)}, bf16[128,4096]{1,0:T(8,128)(2,1)S(1)}, u32[]{:S(2)}, u32[]{:S(2)}) collective-permute-start(bf16[128,4096]{1,0:T(8,128)(2,1)S(1)} %get-tuple-element.35.pair), channel_id=1, source_target_pairs={{0,1},{1,2},{2,3},{3,0},{4,5},{5,6},{6,7},{7,4},{8,9},{9,10},{10,1... | collective-permute-start | bytes 3145736 | tf_op jit(solution)/shard_map/ppermute | solution.py:357
  126.7 5.3 %copy-start.6 = (bf16[128,4096]{1,0:T(8,128)(2,1)}, bf16[128,4096]{1,0:T(8,128)(2,1)S(1)}, u32[]{:S(2)}) copy-start(bf16[128,4096]{1,0:T(8,128)(2,1)S(1)} %collective-permute-done.11.pair_3) | copy-start | bytes 3145732
  132.0 1.0 copy-start.7
  136.2 20.3 %collective-permute-start.12 = (bf16[64,4864]{1,0:T(8,128)(2,1)}, bf16[64,4864]{1,0:T(8,128)(2,1)S(1)}, u32[]{:S(2)}, u32[]{:S(2)}) collective-permute-start(bf16[64,4864]{1,0:T(8,128)(2,1)} %get-tuple-element.44), channel_id=1, source_target_pairs={{0,1},{1,2},{2,3},{3,0},{4,5},{5,6},{6,7},{7,4},{8,9},{9,10},{10,1... | collective-permute-start | bytes 1867784 | tf_op jit(solution)/shard_map/ppermute | solution.py:357
  138.1 19.7 %collective-permute-start.13 = (bf16[64,4864]{1,0:T(8,128)(2,1)}, bf16[64,4864]{1,0:T(8,128)(2,1)S(1)}, u32[]{:S(2)}, u32[]{:S(2)}) collective-permute-start(bf16[64,4864]{1,0:T(8,128)(2,1)} %get-tuple-element.45), channel_id=1, source_target_pairs={{0,3},{1,0},{2,1},{3,2},{4,7},{5,4},{6,5},{7,6},{8,11},{9,8},{10,9... | collective-permute-start | bytes 1867784 | tf_op jit(solution)/shard_map/ppermute | solution.py:357
  143.3 11.1 %collective-permute-start.14 = (bf16[128,384]{1,0:T(8,128)(2,1)S(1)}, bf16[128,384]{1,0:T(8,128)(2,1)S(1)}, u32[]{:S(2)}, u32[]{:S(2)}) collective-permute-start(bf16[128,384]{1,0:T(8,128)(2,1)S(1)} %copy-done.16), channel_id=1, source_target_pairs={{0,2},{1,3},{2,0},{3,1},{4,6},{5,7},{6,4},{7,5},{8,10},{9,11},{10,... | collective-permute-start | bytes 294920 | tf_op jit(solution)/shard_map/ppermute | solution.py:357
  154.4 3.4 %copy-start.15 = (bf16[128,384]{1,0:T(8,128)(2,1)}, bf16[128,384]{1,0:T(8,128)(2,1)S(1)}, u32[]{:S(2)}) copy-start(bf16[128,384]{1,0:T(8,128)(2,1)S(1)} %collective-permute-done.14.grads_2) | copy-start | bytes 294916
  156.5 1.3 copy-start.10
  158.7 5.1 %copy-start.2 = (bf16[128,128]{1,0:T(8,128)(2,1)S(1)}, bf16[128,128]{1,0:T(8,128)(2,1)}, u32[]{:S(2)}) copy-start(bf16[128,128]{1,0:T(8,128)(2,1)} %get-tuple-element.40.hit0) | copy-start | bytes 98308
  158.7 5.1 %copy-start.3 = (bf16[128,128]{1,0:T(8,128)(2,1)S(1)}, bf16[128,128]{1,0:T(8,128)(2,1)}, u32[]{:S(2)}) copy-start(bf16[128,128]{1,0:T(8,128)(2,1)} %get-tuple-element.41.hit1) | copy-start | bytes 98308
  163.8 14.5 %copy-start.1 = (bf16[2048,128]{1,0:T(8,128)(2,1)S(1)}, bf16[2048,128]{1,0:T(8,128)(2,1)}, u32[]{:S(2)}) copy-start(bf16[2048,128]{1,0:T(8,128)(2,1)} %router.3) | copy-start | bytes 1572868
  163.8 14.5 %copy-start.4 = (f32[8,128]{1,0:T(8,128)S(1)}, f32[8,128]{1,0:T(8,128)}, u32[]{:S(2)}) copy-start(f32[8,128]{1,0:T(8,128)} %get-tuple-element.49.stats) | copy-start | bytes 12292
  163.8 14.5 %copy-start.5 = (s32[128,2]{0,1:T(2,128)S(1)}, s32[128,2]{0,1:T(2,128)}, u32[]{:S(2)}) copy-start(s32[128,2]{0,1:T(2,128)} %param.9) | copy-start | bytes 3076
  (2 other events, 1.6 us)

commit v4 on v3

--- a/solution.py
+++ b/solution.py
@@ -245,20 +245,10 @@
     )
 
 
-def hop_kernel(sc, pair_1, pair_3, grads_1, grads_3, out_1, out_3):
-    for out, rows, grads in ((out_1, pair_1[0:64, :], grads_1), (out_3, pair_3[64:, :], grads_3)):
-        out[:, 0 : 2 * D] = rows
-        for h in range(2):
-            at = 2 * D + 3 * FQ * h
-            out[:, at : at + 3 * FQ] = grads[64 * h : 64 * (h + 1), :]
-
-
-def sums_kernel(sc, pair, pair_1, pair_3, hop_1, hop_3, grads_0, grads_2, *outs):
-    gate, up, down, down_norms, norms = outs
-    pairs = [pair[...], pair_1[...], hop_1[:, 0 : 2 * D], hop_3[:, 0 : 2 * D], pair_3[...]]
-    grads = [grads_0[...]]
-    halves = [slice(2 * D + 3 * FQ * h, 2 * D + 3 * FQ * (h + 1)) for h in range(2)]
-    grads += [hop_1[:, at] for at in halves] + [grads_2[...]] + [hop_3[:, at] for at in halves]
+def sums_kernel(sc, pair, pair_1, top, bottom, pair_3, *refs):
+    grads = refs[0:4]
+    gate, up, down, down_norms, norms = refs[4:]
+    pairs = (pair, pair_1, top, bottom, pair_3)
     toks = jnp.concatenate([x[:, 0:D] for x in pairs], axis=0)
     cots = jnp.concatenate([x[:, D:] for x in pairs], axis=0)
     g_in = jnp.concatenate([g[:, 0 : 2 * FQ] for g in grads], axis=0)
@@ -360,10 +350,10 @@
     down_3 = shift(down_w, 3)
     up_1 = shift(up_w, 1)
     up_3 = shift(up_w, 3)
+    down_1 = shift(down_w, 1)
+    gate_3 = shift(gate_w, 3)
     gate_2 = shift(gate_1, 1)
     down_2 = shift(down_3, 3)
-    down_1 = shift(down_w, 1)
-    gate_3 = shift(gate_w, 3)
     up_2a = shift(up_1[0 : D // 2], 1)
     up_2b = shift(up_3[D // 2 :], 3)
 
@@ -413,19 +403,15 @@
     )
     home = lax.all_to_all(send_back.reshape(EXPERTS, 8, 2 * CH + 128), EP, 0, 0, tiled=True)
     home = home.reshape(SENT, 2 * CH + 128)
-    hops = call(
-        hop_kernel,
-        sc,
-        tuple(whole(far(x)) for x in (pair_1, pair_3, grads[1], grads[3])),
-        (hbm((64, 2 * D + 6 * FQ), BF16),) * 2,
-    )
-    hop_1 = shift(hops[0], 1)
-    hop_3 = shift(hops[1], 3)
-    grads_2 = shift(grads[2], 2)
+    grads[2] = shift(grads[2], 2)
+    top = shift(pair_1[0:64], 1)
+    bottom = shift(pair_3[64:], 3)
+    grads[1] = shift(grads[1], 1)
+    grads[3] = shift(grads[3], 3)
     grad_gate, grad_up, grad_down, down_norms, norms = call(
         sums_kernel,
         sc,
-        tuple(whole(far(x)) for x in (pair, pair_1, pair_3, hop_1, hop_3, grads[0], grads_2)),
+        tuple(whole(far(x)) for x in (pair, pair_1, top, bottom, pair_3, *grads)),
         (
             sds((D, FQ), BF16),
             sds((D, FQ), BF16),

time: 181 us -> 174 us (0.961)
  waiting for transfers between devices: 54.2 us -> 43.9 us
  starting transfers between devices: 80.7 us -> 89.7 us
  Pallas kernels: 26.3 us -> 23 us
    ppermute x15 -> x17, waiting for transfers between devices: 54.2 us -> 43.9 us  [shift(): return lax.ppermute(x, 'tp', [(a, (a + d) % TP) for a in range(TP)])]
    ppermute x15 -> x17, starting transfers between devices: 49.5 us -> 58.5 us  [shift(): return lax.ppermute(x, 'tp', [(a, (a + d) % TP) for a in range(TP)])]
    pallas_call x8 -> x7, Pallas kernels: 26.3 us -> 23 us  [call(): pl.pallas_call(kernel, grid_spec=pltpu.PrefetchScalarGridSpec(num_scalar_...]
  transfers between devices with their start and end apart: 17 -> 19, of which waited for: 9 -> 7; matrix products, arithmetic and copies ran while one was open for 1% -> 1% of each run, Pallas kernels for 8% -> 7%
where the time goes in v4:
time: 174 us; the launch traced here: 173 us
  starting transfers between devices  89.7 us (52%)
  waiting for transfers between devices  43.9 us (25%)
  Pallas kernels  23 us (13%)
  blocking collectives  11.9 us (7%)
  local copies, waits for them, and re-layouts  3.37 us (2%)
    ppermute x17, starting transfers between devices, shift(): return lax.ppermute(x, 'tp', [(a, (a + d) % TP) for a in range(TP)])  58.5 us
    ppermute x17, waiting for transfers between devices, shift(): return lax.ppermute(x, 'tp', [(a, (a + d) % TP) for a in range(TP)])  43.9 us
    pallas_call x7, Pallas kernels, call(): pl.pallas_call(kernel, grid_spec=pltpu.PrefetchScalarGridSpec(num_scalar_...  23 us
    all_to_all x1, starting transfers between devices, layer(): lax.all_to_all(send.reshape(EXPERTS, 8, 2 * CH + 128), EP, 0, 0, tiled=True)  17.5 us
    all_to_all x1, starting transfers between devices, layer(): lax.all_to_all(send_back.reshape(EXPERTS, 8, 2 * CH + 128), EP, 0, 0, til...  13.7 us
    all_to_all x1, blocking collectives, layer(): parts = lax.all_to_all(parts, 'tp', 0, 0, tiled=True)  11.9 us
  transfers between devices with their start and end apart: 19, of which 7 were waited for; matrix products, arithmetic and copies ran while one was open for 1% of the time, Pallas kernels for 7%

profile of v4, /device:TPU:8, one launch (start us, length us, event | category | flops | bytes accessed | tf_op | source)
XLA Modules:
  0.0 173.1 jit_solution(10094949356762322)
XLA Ops:
  0.7 4.2 %shard_map.142 = (bf16[1024,640]{1,0:T(8,128)(2,1)}, bf16[128,128]{1,0:T(8,128)(2,1)}, bf16[128,128]{1,0:T(8,128)(2,1)}, f32[8,128]{1,0:T(8,128)}) custom-call(s32[2]{0:T(128)S(1)} %pad_add_fusion.sc, bf16[128,2048]{1,0:T(8,128)(2,1)} %tok.1, bf16[128,2048]{1,0:T(8,128)(2,1)} %cot.1, s32[2,128]{1,0:T(2,128)} %bitcast.18, bf16[2048,128]{1,0:T(8,128)(2,1)} %router.3), custom_call_target="tpu_custom_call" | custom-call | tf_op jit(solution)/shard_map/pallas_call | solution.py:79
  4.9 17.5 %all-to-all-start = ((bf16[128,8,640]{2,1,0:T(8,128)(2,1)}), bf16[128,8,640]{2,1,0:T(8,128)(2,1)S(1)}, u32[]{:S(2)}, u32[]{:S(2)}) async-start(bf16[128,8,640]{2,1,0:T(8,128)(2,1)} %bitcast.21), calls=%async_computation | async-start | bytes 2621440 | tf_op jit(solution)/shard_map/all_to_all | solution.py:372
  22.4 3.4 %collective-permute-start = (bf16[2048,128]{1,0:T(8,128)(2,1)S(1)}, bf16[2048,128]{1,0:T(8,128)(2,1)}, u32[]{:S(2)}, u32[]{:S(2)}) collective-permute-start(bf16[2048,128]{1,0:T(8,128)(2,1)S(1)} %bitcast.23), channel_id=1, source_target_pairs={{0,1},{1,2},{2,3},{3,0},{4,5},{5,6},{6,7},{7,4},{8,9},{9,10},{10,1... | collective-permute-start | bytes 1572872 | tf_op jit(solution)/shard_map/ppermute | solution.py:347
  25.8 3.7 %collective-permute-start.4 = (bf16[2048,128]{1,0:T(8,128)(2,1)S(1)}, bf16[2048,128]{1,0:T(8,128)(2,1)S(1)}, u32[]{:S(2)}, u32[]{:S(2)}) collective-permute-start(bf16[2048,128]{1,0:T(8,128)(2,1)S(1)} %bitcast.26), channel_id=1, source_target_pairs={{0,3},{1,0},{2,1},{3,2},{4,7},{5,4},{6,5},{7,6},{8,11},{9,8},{10,9... | collective-permute-start | bytes 1572872 | tf_op jit(solution)/shard_map/ppermute | solution.py:347
  29.5 3.5 %collective-permute-start.6 = (bf16[128,2048]{1,0:T(8,128)(2,1)}, bf16[128,2048]{1,0:T(8,128)(2,1)}, u32[]{:S(2)}, u32[]{:S(2)}) collective-permute-start(bf16[128,2048]{1,0:T(8,128)(2,1)} %bitcast.7.refs_2_), channel_id=1, source_target_pairs={{0,3},{1,0},{2,1},{3,2},{4,7},{5,4},{6,5},{7,6},{8,11},{9,8},{10,9... | collective-permute-start | bytes 1572872 | tf_op jit(solution)/shard_map/ppermute | solution.py:347
  33.0 2.4 %collective-permute-start.2 = (bf16[2048,128]{1,0:T(8,128)(2,1)S(1)}, bf16[2048,128]{1,0:T(8,128)(2,1)S(1)}, u32[]{:S(2)}, u32[]{:S(2)}) collective-permute-start(bf16[2048,128]{1,0:T(8,128)(2,1)S(1)} %bitcast.27), channel_id=1, source_target_pairs={{0,1},{1,2},{2,3},{3,0},{4,5},{5,6},{6,7},{7,4},{8,9},{9,10},{10,1... | collective-permute-start | bytes 1572872 | tf_op jit(solution)/shard_map/ppermute | solution.py:347
  35.4 4.7 %collective-permute-start.8 = (bf16[2048,128]{1,0:T(8,128)(2,1)S(1)}, bf16[2048,128]{1,0:T(8,128)(2,1)S(1)}, u32[]{:S(2)}, u32[]{:S(2)}) collective-permute-start(bf16[2048,128]{1,0:T(8,128)(2,1)S(1)} %bitcast.24), channel_id=1, source_target_pairs={{0,3},{1,0},{2,1},{3,2},{4,7},{5,4},{6,5},{7,6},{8,11},{9,8},{10,9... | collective-permute-start | bytes 1572872 | tf_op jit(solution)/shard_map/ppermute | solution.py:347
  40.4 2.2 %collective-permute-start.9 = (bf16[128,2048]{1,0:T(8,128)(2,1)}, bf16[128,2048]{1,0:T(8,128)(2,1)}, u32[]{:S(2)}, u32[]{:S(2)}) collective-permute-start(bf16[128,2048]{1,0:T(8,128)(2,1)} %bitcast.7.refs_2_), channel_id=1, source_target_pairs={{0,1},{1,2},{2,3},{3,0},{4,5},{5,6},{6,7},{7,4},{8,9},{9,10},{10,1... | collective-permute-start | bytes 1572872 | tf_op jit(solution)/shard_map/ppermute | solution.py:347
  42.6 3.4 %collective-permute-start.1 = (bf16[2048,128]{1,0:T(8,128)(2,1)}, bf16[2048,128]{1,0:T(8,128)(2,1)}, u32[]{:S(2)}, u32[]{:S(2)}) collective-permute-start(bf16[2048,128]{1,0:T(8,128)(2,1)} %collective-permute-done.refs_6_), channel_id=1, source_target_pairs={{0,1},{1,2},{2,3},{3,0},{4,5},{5,6},{6,7},{7,4},{8,9},{9,10},{10,1... | collective-permute-start | bytes 1572872 | tf_op jit(solution)/shard_map/ppermute | solution.py:347
  46.0 7.8 %collective-permute-done.6.refs_5_ = bf16[128,2048]{1,0:T(8,128)(2,1)} collective-permute-done((bf16[128,2048]{1,0:T(8,128)(2,1)}, bf16[128,2048]{1,0:T(8,128)(2,1)}, u32[]{:S(2)}, u32[]{:S(2)}) %collective-permute-start.6) | collective-permute-done | bytes 524320 | tf_op jit(solution)/shard_map/ppermute | solution.py:347
  53.9 4.9 %collective-permute-start.7 = (bf16[128,2048]{1,0:T(8,128)(2,1)}, bf16[128,2048]{1,0:T(8,128)(2,1)}, u32[]{:S(2)}, u32[]{:S(2)}) collective-permute-start(bf16[128,2048]{1,0:T(8,128)(2,1)} %collective-permute-done.6.refs_5_), channel_id=1, source_target_pairs={{0,3},{1,0},{2,1},{3,2},{4,7},{5,4},{6,5},{7,6},{8,11},{9,8},{10,9... | collective-permute-start | bytes 1572872 | tf_op jit(solution)/shard_map/ppermute | solution.py:347
  59.5 2.2 %collective-permute-start.5 = (bf16[1024,128]{1,0:T(8,128)(2,1)}, bf16[1024,128]{1,0:T(8,128)(2,1)}, u32[]{:S(2)}, u32[]{:S(2)}) collective-permute-start(bf16[1024,128]{1,0:T(8,128)(2,1)} %slice.17), channel_id=1, source_target_pairs={{0,3},{1,0},{2,1},{3,2},{4,7},{5,4},{6,5},{7,6},{8,11},{9,8},{10,9... | collective-permute-start | bytes 786440 | tf_op jit(solution)/shard_map/ppermute | solution.py:347
  62.5 2.5 %collective-permute-done.8.refs_3_ = bf16[2048,128]{1,0:T(8,128)(2,1)S(1)} collective-permute-done((bf16[2048,128]{1,0:T(8,128)(2,1)S(1)}, bf16[2048,128]{1,0:T(8,128)(2,1)S(1)}, u32[]{:S(2)}, u32[]{:S(2)}) %collective-permute-start.8) | collective-permute-done | bytes 524320 | tf_op jit(solution)/shard_map/ppermute | solution.py:347
  65.8 3.4 %collective-permute-start.3 = (bf16[1024,128]{1,0:T(8,128)(2,1)}, bf16[1024,128]{1,0:T(8,128)(2,1)}, u32[]{:S(2)}, u32[]{:S(2)}) collective-permute-start(bf16[1024,128]{1,0:T(8,128)(2,1)} %slice.16), channel_id=1, source_target_pairs={{0,1},{1,2},{2,3},{3,0},{4,5},{5,6},{6,7},{7,4},{8,9},{9,10},{10,1... | collective-permute-start | bytes 786440 | tf_op jit(solution)/shard_map/ppermute | solution.py:347
  69.2 1.4 shard_map.143
  70.6 5.5 %shard_map.144 = (bf16[128,384]{1,0:T(8,128)(2,1)}, bf16[128,384]{1,0:T(8,128)(2,1)}, bf16[128,384]{1,0:T(8,128)(2,1)}, f32[128,2048]{1,0:T(8,128)S(1)}, f32[128,128]{1,0:T(8,128)S(1)}) custom-call(s32[2]{0:T(128)S(1)} %pad_add_fusion.sc, bf16[128,4096]{1,0:T(8,128)(2,1)S(1)} %get-tuple-element.33.pair, bf16[128,128]{1,0:T(8,128)(2,1)} %get-tuple-element.34.info, ...), custom_call_target="tpu_custom_call" | custom-call | tf_op jit(solution)/shard_map/pallas_call | solution.py:79
  76.1 4.7 %collective-permute-done.5.up_b = bf16[1024,128]{1,0:T(8,128)(2,1)} collective-permute-done((bf16[1024,128]{1,0:T(8,128)(2,1)}, bf16[1024,128]{1,0:T(8,128)(2,1)}, u32[]{:S(2)}, u32[]{:S(2)}) %collective-permute-start.5) | collective-permute-done | bytes 262176 | tf_op jit(solution)/shard_map/ppermute | solution.py:347
  80.8 4.4 %shard_map.145 = (bf16[128,384]{1,0:T(8,128)(2,1)}, bf16[1024,640]{1,0:T(8,128)(2,1)}) custom-call(s32[2]{0:T(128)S(1)} %pad_add_fusion.sc, bf16[128,4096]{1,0:T(8,128)(2,1)S(1)} %get-tuple-element.33.pair, bf16[128,128]{1,0:T(8,128)(2,1)} %get-tuple-element.34.info, bf16[2048,128]{1,0:T(8,128)(2,1)} %collective-permute-done.1.gate, ...), custom_call_target="tpu_custom_call" | custom-call | tf_op jit(solution)/shard_map/pallas_call | solution.py:79
  85.3 13.7 %all-to-all-start.1 = ((bf16[128,8,640]{2,1,0:T(8,128)(2,1)}), bf16[128,8,640]{2,1,0:T(8,128)(2,1)S(1)}, u32[]{:S(2)}, u32[]{:S(2)}) async-start(bf16[128,8,640]{2,1,0:T(8,128)(2,1)} %bitcast.20), calls=%async_computation.1 | async-start | bytes 2621440 | tf_op jit(solution)/shard_map/all_to_all | solution.py:404
  99.0 5.0 %collective-permute-start.12 = (bf16[128,4096]{1,0:T(8,128)(2,1)S(1)}, bf16[128,4096]{1,0:T(8,128)(2,1)S(1)}, u32[]{:S(2)}, u32[]{:S(2)}) collective-permute-start(bf16[128,4096]{1,0:T(8,128)(2,1)S(1)} %get-tuple-element.33.pair), channel_id=1, source_target_pairs={{0,3},{1,0},{2,1},{3,2},{4,7},{5,4},{6,5},{7,6},{8,11},{9,8},{10,9... | collective-permute-start | bytes 3145736 | tf_op jit(solution)/shard_map/ppermute | solution.py:347
  104.0 1.9 %collective-permute-start.10 = (bf16[128,4096]{1,0:T(8,128)(2,1)S(1)}, bf16[128,4096]{1,0:T(8,128)(2,1)S(1)}, u32[]{:S(2)}, u32[]{:S(2)}) collective-permute-start(bf16[128,4096]{1,0:T(8,128)(2,1)S(1)} %get-tuple-element.33.pair), channel_id=1, source_target_pairs={{0,1},{1,2},{2,3},{3,0},{4,5},{5,6},{6,7},{7,4},{8,9},{9,10},{10,1... | collective-permute-start | bytes 3145736 | tf_op jit(solution)/shard_map/ppermute | solution.py:347
  106.0 20.7 %collective-permute-done.12.pair_3 = bf16[128,4096]{1,0:T(8,128)(2,1)S(1)} collective-permute-done((bf16[128,4096]{1,0:T(8,128)(2,1)S(1)}, bf16[128,4096]{1,0:T(8,128)(2,1)S(1)}, u32[]{:S(2)}, u32[]{:S(2)}) %collective-permute-start.12) | collective-permute-done | bytes 1048608 | tf_op jit(solution)/shard_map/ppermute | solution.py:347
  126.7 5.6 %collective-permute-start.13 = (bf16[64,4096]{1,0:T(8,128)(2,1)S(1)}, bf16[64,4096]{1,0:T(8,128)(2,1)S(1)}, u32[]{:S(2)}, u32[]{:S(2)}) collective-permute-start(bf16[64,4096]{1,0:T(8,128)(2,1)S(1)} %slice.19), channel_id=1, source_target_pairs={{0,3},{1,0},{2,1},{3,2},{4,7},{5,4},{6,5},{7,6},{8,11},{9,8},{10,9... | collective-permute-start | bytes 1572872 | tf_op jit(solution)/shard_map/ppermute | solution.py:347
  132.4 1.9 %collective-permute-start.11 = (bf16[64,4096]{1,0:T(8,128)(2,1)S(1)}, bf16[64,4096]{1,0:T(8,128)(2,1)S(1)}, u32[]{:S(2)}, u32[]{:S(2)}) collective-permute-start(bf16[64,4096]{1,0:T(8,128)(2,1)S(1)} %slice.18), channel_id=1, source_target_pairs={{0,1},{1,2},{2,3},{3,0},{4,5},{5,6},{6,7},{7,4},{8,9},{9,10},{10,1... | collective-permute-start | bytes 1572872 | tf_op jit(solution)/shard_map/ppermute | solution.py:347
  134.4 3.4 %collective-permute-start.15 = (bf16[128,384]{1,0:T(8,128)(2,1)S(1)}, bf16[128,384]{1,0:T(8,128)(2,1)S(1)}, u32[]{:S(2)}, u32[]{:S(2)}) collective-permute-start(bf16[128,384]{1,0:T(8,128)(2,1)S(1)} %copy-done.20), channel_id=1, source_target_pairs={{0,2},{1,3},{2,0},{3,1},{4,6},{5,7},{6,4},{7,5},{8,10},{9,11},{10,... | collective-permute-start | bytes 294920 | tf_op jit(solution)/shard_map/ppermute | solution.py:347
  137.7 4.5 %collective-permute-start.14 = (bf16[128,384]{1,0:T(8,128)(2,1)S(1)}, bf16[128,384]{1,0:T(8,128)(2,1)S(1)}, u32[]{:S(2)}, u32[]{:S(2)}) collective-permute-start(bf16[128,384]{1,0:T(8,128)(2,1)S(1)} %copy-done.19), channel_id=1, source_target_pairs={{0,1},{1,2},{2,3},{3,0},{4,5},{5,6},{6,7},{7,4},{8,9},{9,10},{10,1... | collective-permute-start | bytes 294920 | tf_op jit(solution)/shard_map/ppermute | solution.py:347
  142.3 2.5 %collective-permute-start.16 = (bf16[128,384]{1,0:T(8,128)(2,1)S(1)}, bf16[128,384]{1,0:T(8,128)(2,1)S(1)}, u32[]{:S(2)}, u32[]{:S(2)}) collective-permute-start(bf16[128,384]{1,0:T(8,128)(2,1)S(1)} %copy-done.18), channel_id=1, source_target_pairs={{0,3},{1,0},{2,1},{3,2},{4,7},{5,4},{6,5},{7,6},{8,11},{9,8},{10,9... | collective-permute-start | bytes 294920 | tf_op jit(solution)/shard_map/ppermute | solution.py:347
  144.8 5.3 %collective-permute-done.15.refs_2_ = bf16[128,384]{1,0:T(8,128)(2,1)S(1)} collective-permute-done((bf16[128,384]{1,0:T(8,128)(2,1)S(1)}, bf16[128,384]{1,0:T(8,128)(2,1)S(1)}, u32[]{:S(2)}, u32[]{:S(2)}) %collective-permute-start.15) | collective-permute-done | bytes 98336 | tf_op jit(solution)/shard_map/ppermute | solution.py:347
  150.1 2.4 %collective-permute-done.14.refs_1_ = bf16[128,384]{1,0:T(8,128)(2,1)S(1)} collective-permute-done((bf16[128,384]{1,0:T(8,128)(2,1)S(1)}, bf16[128,384]{1,0:T(8,128)(2,1)S(1)}, u32[]{:S(2)}, u32[]{:S(2)}) %collective-permute-start.14) | collective-permute-done | bytes 98336 | tf_op jit(solution)/shard_map/ppermute | solution.py:347
  153.6 5.1 %shard_map.146 = (bf16[2048,128]{1,0:T(8,128)(2,1)}, bf16[2048,128]{1,0:T(8,128)(2,1)}, bf16[128,2048]{1,0:T(8,128)(2,1)}, f32[1,128]{1,0:T(1,128)}, bf16[16,512]{1,0:T(8,128)(2,1)S(1)}) custom-call(s32[2]{0:T(128)S(1)} %pad_add_fusion.sc, bf16[128,4096]{1,0:T(8,128)(2,1)} %copy-done, bf16[128,4096]{1,0:T(8,128)(2,1)} %copy-done.7, ...), custom_call_target="tpu_custom_call" | custom-call | tf_op jit(solution)/shard_map/pallas_call | solution.py:79
  159.8 11.9 %all_to_all.15.got = bf16[4,160,512]{2,1,0:T(8,128)(2,1)S(1)} all-to-all(bf16[4,160,512]{2,1,0:T(8,128)(2,1)S(1)} %shard_map.147), channel_id=1, replica_groups=mesh['ep_0'=8,'ep_1'=8,'ep_2'=2,'tp'=4] {'tp'}, dimensions={0} | all-to-all | bytes 1310720 | tf_op jit(solution)/shard_map/all_to_all | solution.py:430
  171.6 1.4 shard_map.148
  (61 shorter events, 4.9 us)
Async XLA Ops:
  4.9 17.5 %copy-start.10 = (bf16[1,2048,128]{2,1,0:T(8,128)(2,1)S(1)}, bf16[1,2048,128]{2,1,0:T(8,128)(2,1)}, u32[]{:S(2)}) copy-start(bf16[1,2048,128]{2,1,0:T(8,128)(2,1)} %param.11) | copy-start | bytes 1572868
  4.9 20.9 %copy-start.11 = (bf16[1,2048,128]{2,1,0:T(8,128)(2,1)S(1)}, bf16[1,2048,128]{2,1,0:T(8,128)(2,1)}, u32[]{:S(2)}) copy-start(bf16[1,2048,128]{2,1,0:T(8,128)(2,1)} %param.12) | copy-start | bytes 1572868
  4.9 64.3 %all-to-all-start = ((bf16[128,8,640]{2,1,0:T(8,128)(2,1)}), bf16[128,8,640]{2,1,0:T(8,128)(2,1)S(1)}, u32[]{:S(2)}, u32[]{:S(2)}) async-start(bf16[128,8,640]{2,1,0:T(8,128)(2,1)} %bitcast.21), calls=%async_computation | async-start | bytes 2621440 | tf_op jit(solution)/shard_map/all_to_all | solution.py:372
  22.4 18.0 %collective-permute-start = (bf16[2048,128]{1,0:T(8,128)(2,1)S(1)}, bf16[2048,128]{1,0:T(8,128)(2,1)}, u32[]{:S(2)}, u32[]{:S(2)}) collective-permute-start(bf16[2048,128]{1,0:T(8,128)(2,1)S(1)} %bitcast.23), channel_id=1, source_target_pairs={{0,1},{1,2},{2,3},{3,0},{4,5},{5,6},{6,7},{7,4},{8,9},{9,10},{10,1... | collective-permute-start | bytes 1572872 | tf_op jit(solution)/shard_map/ppermute | solution.py:347
  25.8 16.8 %collective-permute-start.4 = (bf16[2048,128]{1,0:T(8,128)(2,1)S(1)}, bf16[2048,128]{1,0:T(8,128)(2,1)S(1)}, u32[]{:S(2)}, u32[]{:S(2)}) collective-permute-start(bf16[2048,128]{1,0:T(8,128)(2,1)S(1)} %bitcast.26), channel_id=1, source_target_pairs={{0,3},{1,0},{2,1},{3,2},{4,7},{5,4},{6,5},{7,6},{8,11},{9,8},{10,9... | collective-permute-start | bytes 1572872 | tf_op jit(solution)/shard_map/ppermute | solution.py:347
  29.5 24.4 %collective-permute-start.6 = (bf16[128,2048]{1,0:T(8,128)(2,1)}, bf16[128,2048]{1,0:T(8,128)(2,1)}, u32[]{:S(2)}, u32[]{:S(2)}) collective-permute-start(bf16[128,2048]{1,0:T(8,128)(2,1)} %bitcast.7.refs_2_), channel_id=1, source_target_pairs={{0,3},{1,0},{2,1},{3,2},{4,7},{5,4},{6,5},{7,6},{8,11},{9,8},{10,9... | collective-permute-start | bytes 1572872 | tf_op jit(solution)/shard_map/ppermute | solution.py:347
  33.0 26.5 %collective-permute-start.2 = (bf16[2048,128]{1,0:T(8,128)(2,1)S(1)}, bf16[2048,128]{1,0:T(8,128)(2,1)S(1)}, u32[]{:S(2)}, u32[]{:S(2)}) collective-permute-start(bf16[2048,128]{1,0:T(8,128)(2,1)S(1)} %bitcast.27), channel_id=1, source_target_pairs={{0,1},{1,2},{2,3},{3,0},{4,5},{5,6},{6,7},{7,4},{8,9},{9,10},{10,1... | collective-permute-start | bytes 1572872 | tf_op jit(solution)/shard_map/ppermute | solution.py:347
  35.4 29.6 %collective-permute-start.8 = (bf16[2048,128]{1,0:T(8,128)(2,1)S(1)}, bf16[2048,128]{1,0:T(8,128)(2,1)S(1)}, u32[]{:S(2)}, u32[]{:S(2)}) collective-permute-start(bf16[2048,128]{1,0:T(8,128)(2,1)S(1)} %bitcast.24), channel_id=1, source_target_pairs={{0,3},{1,0},{2,1},{3,2},{4,7},{5,4},{6,5},{7,6},{8,11},{9,8},{10,9... | collective-permute-start | bytes 1572872 | tf_op jit(solution)/shard_map/ppermute | solution.py:347
  40.4 30.2 %collective-permute-start.9 = (bf16[128,2048]{1,0:T(8,128)(2,1)}, bf16[128,2048]{1,0:T(8,128)(2,1)}, u32[]{:S(2)}, u32[]{:S(2)}) collective-permute-start(bf16[128,2048]{1,0:T(8,128)(2,1)} %bitcast.7.refs_2_), channel_id=1, source_target_pairs={{0,1},{1,2},{2,3},{3,0},{4,5},{5,6},{6,7},{7,4},{8,9},{9,10},{10,1... | collective-permute-start | bytes 1572872 | tf_op jit(solution)/shard_map/ppermute | solution.py:347
  42.6 28.0 %copy-start.8 = (bf16[2048,128]{1,0:T(8,128)(2,1)}, bf16[2048,128]{1,0:T(8,128)(2,1)S(1)}, u32[]{:S(2)}) copy-start(bf16[2048,128]{1,0:T(8,128)(2,1)S(1)} %collective-permute-done.4.refs_4_) | copy-start | bytes 1572868
  42.6 38.2 %collective-permute-start.1 = (bf16[2048,128]{1,0:T(8,128)(2,1)}, bf16[2048,128]{1,0:T(8,128)(2,1)}, u32[]{:S(2)}, u32[]{:S(2)}) collective-permute-start(bf16[2048,128]{1,0:T(8,128)(2,1)} %collective-permute-done.refs_6_), channel_id=1, source_target_pairs={{0,1},{1,2},{2,3},{3,0},{4,5},{5,6},{6,7},{7,4},{8,9},{9,10},{10,1... | collective-permute-start | bytes 1572872 | tf_op jit(solution)/shard_map/ppermute | solution.py:347
  53.9 27.0 %collective-permute-start.7 = (bf16[128,2048]{1,0:T(8,128)(2,1)}, bf16[128,2048]{1,0:T(8,128)(2,1)}, u32[]{:S(2)}, u32[]{:S(2)}) collective-permute-start(bf16[128,2048]{1,0:T(8,128)(2,1)} %collective-permute-done.6.refs_5_), channel_id=1, source_target_pairs={{0,3},{1,0},{2,1},{3,2},{4,7},{5,4},{6,5},{7,6},{8,11},{9,8},{10,9... | collective-permute-start | bytes 1572872 | tf_op jit(solution)/shard_map/ppermute | solution.py:347
  59.5 11.1 %copy-start.9 = (bf16[2048,128]{1,0:T(8,128)(2,1)}, bf16[2048,128]{1,0:T(8,128)(2,1)S(1)}, u32[]{:S(2)}) copy-start(bf16[2048,128]{1,0:T(8,128)(2,1)S(1)} %collective-permute-done.2.refs_7_) | copy-start | bytes 1572868
  59.5 21.3 %collective-permute-start.5 = (bf16[1024,128]{1,0:T(8,128)(2,1)}, bf16[1024,128]{1,0:T(8,128)(2,1)}, u32[]{:S(2)}, u32[]{:S(2)}) collective-permute-start(bf16[1024,128]{1,0:T(8,128)(2,1)} %slice.17), channel_id=1, source_target_pairs={{0,3},{1,0},{2,1},{3,2},{4,7},{5,4},{6,5},{7,6},{8,11},{9,8},{10,9... | collective-permute-start | bytes 786440 | tf_op jit(solution)/shard_map/ppermute | solution.py:347
  65.8 15.0 %collective-permute-start.3 = (bf16[1024,128]{1,0:T(8,128)(2,1)}, bf16[1024,128]{1,0:T(8,128)(2,1)}, u32[]{:S(2)}, u32[]{:S(2)}) collective-permute-start(bf16[1024,128]{1,0:T(8,128)(2,1)} %slice.16), channel_id=1, source_target_pairs={{0,1},{1,2},{2,3},{3,0},{4,5},{5,6},{6,7},{7,4},{8,9},{9,10},{10,1... | collective-permute-start | bytes 786440 | tf_op jit(solution)/shard_map/ppermute | solution.py:347
  70.6 33.4 %copy-start = (bf16[128,4096]{1,0:T(8,128)(2,1)}, bf16[128,4096]{1,0:T(8,128)(2,1)S(1)}, u32[]{:S(2)}) copy-start(bf16[128,4096]{1,0:T(8,128)(2,1)S(1)} %get-tuple-element.33.pair) | copy-start | bytes 3145732
  85.3 73.4 %all-to-all-start.1 = ((bf16[128,8,640]{2,1,0:T(8,128)(2,1)}), bf16[128,8,640]{2,1,0:T(8,128)(2,1)S(1)}, u32[]{:S(2)}, u32[]{:S(2)}) async-start(bf16[128,8,640]{2,1,0:T(8,128)(2,1)} %bitcast.20), calls=%async_computation.1 | async-start | bytes 2621440 | tf_op jit(solution)/shard_map/all_to_all | solution.py:404
  99.0 35.4 %copy-start.20 = (bf16[128,384]{1,0:T(8,128)(2,1)S(1)}, bf16[128,384]{1,0:T(8,128)(2,1)}, u32[]{:S(2)}) copy-start(bf16[128,384]{1,0:T(8,128)(2,1)} %get-tuple-element.42) | copy-start | bytes 294916
  99.0 38.7 %copy-start.19 = (bf16[128,384]{1,0:T(8,128)(2,1)S(1)}, bf16[128,384]{1,0:T(8,128)(2,1)}, u32[]{:S(2)}) copy-start(bf16[128,384]{1,0:T(8,128)(2,1)} %get-tuple-element.41) | copy-start | bytes 294916
  99.0 43.3 %copy-start.18 = (bf16[128,384]{1,0:T(8,128)(2,1)S(1)}, bf16[128,384]{1,0:T(8,128)(2,1)}, u32[]{:S(2)}) copy-start(bf16[128,384]{1,0:T(8,128)(2,1)} %get-tuple-element.43) | copy-start | bytes 294916
  99.0 27.7 %collective-permute-start.12 = (bf16[128,4096]{1,0:T(8,128)(2,1)S(1)}, bf16[128,4096]{1,0:T(8,128)(2,1)S(1)}, u32[]{:S(2)}, u32[]{:S(2)}) collective-permute-start(bf16[128,4096]{1,0:T(8,128)(2,1)S(1)} %get-tuple-element.33.pair), channel_id=1, source_target_pairs={{0,3},{1,0},{2,1},{3,2},{4,7},{5,4},{6,5},{7,6},{8,11},{9,8},{10,9... | collective-permute-start | bytes 3145736 | tf_op jit(solution)/shard_map/ppermute | solution.py:347
  104.0 28.3 %collective-permute-start.10 = (bf16[128,4096]{1,0:T(8,128)(2,1)S(1)}, bf16[128,4096]{1,0:T(8,128)(2,1)S(1)}, u32[]{:S(2)}, u32[]{:S(2)}) collective-permute-start(bf16[128,4096]{1,0:T(8,128)(2,1)S(1)} %get-tuple-element.33.pair), channel_id=1, source_target_pairs={{0,1},{1,2},{2,3},{3,0},{4,5},{5,6},{6,7},{7,4},{8,9},{9,10},{10,1... | collective-permute-start | bytes 3145736 | tf_op jit(solution)/shard_map/ppermute | solution.py:347
  126.7 25.9 %copy-start.6 = (bf16[128,4096]{1,0:T(8,128)(2,1)}, bf16[128,4096]{1,0:T(8,128)(2,1)S(1)}, u32[]{:S(2)}) copy-start(bf16[128,4096]{1,0:T(8,128)(2,1)S(1)} %collective-permute-done.12.pair_3) | copy-start | bytes 3145732
  126.7 25.8 %collective-permute-start.13 = (bf16[64,4096]{1,0:T(8,128)(2,1)S(1)}, bf16[64,4096]{1,0:T(8,128)(2,1)S(1)}, u32[]{:S(2)}, u32[]{:S(2)}) collective-permute-start(bf16[64,4096]{1,0:T(8,128)(2,1)S(1)} %slice.19), channel_id=1, source_target_pairs={{0,3},{1,0},{2,1},{3,2},{4,7},{5,4},{6,5},{7,6},{8,11},{9,8},{10,9... | collective-permute-start | bytes 1572872 | tf_op jit(solution)/shard_map/ppermute | solution.py:347
  132.4 20.2 %copy-start.7 = (bf16[128,4096]{1,0:T(8,128)(2,1)}, bf16[128,4096]{1,0:T(8,128)(2,1)S(1)}, u32[]{:S(2)}) copy-start(bf16[128,4096]{1,0:T(8,128)(2,1)S(1)} %collective-permute-done.10.pair_1) | copy-start | bytes 3145732
  132.4 20.2 %collective-permute-start.11 = (bf16[64,4096]{1,0:T(8,128)(2,1)S(1)}, bf16[64,4096]{1,0:T(8,128)(2,1)S(1)}, u32[]{:S(2)}, u32[]{:S(2)}) collective-permute-start(bf16[64,4096]{1,0:T(8,128)(2,1)S(1)} %slice.18), channel_id=1, source_target_pairs={{0,1},{1,2},{2,3},{3,0},{4,5},{5,6},{6,7},{7,4},{8,9},{9,10},{10,1... | collective-permute-start | bytes 1572872 | tf_op jit(solution)/shard_map/ppermute | solution.py:347
  134.4 15.8 %collective-permute-start.15 = (bf16[128,384]{1,0:T(8,128)(2,1)S(1)}, bf16[128,384]{1,0:T(8,128)(2,1)S(1)}, u32[]{:S(2)}, u32[]{:S(2)}) collective-permute-start(bf16[128,384]{1,0:T(8,128)(2,1)S(1)} %copy-done.20), channel_id=1, source_target_pairs={{0,2},{1,3},{2,0},{3,1},{4,6},{5,7},{6,4},{7,5},{8,10},{9,11},{10,... | collective-permute-start | bytes 294920 | tf_op jit(solution)/shard_map/ppermute | solution.py:347
  137.7 14.8 %collective-permute-start.14 = (bf16[128,384]{1,0:T(8,128)(2,1)S(1)}, bf16[128,384]{1,0:T(8,128)(2,1)S(1)}, u32[]{:S(2)}, u32[]{:S(2)}) collective-permute-start(bf16[128,384]{1,0:T(8,128)(2,1)S(1)} %copy-done.19), channel_id=1, source_target_pairs={{0,1},{1,2},{2,3},{3,0},{4,5},{5,6},{6,7},{7,4},{8,9},{9,10},{10,1... | collective-permute-start | bytes 294920 | tf_op jit(solution)/shard_map/ppermute | solution.py:347
  142.3 10.3 %collective-permute-start.16 = (bf16[128,384]{1,0:T(8,128)(2,1)S(1)}, bf16[128,384]{1,0:T(8,128)(2,1)S(1)}, u32[]{:S(2)}, u32[]{:S(2)}) collective-permute-start(bf16[128,384]{1,0:T(8,128)(2,1)S(1)} %copy-done.18), channel_id=1, source_target_pairs={{0,3},{1,0},{2,1},{3,2},{4,7},{5,4},{6,5},{7,6},{8,11},{9,8},{10,9... | collective-permute-start | bytes 294920 | tf_op jit(solution)/shard_map/ppermute | solution.py:347
  158.7 12.9 %copy-start.1 = (bf16[2048,128]{1,0:T(8,128)(2,1)S(1)}, bf16[2048,128]{1,0:T(8,128)(2,1)}, u32[]{:S(2)}) copy-start(bf16[2048,128]{1,0:T(8,128)(2,1)} %router.3) | copy-start | bytes 1572868
  158.7 12.9 %copy-start.4 = (f32[8,128]{1,0:T(8,128)S(1)}, f32[8,128]{1,0:T(8,128)}, u32[]{:S(2)}) copy-start(f32[8,128]{1,0:T(8,128)} %get-tuple-element.45.stats) | copy-start | bytes 12292
  158.7 12.9 %copy-start.5 = (s32[128,2]{0,1:T(2,128)S(1)}, s32[128,2]{0,1:T(2,128)}, u32[]{:S(2)}) copy-start(s32[128,2]{0,1:T(2,128)} %param.9) | copy-start | bytes 3076
  (8 other events, 16.6 us)

commit v5 on v4

--- a/solution.py
+++ b/solution.py
@@ -151,19 +151,20 @@
     )
 
 
-def rows_kernel(sc, got, pair, info, scratch):
+def rows_kernel(sc, got, pair, scratch):
     fill(scratch, got)
     for u in range(8):
         part = gather(scratch, u)
         pair[:, CH * u : CH * (u + 1)] = part[:, 0:CH]
         pair[:, D + CH * u : D + CH * (u + 1)] = part[:, CH : 2 * CH]
         if u == 0:
-            info[...] = part[:, 2 * CH :]
-
-
-def quarter(pair, about, both, down, grads):
+            pair[:, 2 * D :] = part[:, 2 * CH :]
+
+
+def hidden_grads(pair, both, down):
     pre = dot(pair[:, 0:D], both)
-    back_raw = dot(pair[:, D:], down, 1, 1)
+    back_raw = dot(pair[:, D : 2 * D], down, 1, 1)
+    about = pair[:, 2 * D :].astype(F32)
     pre_gate = pre[:, 0:FQ]
     pre_up = pre[:, FQ:]
     gating = about[:, 0:1] + about[:, 1:2] + about[:, 2:3]
@@ -174,14 +175,12 @@
     gg = jnp.sum(hidden * back_raw, axis=1, keepdims=True)
     scaled = gating * back_raw
     g_in = jnp.concatenate([scaled * pre_up * slope, scaled * activated], axis=1).astype(BF16)
-    grads[:, 0 : 2 * FQ] = g_in
-    grads[:, 2 * FQ :] = (gating * hidden).astype(BF16)
-    return gg, dot(g_in, both, 1, 1)
-
-
-def three_kernel(sc, pair, info, *refs):
-    weights, outs = refs[0:9], refs[9:12]
-    back, gg_out, held, held_down, sems = refs[12:]
+    return g_in, (gating * hidden).astype(BF16), gg
+
+
+def three_kernel(sc, pair, *refs):
+    weights = refs[0:9]
+    grads, back, gg_out, held, held_down, sems = refs[9:]
     copies = []
     for k in range(3):
         gate, up, down = weights[3 * k : 3 * k + 3]
@@ -194,13 +193,15 @@
         )
         for c in copies[k]:
             c.start()
-    about = info[...].astype(F32)
     gg = None
-    for k, grads in enumerate(outs):
+    for k in range(3):
         for c in copies[k]:
             c.wait()
-        part, term = quarter(pair, about, held[k], held_down[k], grads)
-        if gg is None:
+        g_in, scaled, part = hidden_grads(pair, held[k], held_down[k])
+        term = dot(g_in, held[k], 1, 1)
+        if k == 0:
+            grads[:, 0 : 2 * FQ] = g_in
+            grads[:, 2 * FQ :] = scaled
             gg = part
             back[...] = term
         else:
@@ -209,13 +210,21 @@
     gg_out[...] = jnp.broadcast_to(gg, (128, 128))
 
 
-def emit_kernel(sc, pair, info, gate, up_a, up_b, down, back, gg_in, grads, send, scratch):
-    about = info[...].astype(F32)
+def redo_kernel(sc, pair_1, pair_3, gate, up, down, out_1, out_3):
+    both = jnp.concatenate([gate[...], up[...]], axis=1)
+    for pair, out in ((pair_1, out_1), (pair_3, out_3)):
+        g_in, scaled, _ = hidden_grads(pair, both, down[...])
+        out[:, 0 : 2 * FQ] = g_in
+        out[:, 2 * FQ :] = scaled
+
+
+def emit_kernel(sc, pair, gate, up_a, up_b, down, back, gg_in, send, scratch):
+    about = pair[:, 2 * D :].astype(F32)
     up = jnp.concatenate([up_a[...], up_b[...]], axis=0)
     both = jnp.concatenate([gate[...], up], axis=1)
-    gg, term = quarter(pair, about, both, down[...], grads)
+    g_in, _, gg = hidden_grads(pair, both, down[...])
+    term = back[...] + dot(g_in, both, 1, 1)
     gg = gg + gg_in[:, 0:1]
-    term = back[...] + term
     own = (about[:, 3:4] + about[:, 4:5] + about[:, 5:6]) * gg
     other = (about[:, 6:7] + about[:, 7:8] + about[:, 8:9]) * gg
     other_expert = about[:, 9:10].astype(jnp.int32)
@@ -245,14 +254,20 @@
     )
 
 
-def sums_kernel(sc, pair, pair_1, top, bottom, pair_3, *refs):
-    grads = refs[0:4]
-    gate, up, down, down_norms, norms = refs[4:]
-    pairs = (pair, pair_1, top, bottom, pair_3)
+def sums_kernel(
+    sc, pair, pair_1, top, bottom, pair_3, grads_0, grads_1, grads_3, gate_w, up_w, down_w, *outs
+):
+    gate, up, down, down_norms, norms = outs
+    distant = jnp.concatenate([top[...], bottom[...]], axis=0)
+    both = jnp.concatenate([gate_w[...], up_w[...]], axis=1)
+    far_in, far_scaled, _ = hidden_grads(distant, both, down_w[...])
+    pairs = (pair, pair_1, distant, pair_3)
     toks = jnp.concatenate([x[:, 0:D] for x in pairs], axis=0)
-    cots = jnp.concatenate([x[:, D:] for x in pairs], axis=0)
-    g_in = jnp.concatenate([g[:, 0 : 2 * FQ] for g in grads], axis=0)
-    scaled = jnp.concatenate([g[:, 2 * FQ :] for g in grads], axis=0)
+    cots = jnp.concatenate([x[:, D : 2 * D] for x in pairs], axis=0)
+    at = slice(0, 2 * FQ)
+    g_in = jnp.concatenate([grads_0[:, at], grads_1[:, at], far_in, grads_3[:, at]], axis=0)
+    at = slice(2 * FQ, 3 * FQ)
+    scaled = jnp.concatenate([grads_0[:, at], grads_1[:, at], far_scaled, grads_3[:, at]], axis=0)
     in_sums = dot(toks, g_in, 0, 0)
     gate[...] = in_sums[:, 0:FQ].astype(BF16)
     up[...] = in_sums[:, FQ:].astype(BF16)
@@ -370,48 +385,54 @@
         (pltpu.VMEM((2 * CH // 128, SENT, 128), F32),),
     )
     got = lax.all_to_all(send.reshape(EXPERTS, 8, 2 * CH + 128), EP, 0, 0, tiled=True)
-    pair, info = call(
+    (pair,) = call(
         rows_kernel,
         sc,
         (got.reshape(SENT, 2 * CH + 128),),
-        (vmem((128, 2 * D), BF16), hbm((128, 128), BF16)),
+        (vmem((128, 2 * D + 128), BF16),),
         (pltpu.VMEM((2 * CH // 128 + 1, SENT, 128), F32),),
     )
     pair_1 = shift(pair, 1)
     pair_3 = shift(pair, 3)
     quarter_grads = hbm((128, 3 * FQ), BF16)
-    grads = [None] * TP
     in_place = pl.BlockSpec(memory_space=pltpu.HBM)
     weights = (gate_w, up_w, down_w, gate_3, up_3, down_3, gate_1, up_1, down_1)
-    grads[0], grads[1], grads[3], back, gg = call(
+    grads_0, back, gg = call(
         three_kernel,
         sc,
-        (pair, whole(far(info)), *((far(x), in_place) for x in weights)),
-        (quarter_grads,) * 3 + (vmem((128, D), F32), vmem((128, 128), F32)),
+        (pair, *((far(x), in_place) for x in weights)),
+        (quarter_grads, vmem((128, D), F32), vmem((128, 128), F32)),
         (
             pltpu.VMEM((3, D, 2 * FQ), BF16),
             pltpu.VMEM((3, FQ, D), BF16),
             pltpu.SemaphoreType.DMA((9,)),
         ),
     )
-    grads[2], send_back = call(
+    (send_back,) = call(
         emit_kernel,
         sc,
-        (pair, *(whole(far(x)) for x in (info, gate_2, up_2a, up_2b, down_2)), back, gg),
-        (quarter_grads, hbm((SENT, 2 * CH + 128), BF16)),
+        (pair, *(whole(far(x)) for x in (gate_2, up_2a, up_2b, down_2)), back, gg),
+        (hbm((SENT, 2 * CH + 128), BF16),),
         (pltpu.VMEM((CH // 128, SENT, 128), F32),),
     )
     home = lax.all_to_all(send_back.reshape(EXPERTS, 8, 2 * CH + 128), EP, 0, 0, tiled=True)
     home = home.reshape(SENT, 2 * CH + 128)
-    grads[2] = shift(grads[2], 2)
     top = shift(pair_1[0:64], 1)
     bottom = shift(pair_3[64:], 3)
-    grads[1] = shift(grads[1], 1)
-    grads[3] = shift(grads[3], 3)
+    own_weights = tuple(whole(far(x)) for x in (gate_w, up_w, down_w))
+    grads_1, grads_3 = call(
+        redo_kernel,
+        sc,
+        (*(whole(far(x)) for x in (pair_1, pair_3)), *own_weights),
+        (quarter_grads,) * 2,
+    )
     grad_gate, grad_up, grad_down, down_norms, norms = call(
         sums_kernel,
         sc,
-        tuple(whole(far(x)) for x in (pair, pair_1, top, bottom, pair_3, *grads)),
+        (
+            *(whole(far(x)) for x in (pair, pair_1, top, bottom, pair_3, grads_0, grads_1, grads_3)),
+            *own_weights,
+        ),
         (
             sds((D, FQ), BF16),
             sds((D, FQ), BF16),

time: 174 us -> 171 us (0.983)
  starting transfers between devices: 89.7 us -> 79.4 us
  waiting for transfers between devices: 43.9 us -> 48.5 us
  Pallas kernels: 23 us -> 26.1 us
    ppermute x17 -> x14, starting transfers between devices: 58.5 us -> 48.1 us  [shift(): return lax.ppermute(x, 'tp', [(a, (a + d) % TP) for a in range(TP)])]
    ppermute x17 -> x14, waiting for transfers between devices: 43.9 us -> 48.5 us  [shift(): return lax.ppermute(x, 'tp', [(a, (a + d) % TP) for a in range(TP)])]
    pallas_call x7 -> x8, Pallas kernels: 23 us -> 26.1 us  [call(): pl.pallas_call(kernel, grid_spec=pltpu.PrefetchScalarGridSpec(num_scalar_...]
  transfers between devices with their start and end apart: 19 -> 16, of which waited for: 7 -> 7; matrix products, arithmetic and copies ran while one was open for 1% -> 1% of each run, Pallas kernels for 7% -> 9%
where the time goes in v5:
time: 171 us; the launch traced here: 170 us
  starting transfers between devices  79.4 us (46%)
  waiting for transfers between devices  48.5 us (28%)
  Pallas kernels  26.1 us (15%)
  blocking collectives  11.9 us (7%)
  local copies, waits for them, and re-layouts  3.17 us (2%)
    ppermute x14, waiting for transfers between devices, shift(): return lax.ppermute(x, 'tp', [(a, (a + d) % TP) for a in range(TP)])  48.5 us
    ppermute x14, starting transfers between devices, shift(): return lax.ppermute(x, 'tp', [(a, (a + d) % TP) for a in range(TP)])  48.1 us
    pallas_call x8, Pallas kernels, call(): pl.pallas_call(kernel, grid_spec=pltpu.PrefetchScalarGridSpec(num_scalar_...  26.1 us
    all_to_all x1, starting transfers between devices, layer(): lax.all_to_all(send.reshape(EXPERTS, 8, 2 * CH + 128), EP, 0, 0, tiled=True)  17.5 us
    all_to_all x1, starting transfers between devices, layer(): lax.all_to_all(send_back.reshape(EXPERTS, 8, 2 * CH + 128), EP, 0, 0, til...  13.7 us
    all_to_all x1, blocking collectives, layer(): parts = lax.all_to_all(parts, 'tp', 0, 0, tiled=True)  11.9 us
  transfers between devices with their start and end apart: 16, of which 7 were waited for; matrix products, arithmetic and copies ran while one was open for 1% of the time, Pallas kernels for 9%

profile of v5, /device:TPU:8, one launch (start us, length us, event | category | flops | bytes accessed | tf_op | source)
XLA Modules:
  0.0 170.1 jit_solution(13155109644957014885)
XLA Ops:
  0.7 4.1 %shard_map.142 = (bf16[1024,640]{1,0:T(8,128)(2,1)}, bf16[128,128]{1,0:T(8,128)(2,1)}, bf16[128,128]{1,0:T(8,128)(2,1)}, f32[8,128]{1,0:T(8,128)}) custom-call(s32[2]{0:T(128)S(1)} %pad_add_fusion.sc, bf16[128,2048]{1,0:T(8,128)(2,1)} %tok.1, bf16[128,2048]{1,0:T(8,128)(2,1)} %cot.1, s32[2,128]{1,0:T(2,128)} %bitcast.18, bf16[2048,128]{1,0:T(8,128)(2,1)} %router.3), custom_call_target="tpu_custom_call" | custom-call | tf_op jit(solution)/shard_map/pallas_call | solution.py:79
  4.9 17.5 %all-to-all-start = ((bf16[128,8,640]{2,1,0:T(8,128)(2,1)}), bf16[128,8,640]{2,1,0:T(8,128)(2,1)S(1)}, u32[]{:S(2)}, u32[]{:S(2)}) async-start(bf16[128,8,640]{2,1,0:T(8,128)(2,1)} %bitcast.31), calls=%async_computation | async-start | bytes 2621440 | tf_op jit(solution)/shard_map/all_to_all | solution.py:387
  22.4 3.4 %collective-permute-start = (bf16[2048,128]{1,0:T(8,128)(2,1)S(1)}, bf16[2048,128]{1,0:T(8,128)(2,1)}, u32[]{:S(2)}, u32[]{:S(2)}) collective-permute-start(bf16[2048,128]{1,0:T(8,128)(2,1)S(1)} %bitcast.24), channel_id=1, source_target_pairs={{0,1},{1,2},{2,3},{3,0},{4,5},{5,6},{6,7},{7,4},{8,9},{9,10},{10,1... | collective-permute-start | bytes 1572872 | tf_op jit(solution)/shard_map/ppermute | solution.py:362
  25.8 3.7 %collective-permute-start.4 = (bf16[2048,128]{1,0:T(8,128)(2,1)S(1)}, bf16[2048,128]{1,0:T(8,128)(2,1)S(1)}, u32[]{:S(2)}, u32[]{:S(2)}) collective-permute-start(bf16[2048,128]{1,0:T(8,128)(2,1)S(1)} %bitcast.29), channel_id=1, source_target_pairs={{0,3},{1,0},{2,1},{3,2},{4,7},{5,4},{6,5},{7,6},{8,11},{9,8},{10,9... | collective-permute-start | bytes 1572872 | tf_op jit(solution)/shard_map/ppermute | solution.py:362
  29.5 3.5 %collective-permute-start.6 = (bf16[128,2048]{1,0:T(8,128)(2,1)}, bf16[128,2048]{1,0:T(8,128)(2,1)}, u32[]{:S(2)}, u32[]{:S(2)}) collective-permute-start(bf16[128,2048]{1,0:T(8,128)(2,1)} %bitcast.7.refs_2_.down.down_w), channel_id=1, source_target_pairs={{0,3},{1,0},{2,1},{3,2},{4,7},{5,4},{6,5},{7,6},{8,11},{9,8},{10,9... | collective-permute-start | bytes 1572872 | tf_op jit(solution)/shard_map/ppermute | solution.py:362
  32.9 2.4 %collective-permute-start.2 = (bf16[2048,128]{1,0:T(8,128)(2,1)S(1)}, bf16[2048,128]{1,0:T(8,128)(2,1)S(1)}, u32[]{:S(2)}, u32[]{:S(2)}) collective-permute-start(bf16[2048,128]{1,0:T(8,128)(2,1)S(1)} %bitcast.30), channel_id=1, source_target_pairs={{0,1},{1,2},{2,3},{3,0},{4,5},{5,6},{6,7},{7,4},{8,9},{9,10},{10,1... | collective-permute-start | bytes 1572872 | tf_op jit(solution)/shard_map/ppermute | solution.py:362
  35.3 4.7 %collective-permute-start.8 = (bf16[2048,128]{1,0:T(8,128)(2,1)S(1)}, bf16[2048,128]{1,0:T(8,128)(2,1)S(1)}, u32[]{:S(2)}, u32[]{:S(2)}) collective-permute-start(bf16[2048,128]{1,0:T(8,128)(2,1)S(1)} %bitcast.25), channel_id=1, source_target_pairs={{0,3},{1,0},{2,1},{3,2},{4,7},{5,4},{6,5},{7,6},{8,11},{9,8},{10,9... | collective-permute-start | bytes 1572872 | tf_op jit(solution)/shard_map/ppermute | solution.py:362
  40.4 2.2 %collective-permute-start.9 = (bf16[128,2048]{1,0:T(8,128)(2,1)}, bf16[128,2048]{1,0:T(8,128)(2,1)}, u32[]{:S(2)}, u32[]{:S(2)}) collective-permute-start(bf16[128,2048]{1,0:T(8,128)(2,1)} %bitcast.7.refs_2_.down.down_w), channel_id=1, source_target_pairs={{0,1},{1,2},{2,3},{3,0},{4,5},{5,6},{6,7},{7,4},{8,9},{9,10},{10,1... | collective-permute-start | bytes 1572872 | tf_op jit(solution)/shard_map/ppermute | solution.py:362
  42.6 3.4 %collective-permute-start.1 = (bf16[2048,128]{1,0:T(8,128)(2,1)}, bf16[2048,128]{1,0:T(8,128)(2,1)}, u32[]{:S(2)}, u32[]{:S(2)}) collective-permute-start(bf16[2048,128]{1,0:T(8,128)(2,1)} %collective-permute-done.refs_6_), channel_id=1, source_target_pairs={{0,1},{1,2},{2,3},{3,0},{4,5},{5,6},{6,7},{7,4},{8,9},{9,10},{10,1... | collective-permute-start | bytes 1572872 | tf_op jit(solution)/shard_map/ppermute | solution.py:362
  46.0 7.8 %collective-permute-done.6.refs_5_ = bf16[128,2048]{1,0:T(8,128)(2,1)} collective-permute-done((bf16[128,2048]{1,0:T(8,128)(2,1)}, bf16[128,2048]{1,0:T(8,128)(2,1)}, u32[]{:S(2)}, u32[]{:S(2)}) %collective-permute-start.6) | collective-permute-done | bytes 524320 | tf_op jit(solution)/shard_map/ppermute | solution.py:362
  53.8 4.9 %collective-permute-start.7 = (bf16[128,2048]{1,0:T(8,128)(2,1)}, bf16[128,2048]{1,0:T(8,128)(2,1)}, u32[]{:S(2)}, u32[]{:S(2)}) collective-permute-start(bf16[128,2048]{1,0:T(8,128)(2,1)} %collective-permute-done.6.refs_5_), channel_id=1, source_target_pairs={{0,3},{1,0},{2,1},{3,2},{4,7},{5,4},{6,5},{7,6},{8,11},{9,8},{10,9... | collective-permute-start | bytes 1572872 | tf_op jit(solution)/shard_map/ppermute | solution.py:362
  59.4 2.2 %collective-permute-start.5 = (bf16[1024,128]{1,0:T(8,128)(2,1)}, bf16[1024,128]{1,0:T(8,128)(2,1)}, u32[]{:S(2)}, u32[]{:S(2)}) collective-permute-start(bf16[1024,128]{1,0:T(8,128)(2,1)} %slice.17), channel_id=1, source_target_pairs={{0,3},{1,0},{2,1},{3,2},{4,7},{5,4},{6,5},{7,6},{8,11},{9,8},{10,9... | collective-permute-start | bytes 786440 | tf_op jit(solution)/shard_map/ppermute | solution.py:362
  62.4 2.6 %collective-permute-done.8.refs_3_ = bf16[2048,128]{1,0:T(8,128)(2,1)S(1)} collective-permute-done((bf16[2048,128]{1,0:T(8,128)(2,1)S(1)}, bf16[2048,128]{1,0:T(8,128)(2,1)S(1)}, u32[]{:S(2)}, u32[]{:S(2)}) %collective-permute-start.8) | collective-permute-done | bytes 524320 | tf_op jit(solution)/shard_map/ppermute | solution.py:362
  65.8 3.4 %collective-permute-start.3 = (bf16[1024,128]{1,0:T(8,128)(2,1)}, bf16[1024,128]{1,0:T(8,128)(2,1)}, u32[]{:S(2)}, u32[]{:S(2)}) collective-permute-start(bf16[1024,128]{1,0:T(8,128)(2,1)} %slice.16), channel_id=1, source_target_pairs={{0,1},{1,2},{2,3},{3,0},{4,5},{5,6},{6,7},{7,4},{8,9},{9,10},{10,1... | collective-permute-start | bytes 786440 | tf_op jit(solution)/shard_map/ppermute | solution.py:362
  69.2 1.2 shard_map.143.pair
  70.4 4.3 %shard_map.144 = (bf16[128,384]{1,0:T(8,128)(2,1)}, f32[128,2048]{1,0:T(8,128)S(1)}, f32[128,128]{1,0:T(8,128)S(1)}) custom-call(s32[2]{0:T(128)S(1)} %pad_add_fusion.sc, bf16[128,4224]{1,0:T(8,128)(2,1)S(1)} %shard_map.143.pair, bf16[2048,128]{1,0:T(8,128)(2,1)} %bitcast.21, bf16[2048,128]{1,0:T(8,128)(2,1)} %bitcast.26, ...), custom_call_target="tpu_custom_call" | custom-call | tf_op jit(solution)/shard_map/pallas_call | solution.py:79
  74.8 6.0 %collective-permute-done.5.up_b = bf16[1024,128]{1,0:T(8,128)(2,1)} collective-permute-done((bf16[1024,128]{1,0:T(8,128)(2,1)}, bf16[1024,128]{1,0:T(8,128)(2,1)}, u32[]{:S(2)}, u32[]{:S(2)}) %collective-permute-start.5) | collective-permute-done | bytes 262176 | tf_op jit(solution)/shard_map/ppermute | solution.py:362
  80.8 4.4 %shard_map.145 = bf16[1024,640]{1,0:T(8,128)(2,1)} custom-call(s32[2]{0:T(128)S(1)} %pad_add_fusion.sc, bf16[128,4224]{1,0:T(8,128)(2,1)S(1)} %shard_map.143.pair, bf16[2048,128]{1,0:T(8,128)(2,1)} %collective-permute-done.1.gate, bf16[1024,128]{1,0:T(8,128)(2,1)} %collective-permute-done.3.up_a, bf16[1024,128]{1,0:T(8,128)(2,1)} %collective-permute-done.5.up_b, ...), custom_call_target="tpu_custom_call" | custom-call | tf_op jit(solution)/shard_map/pallas_call | solution.py:79
  85.2 13.7 %all-to-all-start.1 = ((bf16[128,8,640]{2,1,0:T(8,128)(2,1)}), bf16[128,8,640]{2,1,0:T(8,128)(2,1)S(1)}, u32[]{:S(2)}, u32[]{:S(2)}) async-start(bf16[128,8,640]{2,1,0:T(8,128)(2,1)} %bitcast.20), calls=%async_computation.1 | async-start | bytes 2621440 | tf_op jit(solution)/shard_map/all_to_all | solution.py:418
  98.9 4.9 %collective-permute-start.12 = (bf16[128,4224]{1,0:T(8,128)(2,1)S(1)}, bf16[128,4224]{1,0:T(8,128)(2,1)S(1)}, u32[]{:S(2)}, u32[]{:S(2)}) collective-permute-start(bf16[128,4224]{1,0:T(8,128)(2,1)S(1)} %shard_map.143.pair), channel_id=1, source_target_pairs={{0,3},{1,0},{2,1},{3,2},{4,7},{5,4},{6,5},{7,6},{8,11},{9,8},{10,9... | collective-permute-start | bytes 3244040 | tf_op jit(solution)/shard_map/ppermute | solution.py:362
  103.8 1.9 %collective-permute-start.10 = (bf16[128,4224]{1,0:T(8,128)(2,1)S(1)}, bf16[128,4224]{1,0:T(8,128)(2,1)S(1)}, u32[]{:S(2)}, u32[]{:S(2)}) collective-permute-start(bf16[128,4224]{1,0:T(8,128)(2,1)S(1)} %shard_map.143.pair), channel_id=1, source_target_pairs={{0,1},{1,2},{2,3},{3,0},{4,5},{5,6},{6,7},{7,4},{8,9},{9,10},{10,1... | collective-permute-start | bytes 3244040 | tf_op jit(solution)/shard_map/ppermute | solution.py:362
  105.7 21.4 %collective-permute-done.12.pair_3 = bf16[128,4224]{1,0:T(8,128)(2,1)S(1)} collective-permute-done((bf16[128,4224]{1,0:T(8,128)(2,1)S(1)}, bf16[128,4224]{1,0:T(8,128)(2,1)S(1)}, u32[]{:S(2)}, u32[]{:S(2)}) %collective-permute-start.12) | collective-permute-done | bytes 1081376 | tf_op jit(solution)/shard_map/ppermute | solution.py:362
  127.2 5.6 %collective-permute-start.13 = (bf16[64,4224]{1,0:T(8,128)(2,1)S(1)}, bf16[64,4224]{1,0:T(8,128)(2,1)S(1)}, u32[]{:S(2)}, u32[]{:S(2)}) collective-permute-start(bf16[64,4224]{1,0:T(8,128)(2,1)S(1)} %slice.19), channel_id=1, source_target_pairs={{0,3},{1,0},{2,1},{3,2},{4,7},{5,4},{6,5},{7,6},{8,11},{9,8},{10,9... | collective-permute-start | bytes 1622024 | tf_op jit(solution)/shard_map/ppermute | solution.py:362
  132.9 2.1 %collective-permute-start.11 = (bf16[64,4224]{1,0:T(8,128)(2,1)S(1)}, bf16[64,4224]{1,0:T(8,128)(2,1)S(1)}, u32[]{:S(2)}, u32[]{:S(2)}) collective-permute-start(bf16[64,4224]{1,0:T(8,128)(2,1)S(1)} %slice.18), channel_id=1, source_target_pairs={{0,1},{1,2},{2,3},{3,0},{4,5},{5,6},{6,7},{7,4},{8,9},{9,10},{10,1... | collective-permute-start | bytes 1622024 | tf_op jit(solution)/shard_map/ppermute | solution.py:362
  135.0 3.9 %shard_map.146 = (bf16[128,384]{1,0:T(8,128)(2,1)}, bf16[128,384]{1,0:T(8,128)(2,1)}) custom-call(s32[2]{0:T(128)S(1)} %pad_add_fusion.sc, bf16[128,4224]{1,0:T(8,128)(2,1)} %copy-done.7, bf16[128,4224]{1,0:T(8,128)(2,1)} %copy-done.6, bf16[2048,128]{1,0:T(8,128)(2,1)} %bitcast.22, bf16[2048,128]{1,0:T(8,128)(2,1)} %bitcast.27, ...), custom_call_target="tpu_custom_call" | custom-call | tf_op jit(solution)/shard_map/pallas_call | solution.py:79
  138.9 4.8 %collective-permute-done.13.bottom = bf16[64,4224]{1,0:T(8,128)(2,1)S(1)} collective-permute-done((bf16[64,4224]{1,0:T(8,128)(2,1)S(1)}, bf16[64,4224]{1,0:T(8,128)(2,1)S(1)}, u32[]{:S(2)}, u32[]{:S(2)}) %collective-permute-start.13) | collective-permute-done | bytes 540704 | tf_op jit(solution)/shard_map/ppermute | solution.py:362
  143.8 5.4 %collective-permute-done.11.top = bf16[64,4224]{1,0:T(8,128)(2,1)S(1)} collective-permute-done((bf16[64,4224]{1,0:T(8,128)(2,1)S(1)}, bf16[64,4224]{1,0:T(8,128)(2,1)S(1)}, u32[]{:S(2)}, u32[]{:S(2)}) %collective-permute-start.11) | collective-permute-done | bytes 540704 | tf_op jit(solution)/shard_map/ppermute | solution.py:362
  149.2 0.8 copy-done.13
  150.0 5.7 %shard_map.147 = (bf16[2048,128]{1,0:T(8,128)(2,1)}, bf16[2048,128]{1,0:T(8,128)(2,1)}, bf16[128,2048]{1,0:T(8,128)(2,1)}, f32[1,128]{1,0:T(1,128)}, bf16[16,512]{1,0:T(8,128)(2,1)S(1)}) custom-call(s32[2]{0:T(128)S(1)} %pad_add_fusion.sc, bf16[128,4224]{1,0:T(8,128)(2,1)} %copy-done, bf16[128,4224]{1,0:T(8,128)(2,1)} %copy-done.7, ...), custom_call_target="tpu_custom_call" | custom-call | tf_op jit(solution)/shard_map/pallas_call | solution.py:79
  155.7 1.0 shard_map.148
  156.8 11.9 %all_to_all.15.got = bf16[4,160,512]{2,1,0:T(8,128)(2,1)S(1)} all-to-all(bf16[4,160,512]{2,1,0:T(8,128)(2,1)S(1)} %shard_map.148), channel_id=1, replica_groups=mesh['ep_0'=8,'ep_1'=8,'ep_2'=2,'tp'=4] {'tp'}, dimensions={0} | all-to-all | bytes 1310720 | tf_op jit(solution)/shard_map/all_to_all | solution.py:451
  168.6 1.4 shard_map.149
  (44 shorter events, 2.9 us)
Async XLA Ops:
  4.9 17.5 %copy-start.8 = (bf16[1,2048,128]{2,1,0:T(8,128)(2,1)S(1)}, bf16[1,2048,128]{2,1,0:T(8,128)(2,1)}, u32[]{:S(2)}) copy-start(bf16[1,2048,128]{2,1,0:T(8,128)(2,1)} %param.11) | copy-start | bytes 1572868
  4.9 20.9 %copy-start.9 = (bf16[1,2048,128]{2,1,0:T(8,128)(2,1)S(1)}, bf16[1,2048,128]{2,1,0:T(8,128)(2,1)}, u32[]{:S(2)}) copy-start(bf16[1,2048,128]{2,1,0:T(8,128)(2,1)} %param.12) | copy-start | bytes 1572868
  4.9 64.3 %all-to-all-start = ((bf16[128,8,640]{2,1,0:T(8,128)(2,1)}), bf16[128,8,640]{2,1,0:T(8,128)(2,1)S(1)}, u32[]{:S(2)}, u32[]{:S(2)}) async-start(bf16[128,8,640]{2,1,0:T(8,128)(2,1)} %bitcast.31), calls=%async_computation | async-start | bytes 2621440 | tf_op jit(solution)/shard_map/all_to_all | solution.py:387
  22.4 18.0 %collective-permute-start = (bf16[2048,128]{1,0:T(8,128)(2,1)S(1)}, bf16[2048,128]{1,0:T(8,128)(2,1)}, u32[]{:S(2)}, u32[]{:S(2)}) collective-permute-start(bf16[2048,128]{1,0:T(8,128)(2,1)S(1)} %bitcast.24), channel_id=1, source_target_pairs={{0,1},{1,2},{2,3},{3,0},{4,5},{5,6},{6,7},{7,4},{8,9},{9,10},{10,1... | collective-permute-start | bytes 1572872 | tf_op jit(solution)/shard_map/ppermute | solution.py:362
  25.8 16.8 %collective-permute-start.4 = (bf16[2048,128]{1,0:T(8,128)(2,1)S(1)}, bf16[2048,128]{1,0:T(8,128)(2,1)S(1)}, u32[]{:S(2)}, u32[]{:S(2)}) collective-permute-start(bf16[2048,128]{1,0:T(8,128)(2,1)S(1)} %bitcast.29), channel_id=1, source_target_pairs={{0,3},{1,0},{2,1},{3,2},{4,7},{5,4},{6,5},{7,6},{8,11},{9,8},{10,9... | collective-permute-start | bytes 1572872 | tf_op jit(solution)/shard_map/ppermute | solution.py:362
  29.5 24.4 %collective-permute-start.6 = (bf16[128,2048]{1,0:T(8,128)(2,1)}, bf16[128,2048]{1,0:T(8,128)(2,1)}, u32[]{:S(2)}, u32[]{:S(2)}) collective-permute-start(bf16[128,2048]{1,0:T(8,128)(2,1)} %bitcast.7.refs_2_.down.down_w), channel_id=1, source_target_pairs={{0,3},{1,0},{2,1},{3,2},{4,7},{5,4},{6,5},{7,6},{8,11},{9,8},{10,9... | collective-permute-start | bytes 1572872 | tf_op jit(solution)/shard_map/ppermute | solution.py:362
  32.9 26.5 %collective-permute-start.2 = (bf16[2048,128]{1,0:T(8,128)(2,1)S(1)}, bf16[2048,128]{1,0:T(8,128)(2,1)S(1)}, u32[]{:S(2)}, u32[]{:S(2)}) collective-permute-start(bf16[2048,128]{1,0:T(8,128)(2,1)S(1)} %bitcast.30), channel_id=1, source_target_pairs={{0,1},{1,2},{2,3},{3,0},{4,5},{5,6},{6,7},{7,4},{8,9},{9,10},{10,1... | collective-permute-start | bytes 1572872 | tf_op jit(solution)/shard_map/ppermute | solution.py:362
  35.3 29.6 %collective-permute-start.8 = (bf16[2048,128]{1,0:T(8,128)(2,1)S(1)}, bf16[2048,128]{1,0:T(8,128)(2,1)S(1)}, u32[]{:S(2)}, u32[]{:S(2)}) collective-permute-start(bf16[2048,128]{1,0:T(8,128)(2,1)S(1)} %bitcast.25), channel_id=1, source_target_pairs={{0,3},{1,0},{2,1},{3,2},{4,7},{5,4},{6,5},{7,6},{8,11},{9,8},{10,9... | collective-permute-start | bytes 1572872 | tf_op jit(solution)/shard_map/ppermute | solution.py:362
  40.4 30.0 %collective-permute-start.9 = (bf16[128,2048]{1,0:T(8,128)(2,1)}, bf16[128,2048]{1,0:T(8,128)(2,1)}, u32[]{:S(2)}, u32[]{:S(2)}) collective-permute-start(bf16[128,2048]{1,0:T(8,128)(2,1)} %bitcast.7.refs_2_.down.down_w), channel_id=1, source_target_pairs={{0,1},{1,2},{2,3},{3,0},{4,5},{5,6},{6,7},{7,4},{8,9},{9,10},{10,1... | collective-permute-start | bytes 1572872 | tf_op jit(solution)/shard_map/ppermute | solution.py:362
  42.6 27.8 %copy-start.10 = (bf16[2048,128]{1,0:T(8,128)(2,1)}, bf16[2048,128]{1,0:T(8,128)(2,1)S(1)}, u32[]{:S(2)}) copy-start(bf16[2048,128]{1,0:T(8,128)(2,1)S(1)} %collective-permute-done.4.refs_4_) | copy-start | bytes 1572868
  42.6 38.2 %collective-permute-start.1 = (bf16[2048,128]{1,0:T(8,128)(2,1)}, bf16[2048,128]{1,0:T(8,128)(2,1)}, u32[]{:S(2)}, u32[]{:S(2)}) collective-permute-start(bf16[2048,128]{1,0:T(8,128)(2,1)} %collective-permute-done.refs_6_), channel_id=1, source_target_pairs={{0,1},{1,2},{2,3},{3,0},{4,5},{5,6},{6,7},{7,4},{8,9},{9,10},{10,1... | collective-permute-start | bytes 1572872 | tf_op jit(solution)/shard_map/ppermute | solution.py:362
  53.8 27.0 %collective-permute-start.7 = (bf16[128,2048]{1,0:T(8,128)(2,1)}, bf16[128,2048]{1,0:T(8,128)(2,1)}, u32[]{:S(2)}, u32[]{:S(2)}) collective-permute-start(bf16[128,2048]{1,0:T(8,128)(2,1)} %collective-permute-done.6.refs_5_), channel_id=1, source_target_pairs={{0,3},{1,0},{2,1},{3,2},{4,7},{5,4},{6,5},{7,6},{8,11},{9,8},{10,9... | collective-permute-start | bytes 1572872 | tf_op jit(solution)/shard_map/ppermute | solution.py:362
  59.4 11.0 %copy-start.11 = (bf16[2048,128]{1,0:T(8,128)(2,1)}, bf16[2048,128]{1,0:T(8,128)(2,1)S(1)}, u32[]{:S(2)}) copy-start(bf16[2048,128]{1,0:T(8,128)(2,1)S(1)} %collective-permute-done.2.refs_7_) | copy-start | bytes 1572868
  59.4 21.4 %collective-permute-start.5 = (bf16[1024,128]{1,0:T(8,128)(2,1)}, bf16[1024,128]{1,0:T(8,128)(2,1)}, u32[]{:S(2)}, u32[]{:S(2)}) collective-permute-start(bf16[1024,128]{1,0:T(8,128)(2,1)} %slice.17), channel_id=1, source_target_pairs={{0,3},{1,0},{2,1},{3,2},{4,7},{5,4},{6,5},{7,6},{8,11},{9,8},{10,9... | collective-permute-start | bytes 786440 | tf_op jit(solution)/shard_map/ppermute | solution.py:362
  65.0 0.8 copy-start.14
  65.8 15.0 %collective-permute-start.3 = (bf16[1024,128]{1,0:T(8,128)(2,1)}, bf16[1024,128]{1,0:T(8,128)(2,1)}, u32[]{:S(2)}, u32[]{:S(2)}) collective-permute-start(bf16[1024,128]{1,0:T(8,128)(2,1)} %slice.16), channel_id=1, source_target_pairs={{0,1},{1,2},{2,3},{3,0},{4,5},{5,6},{6,7},{7,4},{8,9},{9,10},{10,1... | collective-permute-start | bytes 786440 | tf_op jit(solution)/shard_map/ppermute | solution.py:362
  70.4 33.4 %copy-start = (bf16[128,4224]{1,0:T(8,128)(2,1)}, bf16[128,4224]{1,0:T(8,128)(2,1)S(1)}, u32[]{:S(2)}) copy-start(bf16[128,4224]{1,0:T(8,128)(2,1)S(1)} %shard_map.143.pair) | copy-start | bytes 3244036
  85.2 70.5 %all-to-all-start.1 = ((bf16[128,8,640]{2,1,0:T(8,128)(2,1)}), bf16[128,8,640]{2,1,0:T(8,128)(2,1)S(1)}, u32[]{:S(2)}, u32[]{:S(2)}) async-start(bf16[128,8,640]{2,1,0:T(8,128)(2,1)} %bitcast.20), calls=%async_computation.1 | async-start | bytes 2621440 | tf_op jit(solution)/shard_map/all_to_all | solution.py:418
  98.9 28.3 %collective-permute-start.12 = (bf16[128,4224]{1,0:T(8,128)(2,1)S(1)}, bf16[128,4224]{1,0:T(8,128)(2,1)S(1)}, u32[]{:S(2)}, u32[]{:S(2)}) collective-permute-start(bf16[128,4224]{1,0:T(8,128)(2,1)S(1)} %shard_map.143.pair), channel_id=1, source_target_pairs={{0,3},{1,0},{2,1},{3,2},{4,7},{5,4},{6,5},{7,6},{8,11},{9,8},{10,9... | collective-permute-start | bytes 3244040 | tf_op jit(solution)/shard_map/ppermute | solution.py:362
  103.8 29.0 %collective-permute-start.10 = (bf16[128,4224]{1,0:T(8,128)(2,1)S(1)}, bf16[128,4224]{1,0:T(8,128)(2,1)S(1)}, u32[]{:S(2)}, u32[]{:S(2)}) collective-permute-start(bf16[128,4224]{1,0:T(8,128)(2,1)S(1)} %shard_map.143.pair), channel_id=1, source_target_pairs={{0,1},{1,2},{2,3},{3,0},{4,5},{5,6},{6,7},{7,4},{8,9},{9,10},{10,1... | collective-permute-start | bytes 3244040 | tf_op jit(solution)/shard_map/ppermute | solution.py:362
  127.2 7.8 %copy-start.6 = (bf16[128,4224]{1,0:T(8,128)(2,1)}, bf16[128,4224]{1,0:T(8,128)(2,1)S(1)}, u32[]{:S(2)}) copy-start(bf16[128,4224]{1,0:T(8,128)(2,1)S(1)} %collective-permute-done.12.pair_3) | copy-start | bytes 3244036
  127.2 16.5 %collective-permute-start.13 = (bf16[64,4224]{1,0:T(8,128)(2,1)S(1)}, bf16[64,4224]{1,0:T(8,128)(2,1)S(1)}, u32[]{:S(2)}, u32[]{:S(2)}) collective-permute-start(bf16[64,4224]{1,0:T(8,128)(2,1)S(1)} %slice.19), channel_id=1, source_target_pairs={{0,3},{1,0},{2,1},{3,2},{4,7},{5,4},{6,5},{7,6},{8,11},{9,8},{10,9... | collective-permute-start | bytes 1622024 | tf_op jit(solution)/shard_map/ppermute | solution.py:362
  132.8 2.2 %copy-start.7 = (bf16[128,4224]{1,0:T(8,128)(2,1)}, bf16[128,4224]{1,0:T(8,128)(2,1)S(1)}, u32[]{:S(2)}) copy-start(bf16[128,4224]{1,0:T(8,128)(2,1)S(1)} %collective-permute-done.10.pair_1) | copy-start | bytes 3244036
  132.9 16.3 %collective-permute-start.11 = (bf16[64,4224]{1,0:T(8,128)(2,1)S(1)}, bf16[64,4224]{1,0:T(8,128)(2,1)S(1)}, u32[]{:S(2)}, u32[]{:S(2)}) collective-permute-start(bf16[64,4224]{1,0:T(8,128)(2,1)S(1)} %slice.18), channel_id=1, source_target_pairs={{0,1},{1,2},{2,3},{3,0},{4,5},{5,6},{6,7},{7,4},{8,9},{9,10},{10,1... | collective-permute-start | bytes 1622024 | tf_op jit(solution)/shard_map/ppermute | solution.py:362
  143.8 5.4 %copy-start.12 = (bf16[64,4224]{1,0:T(8,128)(2,1)}, bf16[64,4224]{1,0:T(8,128)(2,1)S(1)}, u32[]{:S(2)}) copy-start(bf16[64,4224]{1,0:T(8,128)(2,1)S(1)} %collective-permute-done.13.bottom) | copy-start | bytes 1622020
  149.2 0.8 copy-start.13
  150.0 5.7 %copy-start.2 = (bf16[128,128]{1,0:T(8,128)(2,1)S(1)}, bf16[128,128]{1,0:T(8,128)(2,1)}, u32[]{:S(2)}) copy-start(bf16[128,128]{1,0:T(8,128)(2,1)} %get-tuple-element.31.hit0) | copy-start | bytes 98308
  150.0 5.7 %copy-start.3 = (bf16[128,128]{1,0:T(8,128)(2,1)S(1)}, bf16[128,128]{1,0:T(8,128)(2,1)}, u32[]{:S(2)}) copy-start(bf16[128,128]{1,0:T(8,128)(2,1)} %get-tuple-element.32.hit1) | copy-start | bytes 98308
  155.7 12.9 %copy-start.1 = (bf16[2048,128]{1,0:T(8,128)(2,1)S(1)}, bf16[2048,128]{1,0:T(8,128)(2,1)}, u32[]{:S(2)}) copy-start(bf16[2048,128]{1,0:T(8,128)(2,1)} %router.3) | copy-start | bytes 1572868
  155.7 12.9 %copy-start.4 = (f32[8,128]{1,0:T(8,128)S(1)}, f32[8,128]{1,0:T(8,128)}, u32[]{:S(2)}) copy-start(f32[8,128]{1,0:T(8,128)} %get-tuple-element.37.stats) | copy-start | bytes 12292
  155.7 12.9 %copy-start.5 = (s32[128,2]{0,1:T(2,128)S(1)}, s32[128,2]{0,1:T(2,128)}, u32[]{:S(2)}) copy-start(s32[128,2]{0,1:T(2,128)} %param.9) | copy-start | bytes 3076

commit v6 on v5

--- a/solution.py
+++ b/solution.py
@@ -218,10 +218,9 @@
         out[:, 2 * FQ :] = scaled
 
 
-def emit_kernel(sc, pair, gate, up_a, up_b, down, back, gg_in, send, scratch):
+def emit_kernel(sc, pair, gate, up, down, back, gg_in, send, scratch):
     about = pair[:, 2 * D :].astype(F32)
-    up = jnp.concatenate([up_a[...], up_b[...]], axis=0)
-    both = jnp.concatenate([gate[...], up], axis=1)
+    both = jnp.concatenate([gate[...], up[...]], axis=1)
     g_in, _, gg = hidden_grads(pair, both, down[...])
     term = back[...] + dot(g_in, both, 1, 1)
     gg = gg + gg_in[:, 0:1]
@@ -365,12 +364,11 @@
     down_3 = shift(down_w, 3)
     up_1 = shift(up_w, 1)
     up_3 = shift(up_w, 3)
+    gate_2 = shift(gate_1, 1)
+    gate_3 = shift(gate_w, 3)
     down_1 = shift(down_w, 1)
-    gate_3 = shift(gate_w, 3)
-    gate_2 = shift(gate_1, 1)
     down_2 = shift(down_3, 3)
-    up_2a = shift(up_1[0 : D // 2], 1)
-    up_2b = shift(up_3[D // 2 :], 3)
+    up_2 = shift(up_1, 1)
 
     send, hit0, hit1, stats = call(
         dispatch_kernel,
@@ -411,7 +409,7 @@
     (send_back,) = call(
         emit_kernel,
         sc,
-        (pair, *(whole(far(x)) for x in (gate_2, up_2a, up_2b, down_2)), back, gg),
+        (pair, *(whole(far(x)) for x in (gate_2, up_2, down_2)), back, gg),
         (hbm((SENT, 2 * CH + 128), BF16),),
         (pltpu.VMEM((CH // 128, SENT, 128), F32),),
     )

time: 171 us -> 177 us (1.035)
  waiting for transfers between devices: 48.5 us -> 63.7 us
  starting transfers between devices: 79.4 us -> 72.1 us
  local copies, waits for them, and re-layouts: 3.17 us -> 0.94 us
    ppermute x14 -> x13, waiting for transfers between devices: 48.5 us -> 63.7 us  [shift(): return lax.ppermute(x, 'tp', [(a, (a + d) % TP) for a in range(TP)])]
    ppermute x14 -> x13, starting transfers between devices: 48.1 us -> 40.8 us  [shift(): return lax.ppermute(x, 'tp', [(a, (a + d) % TP) for a in range(TP)])]
  transfers between devices with their start and end apart: 16 -> 15, of which waited for: 7 -> 8; matrix products, arithmetic and copies ran while one was open for 1% -> 0% of each run, Pallas kernels for 9% -> 9%
where the time goes in v6:
time: 177 us; the launch traced here: 176 us
  starting transfers between devices  72.1 us (41%)
  waiting for transfers between devices  63.7 us (36%)
  Pallas kernels  26.1 us (15%)
  blocking collectives  12.1 us (7%)
    ppermute x13, waiting for transfers between devices, shift(): return lax.ppermute(x, 'tp', [(a, (a + d) % TP) for a in range(TP)])  63.7 us
    ppermute x13, starting transfers between devices, shift(): return lax.ppermute(x, 'tp', [(a, (a + d) % TP) for a in range(TP)])  40.8 us
    pallas_call x8, Pallas kernels, call(): pl.pallas_call(kernel, grid_spec=pltpu.PrefetchScalarGridSpec(num_scalar_...  26.1 us
    all_to_all x1, starting transfers between devices, layer(): lax.all_to_all(send.reshape(EXPERTS, 8, 2 * CH + 128), EP, 0, 0, tiled=True)  17.5 us
    all_to_all x1, starting transfers between devices, layer(): lax.all_to_all(send_back.reshape(EXPERTS, 8, 2 * CH + 128), EP, 0, 0, til...  13.7 us
    all_to_all x1, blocking collectives, layer(): parts = lax.all_to_all(parts, 'tp', 0, 0, tiled=True)  12.1 us
  transfers between devices with their start and end apart: 15, of which 8 were waited for; matrix products, arithmetic and copies ran while one was open for 0% of the time, Pallas kernels for 9%

profile of v6, /device:TPU:8, one launch (start us, length us, event | category | flops | bytes accessed | tf_op | source)
XLA Modules:
  0.0 176.0 jit_solution(14671218502012732380)
XLA Ops:
  0.7 4.1 %shard_map.142 = (bf16[1024,640]{1,0:T(8,128)(2,1)}, bf16[128,128]{1,0:T(8,128)(2,1)}, bf16[128,128]{1,0:T(8,128)(2,1)}, f32[8,128]{1,0:T(8,128)}) custom-call(s32[2]{0:T(128)S(1)} %pad_add_fusion.sc, bf16[128,2048]{1,0:T(8,128)(2,1)} %tok.1, bf16[128,2048]{1,0:T(8,128)(2,1)} %cot.1, s32[2,128]{1,0:T(2,128)} %bitcast.18, bf16[2048,128]{1,0:T(8,128)(2,1)} %router.3), custom_call_target="tpu_custom_call" | custom-call | tf_op jit(solution)/shard_map/pallas_call | solution.py:79
  4.9 17.5 %all-to-all-start = ((bf16[128,8,640]{2,1,0:T(8,128)(2,1)}), bf16[128,8,640]{2,1,0:T(8,128)(2,1)S(1)}, u32[]{:S(2)}, u32[]{:S(2)}) async-start(bf16[128,8,640]{2,1,0:T(8,128)(2,1)} %bitcast.31), calls=%async_computation | async-start | bytes 2621440 | tf_op jit(solution)/shard_map/all_to_all | solution.py:385
  22.4 4.7 %collective-permute-start.6 = (bf16[2048,128]{1,0:T(8,128)(2,1)S(1)}, bf16[2048,128]{1,0:T(8,128)(2,1)S(1)}, u32[]{:S(2)}, u32[]{:S(2)}) collective-permute-start(bf16[2048,128]{1,0:T(8,128)(2,1)S(1)} %bitcast.24), channel_id=1, source_target_pairs={{0,3},{1,0},{2,1},{3,2},{4,7},{5,4},{6,5},{7,6},{8,11},{9,8},{10,9... | collective-permute-start | bytes 1572872 | tf_op jit(solution)/shard_map/ppermute | solution.py:361
  27.1 1.9 %collective-permute-start = (bf16[2048,128]{1,0:T(8,128)(2,1)S(1)}, bf16[2048,128]{1,0:T(8,128)(2,1)}, u32[]{:S(2)}, u32[]{:S(2)}) collective-permute-start(bf16[2048,128]{1,0:T(8,128)(2,1)S(1)} %bitcast.25), channel_id=1, source_target_pairs={{0,1},{1,2},{2,3},{3,0},{4,5},{5,6},{6,7},{7,4},{8,9},{9,10},{10,1... | collective-permute-start | bytes 1572872 | tf_op jit(solution)/shard_map/ppermute | solution.py:361
  29.0 2.7 %collective-permute-start.2 = (bf16[2048,128]{1,0:T(8,128)(2,1)S(1)}, bf16[2048,128]{1,0:T(8,128)(2,1)}, u32[]{:S(2)}, u32[]{:S(2)}) collective-permute-start(bf16[2048,128]{1,0:T(8,128)(2,1)S(1)} %bitcast.29), channel_id=1, source_target_pairs={{0,1},{1,2},{2,3},{3,0},{4,5},{5,6},{6,7},{7,4},{8,9},{9,10},{10,1... | collective-permute-start | bytes 1572872 | tf_op jit(solution)/shard_map/ppermute | solution.py:361
  31.7 4.4 %collective-permute-start.4 = (bf16[128,2048]{1,0:T(8,128)(2,1)}, bf16[128,2048]{1,0:T(8,128)(2,1)}, u32[]{:S(2)}, u32[]{:S(2)}) collective-permute-start(bf16[128,2048]{1,0:T(8,128)(2,1)} %bitcast.7.refs_2_.down.down_w), channel_id=1, source_target_pairs={{0,3},{1,0},{2,1},{3,2},{4,7},{5,4},{6,5},{7,6},{8,11},{9,8},{10,9... | collective-permute-start | bytes 1572872 | tf_op jit(solution)/shard_map/ppermute | solution.py:361
  36.1 3.9 %collective-permute-start.7 = (bf16[2048,128]{1,0:T(8,128)(2,1)S(1)}, bf16[2048,128]{1,0:T(8,128)(2,1)}, u32[]{:S(2)}, u32[]{:S(2)}) collective-permute-start(bf16[2048,128]{1,0:T(8,128)(2,1)S(1)} %bitcast.30), channel_id=1, source_target_pairs={{0,3},{1,0},{2,1},{3,2},{4,7},{5,4},{6,5},{7,6},{8,11},{9,8},{10,9... | collective-permute-start | bytes 1572872 | tf_op jit(solution)/shard_map/ppermute | solution.py:361
  40.0 2.4 %collective-permute-start.8 = (bf16[128,2048]{1,0:T(8,128)(2,1)}, bf16[128,2048]{1,0:T(8,128)(2,1)}, u32[]{:S(2)}, u32[]{:S(2)}) collective-permute-start(bf16[128,2048]{1,0:T(8,128)(2,1)} %bitcast.7.refs_2_.down.down_w), channel_id=1, source_target_pairs={{0,1},{1,2},{2,3},{3,0},{4,5},{5,6},{6,7},{7,4},{8,9},{9,10},{10,1... | collective-permute-start | bytes 1572872 | tf_op jit(solution)/shard_map/ppermute | solution.py:361
  42.5 2.6 %collective-permute-done.refs_6_ = bf16[2048,128]{1,0:T(8,128)(2,1)} collective-permute-done((bf16[2048,128]{1,0:T(8,128)(2,1)S(1)}, bf16[2048,128]{1,0:T(8,128)(2,1)}, u32[]{:S(2)}, u32[]{:S(2)}) %collective-permute-start) | collective-permute-done | bytes 524320 | tf_op jit(solution)/shard_map/ppermute | solution.py:361
  45.1 1.9 %collective-permute-start.1 = (bf16[2048,128]{1,0:T(8,128)(2,1)}, bf16[2048,128]{1,0:T(8,128)(2,1)}, u32[]{:S(2)}, u32[]{:S(2)}) collective-permute-start(bf16[2048,128]{1,0:T(8,128)(2,1)} %collective-permute-done.refs_6_), channel_id=1, source_target_pairs={{0,1},{1,2},{2,3},{3,0},{4,5},{5,6},{6,7},{7,4},{8,9},{9,10},{10,1... | collective-permute-start | bytes 1572872 | tf_op jit(solution)/shard_map/ppermute | solution.py:361
  47.0 9.3 %collective-permute-done.2.refs_7_ = bf16[2048,128]{1,0:T(8,128)(2,1)} collective-permute-done((bf16[2048,128]{1,0:T(8,128)(2,1)S(1)}, bf16[2048,128]{1,0:T(8,128)(2,1)}, u32[]{:S(2)}, u32[]{:S(2)}) %collective-permute-start.2) | collective-permute-done | bytes 524320 | tf_op jit(solution)/shard_map/ppermute | solution.py:361
  56.3 1.9 %collective-permute-start.3 = (bf16[2048,128]{1,0:T(8,128)(2,1)}, bf16[2048,128]{1,0:T(8,128)(2,1)}, u32[]{:S(2)}, u32[]{:S(2)}) collective-permute-start(bf16[2048,128]{1,0:T(8,128)(2,1)} %collective-permute-done.2.refs_7_), channel_id=1, source_target_pairs={{0,1},{1,2},{2,3},{3,0},{4,5},{5,6},{6,7},{7,4},{8,9},{9,10},{10,1... | collective-permute-start | bytes 1572872 | tf_op jit(solution)/shard_map/ppermute | solution.py:361
  58.2 5.1 %collective-permute-start.5 = (bf16[128,2048]{1,0:T(8,128)(2,1)}, bf16[128,2048]{1,0:T(8,128)(2,1)}, u32[]{:S(2)}, u32[]{:S(2)}) collective-permute-start(bf16[128,2048]{1,0:T(8,128)(2,1)} %collective-permute-done.4.refs_5_), channel_id=1, source_target_pairs={{0,3},{1,0},{2,1},{3,2},{4,7},{5,4},{6,5},{7,6},{8,11},{9,8},{10,9... | collective-permute-start | bytes 1572872 | tf_op jit(solution)/shard_map/ppermute | solution.py:361
  63.4 1.2 shard_map.143.pair
  64.6 2.9 %collective-permute-done.8.refs_8_ = bf16[128,2048]{1,0:T(8,128)(2,1)} collective-permute-done((bf16[128,2048]{1,0:T(8,128)(2,1)}, bf16[128,2048]{1,0:T(8,128)(2,1)}, u32[]{:S(2)}, u32[]{:S(2)}) %collective-permute-start.8) | collective-permute-done | bytes 524320 | tf_op jit(solution)/shard_map/ppermute | solution.py:361
  67.6 4.3 %shard_map.144 = (bf16[128,384]{1,0:T(8,128)(2,1)}, f32[128,2048]{1,0:T(8,128)S(1)}, f32[128,128]{1,0:T(8,128)S(1)}) custom-call(s32[2]{0:T(128)S(1)} %pad_add_fusion.sc, bf16[128,4224]{1,0:T(8,128)(2,1)S(1)} %shard_map.143.pair, bf16[2048,128]{1,0:T(8,128)(2,1)} %bitcast.21, bf16[2048,128]{1,0:T(8,128)(2,1)} %bitcast.26, ...), custom_call_target="tpu_custom_call" | custom-call | tf_op jit(solution)/shard_map/pallas_call | solution.py:79
  71.9 6.9 %collective-permute-done.1.gate = bf16[2048,128]{1,0:T(8,128)(2,1)} collective-permute-done((bf16[2048,128]{1,0:T(8,128)(2,1)}, bf16[2048,128]{1,0:T(8,128)(2,1)}, u32[]{:S(2)}, u32[]{:S(2)}) %collective-permute-start.1) | collective-permute-done | bytes 524320 | tf_op jit(solution)/shard_map/ppermute | solution.py:361
  78.8 10.1 %collective-permute-done.3.up = bf16[2048,128]{1,0:T(8,128)(2,1)} collective-permute-done((bf16[2048,128]{1,0:T(8,128)(2,1)}, bf16[2048,128]{1,0:T(8,128)(2,1)}, u32[]{:S(2)}, u32[]{:S(2)}) %collective-permute-start.3) | collective-permute-done | bytes 524320 | tf_op jit(solution)/shard_map/ppermute | solution.py:361
  88.9 4.3 %shard_map.145 = bf16[1024,640]{1,0:T(8,128)(2,1)} custom-call(s32[2]{0:T(128)S(1)} %pad_add_fusion.sc, bf16[128,4224]{1,0:T(8,128)(2,1)S(1)} %shard_map.143.pair, bf16[2048,128]{1,0:T(8,128)(2,1)} %collective-permute-done.1.gate, bf16[2048,128]{1,0:T(8,128)(2,1)} %collective-permute-done.3.up, bf16[128,2048]{1,0:T(8,128)(2,1)} %collective-permute-done.5.down, ...), custom_call_target="tpu_custom_call" | custom-call | tf_op jit(solution)/shard_map/pallas_call | solution.py:79
  93.2 13.7 %all-to-all-start.1 = ((bf16[128,8,640]{2,1,0:T(8,128)(2,1)}), bf16[128,8,640]{2,1,0:T(8,128)(2,1)S(1)}, u32[]{:S(2)}, u32[]{:S(2)}) async-start(bf16[128,8,640]{2,1,0:T(8,128)(2,1)} %bitcast.20), calls=%async_computation.1 | async-start | bytes 2621440 | tf_op jit(solution)/shard_map/all_to_all | solution.py:416
  107.0 1.9 %collective-permute-start.11 = (bf16[128,4224]{1,0:T(8,128)(2,1)S(1)}, bf16[128,4224]{1,0:T(8,128)(2,1)S(1)}, u32[]{:S(2)}, u32[]{:S(2)}) collective-permute-start(bf16[128,4224]{1,0:T(8,128)(2,1)S(1)} %shard_map.143.pair), channel_id=1, source_target_pairs={{0,3},{1,0},{2,1},{3,2},{4,7},{5,4},{6,5},{7,6},{8,11},{9,8},{10,9... | collective-permute-start | bytes 3244040 | tf_op jit(solution)/shard_map/ppermute | solution.py:361
  108.9 3.9 %collective-permute-start.9 = (bf16[128,4224]{1,0:T(8,128)(2,1)S(1)}, bf16[128,4224]{1,0:T(8,128)(2,1)S(1)}, u32[]{:S(2)}, u32[]{:S(2)}) collective-permute-start(bf16[128,4224]{1,0:T(8,128)(2,1)S(1)} %shard_map.143.pair), channel_id=1, source_target_pairs={{0,1},{1,2},{2,3},{3,0},{4,5},{5,6},{6,7},{7,4},{8,9},{9,10},{10,1... | collective-permute-start | bytes 3244040 | tf_op jit(solution)/shard_map/ppermute | solution.py:361
  112.8 21.9 %collective-permute-done.11.pair_3 = bf16[128,4224]{1,0:T(8,128)(2,1)S(1)} collective-permute-done((bf16[128,4224]{1,0:T(8,128)(2,1)S(1)}, bf16[128,4224]{1,0:T(8,128)(2,1)S(1)}, u32[]{:S(2)}, u32[]{:S(2)}) %collective-permute-start.11) | collective-permute-done | bytes 1081376 | tf_op jit(solution)/shard_map/ppermute | solution.py:361
  134.8 3.4 %collective-permute-start.12 = (bf16[64,4224]{1,0:T(8,128)(2,1)S(1)}, bf16[64,4224]{1,0:T(8,128)(2,1)S(1)}, u32[]{:S(2)}, u32[]{:S(2)}) collective-permute-start(bf16[64,4224]{1,0:T(8,128)(2,1)S(1)} %slice.9), channel_id=1, source_target_pairs={{0,3},{1,0},{2,1},{3,2},{4,7},{5,4},{6,5},{7,6},{8,11},{9,8},{10,9... | collective-permute-start | bytes 1622024 | tf_op jit(solution)/shard_map/ppermute | solution.py:361
  138.3 2.6 %collective-permute-start.10 = (bf16[64,4224]{1,0:T(8,128)(2,1)S(1)}, bf16[64,4224]{1,0:T(8,128)(2,1)S(1)}, u32[]{:S(2)}, u32[]{:S(2)}) collective-permute-start(bf16[64,4224]{1,0:T(8,128)(2,1)S(1)} %slice.8), channel_id=1, source_target_pairs={{0,1},{1,2},{2,3},{3,0},{4,5},{5,6},{6,7},{7,4},{8,9},{9,10},{10,1... | collective-permute-start | bytes 1622024 | tf_op jit(solution)/shard_map/ppermute | solution.py:361
  140.9 3.9 %shard_map.146 = (bf16[128,384]{1,0:T(8,128)(2,1)}, bf16[128,384]{1,0:T(8,128)(2,1)}) custom-call(s32[2]{0:T(128)S(1)} %pad_add_fusion.sc, bf16[128,4224]{1,0:T(8,128)(2,1)} %copy-done.7, bf16[128,4224]{1,0:T(8,128)(2,1)} %copy-done.6, bf16[2048,128]{1,0:T(8,128)(2,1)} %bitcast.22, bf16[2048,128]{1,0:T(8,128)(2,1)} %bitcast.27, ...), custom_call_target="tpu_custom_call" | custom-call | tf_op jit(solution)/shard_map/pallas_call | solution.py:79
  144.8 5.3 %collective-permute-done.12.bottom = bf16[64,4224]{1,0:T(8,128)(2,1)S(1)} collective-permute-done((bf16[64,4224]{1,0:T(8,128)(2,1)S(1)}, bf16[64,4224]{1,0:T(8,128)(2,1)S(1)}, u32[]{:S(2)}, u32[]{:S(2)}) %collective-permute-start.12) | collective-permute-done | bytes 540704 | tf_op jit(solution)/shard_map/ppermute | solution.py:361
  150.1 4.7 %collective-permute-done.10.top = bf16[64,4224]{1,0:T(8,128)(2,1)S(1)} collective-permute-done((bf16[64,4224]{1,0:T(8,128)(2,1)S(1)}, bf16[64,4224]{1,0:T(8,128)(2,1)S(1)}, u32[]{:S(2)}, u32[]{:S(2)}) %collective-permute-start.10) | collective-permute-done | bytes 540704 | tf_op jit(solution)/shard_map/ppermute | solution.py:361
  155.6 5.7 %shard_map.147 = (bf16[2048,128]{1,0:T(8,128)(2,1)}, bf16[2048,128]{1,0:T(8,128)(2,1)}, bf16[128,2048]{1,0:T(8,128)(2,1)}, f32[1,128]{1,0:T(1,128)}, bf16[16,512]{1,0:T(8,128)(2,1)S(1)}) custom-call(s32[2]{0:T(128)S(1)} %pad_add_fusion.sc, bf16[128,4224]{1,0:T(8,128)(2,1)} %copy-done, bf16[128,4224]{1,0:T(8,128)(2,1)} %copy-done.7, ...), custom_call_target="tpu_custom_call" | custom-call | tf_op jit(solution)/shard_map/pallas_call | solution.py:79
  161.4 1.0 shard_map.148
  162.5 12.1 %all_to_all.15.got = bf16[4,160,512]{2,1,0:T(8,128)(2,1)S(1)} all-to-all(bf16[4,160,512]{2,1,0:T(8,128)(2,1)S(1)} %shard_map.148), channel_id=1, replica_groups=mesh['ep_0'=8,'ep_1'=8,'ep_2'=2,'tp'=4] {'tp'}, dimensions={0} | all-to-all | bytes 1310720 | tf_op jit(solution)/shard_map/all_to_all | solution.py:449
  174.6 1.4 shard_map.149
  (36 shorter events, 1.0 us)
Async XLA Ops:
  4.9 17.5 %copy-start.8 = (bf16[1,2048,128]{2,1,0:T(8,128)(2,1)S(1)}, bf16[1,2048,128]{2,1,0:T(8,128)(2,1)}, u32[]{:S(2)}) copy-start(bf16[1,2048,128]{2,1,0:T(8,128)(2,1)} %param.11) | copy-start | bytes 1572868
  4.9 24.1 %copy-start.9 = (bf16[1,2048,128]{2,1,0:T(8,128)(2,1)S(1)}, bf16[1,2048,128]{2,1,0:T(8,128)(2,1)}, u32[]{:S(2)}) copy-start(bf16[1,2048,128]{2,1,0:T(8,128)(2,1)} %param.12) | copy-start | bytes 1572868
  4.9 58.5 %all-to-all-start = ((bf16[128,8,640]{2,1,0:T(8,128)(2,1)}), bf16[128,8,640]{2,1,0:T(8,128)(2,1)S(1)}, u32[]{:S(2)}, u32[]{:S(2)}) async-start(bf16[128,8,640]{2,1,0:T(8,128)(2,1)} %bitcast.31), calls=%async_computation | async-start | bytes 2621440 | tf_op jit(solution)/shard_map/all_to_all | solution.py:385
  22.4 17.6 %collective-permute-start.6 = (bf16[2048,128]{1,0:T(8,128)(2,1)S(1)}, bf16[2048,128]{1,0:T(8,128)(2,1)S(1)}, u32[]{:S(2)}, u32[]{:S(2)}) collective-permute-start(bf16[2048,128]{1,0:T(8,128)(2,1)S(1)} %bitcast.24), channel_id=1, source_target_pairs={{0,3},{1,0},{2,1},{3,2},{4,7},{5,4},{6,5},{7,6},{8,11},{9,8},{10,9... | collective-permute-start | bytes 1572872 | tf_op jit(solution)/shard_map/ppermute | solution.py:361
  27.1 18.0 %collective-permute-start = (bf16[2048,128]{1,0:T(8,128)(2,1)S(1)}, bf16[2048,128]{1,0:T(8,128)(2,1)}, u32[]{:S(2)}, u32[]{:S(2)}) collective-permute-start(bf16[2048,128]{1,0:T(8,128)(2,1)S(1)} %bitcast.25), channel_id=1, source_target_pairs={{0,1},{1,2},{2,3},{3,0},{4,5},{5,6},{6,7},{7,4},{8,9},{9,10},{10,1... | collective-permute-start | bytes 1572872 | tf_op jit(solution)/shard_map/ppermute | solution.py:361
  29.0 27.3 %collective-permute-start.2 = (bf16[2048,128]{1,0:T(8,128)(2,1)S(1)}, bf16[2048,128]{1,0:T(8,128)(2,1)}, u32[]{:S(2)}, u32[]{:S(2)}) collective-permute-start(bf16[2048,128]{1,0:T(8,128)(2,1)S(1)} %bitcast.29), channel_id=1, source_target_pairs={{0,1},{1,2},{2,3},{3,0},{4,5},{5,6},{6,7},{7,4},{8,9},{9,10},{10,1... | collective-permute-start | bytes 1572872 | tf_op jit(solution)/shard_map/ppermute | solution.py:361
  31.7 26.6 %collective-permute-start.4 = (bf16[128,2048]{1,0:T(8,128)(2,1)}, bf16[128,2048]{1,0:T(8,128)(2,1)}, u32[]{:S(2)}, u32[]{:S(2)}) collective-permute-start(bf16[128,2048]{1,0:T(8,128)(2,1)} %bitcast.7.refs_2_.down.down_w), channel_id=1, source_target_pairs={{0,3},{1,0},{2,1},{3,2},{4,7},{5,4},{6,5},{7,6},{8,11},{9,8},{10,9... | collective-permute-start | bytes 1572872 | tf_op jit(solution)/shard_map/ppermute | solution.py:361
  36.1 28.5 %collective-permute-start.7 = (bf16[2048,128]{1,0:T(8,128)(2,1)S(1)}, bf16[2048,128]{1,0:T(8,128)(2,1)}, u32[]{:S(2)}, u32[]{:S(2)}) collective-permute-start(bf16[2048,128]{1,0:T(8,128)(2,1)S(1)} %bitcast.30), channel_id=1, source_target_pairs={{0,3},{1,0},{2,1},{3,2},{4,7},{5,4},{6,5},{7,6},{8,11},{9,8},{10,9... | collective-permute-start | bytes 1572872 | tf_op jit(solution)/shard_map/ppermute | solution.py:361
  40.0 27.5 %copy-start.12 = (bf16[2048,128]{1,0:T(8,128)(2,1)}, bf16[2048,128]{1,0:T(8,128)(2,1)S(1)}, u32[]{:S(2)}) copy-start(bf16[2048,128]{1,0:T(8,128)(2,1)S(1)} %collective-permute-done.6.refs_3_) | copy-start | bytes 1572868
  40.0 27.5 %collective-permute-start.8 = (bf16[128,2048]{1,0:T(8,128)(2,1)}, bf16[128,2048]{1,0:T(8,128)(2,1)}, u32[]{:S(2)}, u32[]{:S(2)}) collective-permute-start(bf16[128,2048]{1,0:T(8,128)(2,1)} %bitcast.7.refs_2_.down.down_w), channel_id=1, source_target_pairs={{0,1},{1,2},{2,3},{3,0},{4,5},{5,6},{6,7},{7,4},{8,9},{9,10},{10,1... | collective-permute-start | bytes 1572872 | tf_op jit(solution)/shard_map/ppermute | solution.py:361
  45.1 33.7 %collective-permute-start.1 = (bf16[2048,128]{1,0:T(8,128)(2,1)}, bf16[2048,128]{1,0:T(8,128)(2,1)}, u32[]{:S(2)}, u32[]{:S(2)}) collective-permute-start(bf16[2048,128]{1,0:T(8,128)(2,1)} %collective-permute-done.refs_6_), channel_id=1, source_target_pairs={{0,1},{1,2},{2,3},{3,0},{4,5},{5,6},{6,7},{7,4},{8,9},{9,10},{10,1... | collective-permute-start | bytes 1572872 | tf_op jit(solution)/shard_map/ppermute | solution.py:361
  56.3 32.6 %collective-permute-start.3 = (bf16[2048,128]{1,0:T(8,128)(2,1)}, bf16[2048,128]{1,0:T(8,128)(2,1)}, u32[]{:S(2)}, u32[]{:S(2)}) collective-permute-start(bf16[2048,128]{1,0:T(8,128)(2,1)} %collective-permute-done.2.refs_7_), channel_id=1, source_target_pairs={{0,1},{1,2},{2,3},{3,0},{4,5},{5,6},{6,7},{7,4},{8,9},{9,10},{10,1... | collective-permute-start | bytes 1572872 | tf_op jit(solution)/shard_map/ppermute | solution.py:361
  58.2 30.7 %collective-permute-start.5 = (bf16[128,2048]{1,0:T(8,128)(2,1)}, bf16[128,2048]{1,0:T(8,128)(2,1)}, u32[]{:S(2)}, u32[]{:S(2)}) collective-permute-start(bf16[128,2048]{1,0:T(8,128)(2,1)} %collective-permute-done.4.refs_5_), channel_id=1, source_target_pairs={{0,3},{1,0},{2,1},{3,2},{4,7},{5,4},{6,5},{7,6},{8,11},{9,8},{10,9... | collective-permute-start | bytes 1572872 | tf_op jit(solution)/shard_map/ppermute | solution.py:361
  64.6 44.3 %copy-start = (bf16[128,4224]{1,0:T(8,128)(2,1)}, bf16[128,4224]{1,0:T(8,128)(2,1)S(1)}, u32[]{:S(2)}) copy-start(bf16[128,4224]{1,0:T(8,128)(2,1)S(1)} %shard_map.143.pair) | copy-start | bytes 3244036
  93.2 68.1 %all-to-all-start.1 = ((bf16[128,8,640]{2,1,0:T(8,128)(2,1)}), bf16[128,8,640]{2,1,0:T(8,128)(2,1)S(1)}, u32[]{:S(2)}, u32[]{:S(2)}) async-start(bf16[128,8,640]{2,1,0:T(8,128)(2,1)} %bitcast.20), calls=%async_computation.1 | async-start | bytes 2621440 | tf_op jit(solution)/shard_map/all_to_all | solution.py:416
  107.0 27.8 %collective-permute-start.11 = (bf16[128,4224]{1,0:T(8,128)(2,1)S(1)}, bf16[128,4224]{1,0:T(8,128)(2,1)S(1)}, u32[]{:S(2)}, u32[]{:S(2)}) collective-permute-start(bf16[128,4224]{1,0:T(8,128)(2,1)S(1)} %shard_map.143.pair), channel_id=1, source_target_pairs={{0,3},{1,0},{2,1},{3,2},{4,7},{5,4},{6,5},{7,6},{8,11},{9,8},{10,9... | collective-permute-start | bytes 3244040 | tf_op jit(solution)/shard_map/ppermute | solution.py:361
  108.9 29.3 %collective-permute-start.9 = (bf16[128,4224]{1,0:T(8,128)(2,1)S(1)}, bf16[128,4224]{1,0:T(8,128)(2,1)S(1)}, u32[]{:S(2)}, u32[]{:S(2)}) collective-permute-start(bf16[128,4224]{1,0:T(8,128)(2,1)S(1)} %shard_map.143.pair), channel_id=1, source_target_pairs={{0,1},{1,2},{2,3},{3,0},{4,5},{5,6},{6,7},{7,4},{8,9},{9,10},{10,1... | collective-permute-start | bytes 3244040 | tf_op jit(solution)/shard_map/ppermute | solution.py:361
  134.7 6.2 %copy-start.6 = (bf16[128,4224]{1,0:T(8,128)(2,1)}, bf16[128,4224]{1,0:T(8,128)(2,1)S(1)}, u32[]{:S(2)}) copy-start(bf16[128,4224]{1,0:T(8,128)(2,1)S(1)} %collective-permute-done.11.pair_3) | copy-start | bytes 3244036
  134.8 15.3 %collective-permute-start.12 = (bf16[64,4224]{1,0:T(8,128)(2,1)S(1)}, bf16[64,4224]{1,0:T(8,128)(2,1)S(1)}, u32[]{:S(2)}, u32[]{:S(2)}) collective-permute-start(bf16[64,4224]{1,0:T(8,128)(2,1)S(1)} %slice.9), channel_id=1, source_target_pairs={{0,3},{1,0},{2,1},{3,2},{4,7},{5,4},{6,5},{7,6},{8,11},{9,8},{10,9... | collective-permute-start | bytes 1622024 | tf_op jit(solution)/shard_map/ppermute | solution.py:361
  138.2 2.7 %copy-start.7 = (bf16[128,4224]{1,0:T(8,128)(2,1)}, bf16[128,4224]{1,0:T(8,128)(2,1)S(1)}, u32[]{:S(2)}) copy-start(bf16[128,4224]{1,0:T(8,128)(2,1)S(1)} %collective-permute-done.9.pair_1) | copy-start | bytes 3244036
  138.3 16.5 %collective-permute-start.10 = (bf16[64,4224]{1,0:T(8,128)(2,1)S(1)}, bf16[64,4224]{1,0:T(8,128)(2,1)S(1)}, u32[]{:S(2)}, u32[]{:S(2)}) collective-permute-start(bf16[64,4224]{1,0:T(8,128)(2,1)S(1)} %slice.8), channel_id=1, source_target_pairs={{0,1},{1,2},{2,3},{3,0},{4,5},{5,6},{6,7},{7,4},{8,9},{9,10},{10,1... | collective-permute-start | bytes 1622024 | tf_op jit(solution)/shard_map/ppermute | solution.py:361
  150.1 4.7 %copy-start.10 = (bf16[64,4224]{1,0:T(8,128)(2,1)}, bf16[64,4224]{1,0:T(8,128)(2,1)S(1)}, u32[]{:S(2)}) copy-start(bf16[64,4224]{1,0:T(8,128)(2,1)S(1)} %collective-permute-done.12.bottom) | copy-start | bytes 1622020
  154.8 0.8 copy-start.11
  155.6 5.7 %copy-start.2 = (bf16[128,128]{1,0:T(8,128)(2,1)S(1)}, bf16[128,128]{1,0:T(8,128)(2,1)}, u32[]{:S(2)}) copy-start(bf16[128,128]{1,0:T(8,128)(2,1)} %get-tuple-element.31.hit0) | copy-start | bytes 98308
  155.6 5.7 %copy-start.3 = (bf16[128,128]{1,0:T(8,128)(2,1)S(1)}, bf16[128,128]{1,0:T(8,128)(2,1)}, u32[]{:S(2)}) copy-start(bf16[128,128]{1,0:T(8,128)(2,1)} %get-tuple-element.32.hit1) | copy-start | bytes 98308
  161.4 13.2 %copy-start.1 = (bf16[2048,128]{1,0:T(8,128)(2,1)S(1)}, bf16[2048,128]{1,0:T(8,128)(2,1)}, u32[]{:S(2)}) copy-start(bf16[2048,128]{1,0:T(8,128)(2,1)} %router.3) | copy-start | bytes 1572868
  161.4 13.2 %copy-start.4 = (f32[8,128]{1,0:T(8,128)S(1)}, f32[8,128]{1,0:T(8,128)}, u32[]{:S(2)}) copy-start(f32[8,128]{1,0:T(8,128)} %get-tuple-element.37.stats) | copy-start | bytes 12292
  161.4 13.2 %copy-start.5 = (s32[128,2]{0,1:T(2,128)S(1)}, s32[128,2]{0,1:T(2,128)}, u32[]{:S(2)}) copy-start(s32[128,2]{0,1:T(2,128)} %param.9) | copy-start | bytes 3076

commit v7 on v6

--- a/solution.py
+++ b/solution.py
@@ -110,7 +110,7 @@
     experts = iota((EXPERTS, TOK), 0)
     picked = [(experts == routing[k : k + 1, :]) for k in range(2)]
     both = (picked[0] | picked[1]).astype(F32)
-    logits = dot(router[...], tok[...], 0, 1)
+    logits = dot(tok[...], router[...]).T
     s = [
         jax.nn.sigmoid(jnp.sum(jnp.where(m, logits, 0.0), axis=0, keepdims=True)) for m in picked
     ]
@@ -161,8 +161,9 @@
             pair[:, 2 * D :] = part[:, 2 * CH :]
 
 
-def hidden_grads(pair, both, down):
-    pre = dot(pair[:, 0:D], both)
+def hidden_grads(pair, both, down, pre=None):
+    if pre is None:
+        pre = dot(pair[:, 0:D], both)
     back_raw = dot(pair[:, D : 2 * D], down, 1, 1)
     about = pair[:, 2 * D :].astype(F32)
     pre_gate = pre[:, 0:FQ]
@@ -218,11 +219,24 @@
         out[:, 2 * FQ :] = scaled
 
 
-def emit_kernel(sc, pair, gate, up, down, back, gg_in, send, scratch):
+def emit_kernel(
+    sc, pair, gate, up, down, back, gg_in, send, scratch, held, held_down, sems
+):
+    copies = [
+        pltpu.make_async_copy(x, t, sems.at[c])
+        for c, (x, t) in enumerate(
+            ((gate, held.at[:, 0:FQ]), (up, held.at[:, FQ : 2 * FQ]), (down, held_down))
+        )
+    ]
+    for c in copies:
+        c.start()
     about = pair[:, 2 * D :].astype(F32)
-    both = jnp.concatenate([gate[...], up[...]], axis=1)
-    g_in, _, gg = hidden_grads(pair, both, down[...])
-    term = back[...] + dot(g_in, both, 1, 1)
+    for c in copies[0:2]:
+        c.wait()
+    pre = dot(pair[:, 0:D], held[...])
+    copies[2].wait()
+    g_in, _, gg = hidden_grads(pair, held[...], held_down[...], pre)
+    term = back[...] + dot(g_in, held[...], 1, 1)
     gg = gg + gg_in[:, 0:1]
     own = (about[:, 3:4] + about[:, 4:5] + about[:, 5:6]) * gg
     other = (about[:, 6:7] + about[:, 7:8] + about[:, 8:9]) * gg
@@ -363,12 +377,12 @@
     gate_1 = shift(gate_w, 1)
     down_3 = shift(down_w, 3)
     up_1 = shift(up_w, 1)
+    gate_2 = shift(gate_1, 1)
     up_3 = shift(up_w, 3)
-    gate_2 = shift(gate_1, 1)
+    down_1 = shift(down_w, 1)
     gate_3 = shift(gate_w, 3)
-    down_1 = shift(down_w, 1)
+    up_2 = shift(up_1, 1)
     down_2 = shift(down_3, 3)
-    up_2 = shift(up_1, 1)
 
     send, hit0, hit1, stats = call(
         dispatch_kernel,
@@ -409,9 +423,14 @@
     (send_back,) = call(
         emit_kernel,
         sc,
-        (pair, *(whole(far(x)) for x in (gate_2, up_2, down_2)), back, gg),
+        (pair, *((far(x), in_place) for x in (gate_2, up_2, down_2)), back, gg),
         (hbm((SENT, 2 * CH + 128), BF16),),
-        (pltpu.VMEM((CH // 128, SENT, 128), F32),),
+        (
+            pltpu.VMEM((CH // 128, SENT, 128), F32),
+            pltpu.VMEM((D, 2 * FQ), BF16),
+            pltpu.VMEM((FQ, D), BF16),
+            pltpu.SemaphoreType.DMA((3,)),
+        ),
     )
     home = lax.all_to_all(send_back.reshape(EXPERTS, 8, 2 * CH + 128), EP, 0, 0, tiled=True)
     home = home.reshape(SENT, 2 * CH + 128)

time: 177 us -> 177 us (level)
  no operation moved by 1% of the time
where the time goes in v7:
time: 177 us; the launch traced here: 176 us
  starting transfers between devices  72.1 us (41%)
  waiting for transfers between devices  63.7 us (36%)
  Pallas kernels  26.2 us (15%)
  blocking collectives  12.1 us (7%)
    ppermute x13, waiting for transfers between devices, shift(): return lax.ppermute(x, 'tp', [(a, (a + d) % TP) for a in range(TP)])  63.7 us
    ppermute x13, starting transfers between devices, shift(): return lax.ppermute(x, 'tp', [(a, (a + d) % TP) for a in range(TP)])  40.8 us
    pallas_call x8, Pallas kernels, call(): pl.pallas_call(kernel, grid_spec=pltpu.PrefetchScalarGridSpec(num_scalar_...  26.2 us
    all_to_all x1, starting transfers between devices, layer(): lax.all_to_all(send.reshape(EXPERTS, 8, 2 * CH + 128), EP, 0, 0, tiled=True)  17.5 us
    all_to_all x1, starting transfers between devices, layer(): lax.all_to_all(send_back.reshape(EXPERTS, 8, 2 * CH + 128), EP, 0, 0, til...  13.7 us
    all_to_all x1, blocking collectives, layer(): parts = lax.all_to_all(parts, 'tp', 0, 0, tiled=True)  12.1 us
  transfers between devices with their start and end apart: 15, of which 8 were waited for; matrix products, arithmetic and copies ran while one was open for 0% of the time, Pallas kernels for 9%

profile of v7, /device:TPU:8, one launch (start us, length us, event | category | flops | bytes accessed | tf_op | source)
XLA Modules:
  0.0 176.1 jit_solution(15495476685407343899)
XLA Ops:
  0.7 4.0 %shard_map.142 = (bf16[1024,640]{1,0:T(8,128)(2,1)}, bf16[128,128]{1,0:T(8,128)(2,1)}, bf16[128,128]{1,0:T(8,128)(2,1)}, f32[8,128]{1,0:T(8,128)}) custom-call(s32[2]{0:T(128)S(1)} %pad_add_fusion.sc, bf16[128,2048]{1,0:T(8,128)(2,1)} %tok.1, bf16[128,2048]{1,0:T(8,128)(2,1)} %cot.1, s32[2,128]{1,0:T(2,128)} %bitcast.18, bf16[2048,128]{1,0:T(8,128)(2,1)} %router.3), custom_call_target="tpu_custom_call" | custom-call | tf_op jit(solution)/shard_map/pallas_call | solution.py:79
  4.7 17.5 %all-to-all-start = ((bf16[128,8,640]{2,1,0:T(8,128)(2,1)}), bf16[128,8,640]{2,1,0:T(8,128)(2,1)S(1)}, u32[]{:S(2)}, u32[]{:S(2)}) async-start(bf16[128,8,640]{2,1,0:T(8,128)(2,1)} %bitcast.31), calls=%async_computation | async-start | bytes 2621440 | tf_op jit(solution)/shard_map/all_to_all | solution.py:399
  22.2 4.7 %collective-permute-start.6 = (bf16[2048,128]{1,0:T(8,128)(2,1)S(1)}, bf16[2048,128]{1,0:T(8,128)(2,1)S(1)}, u32[]{:S(2)}, u32[]{:S(2)}) collective-permute-start(bf16[2048,128]{1,0:T(8,128)(2,1)S(1)} %bitcast.24), channel_id=1, source_target_pairs={{0,3},{1,0},{2,1},{3,2},{4,7},{5,4},{6,5},{7,6},{8,11},{9,8},{10,9... | collective-permute-start | bytes 1572872 | tf_op jit(solution)/shard_map/ppermute | solution.py:375
  26.9 1.9 %collective-permute-start = (bf16[2048,128]{1,0:T(8,128)(2,1)S(1)}, bf16[2048,128]{1,0:T(8,128)(2,1)}, u32[]{:S(2)}, u32[]{:S(2)}) collective-permute-start(bf16[2048,128]{1,0:T(8,128)(2,1)S(1)} %bitcast.25), channel_id=1, source_target_pairs={{0,1},{1,2},{2,3},{3,0},{4,5},{5,6},{6,7},{7,4},{8,9},{9,10},{10,1... | collective-permute-start | bytes 1572872 | tf_op jit(solution)/shard_map/ppermute | solution.py:375
  28.8 2.7 %collective-permute-start.2 = (bf16[2048,128]{1,0:T(8,128)(2,1)S(1)}, bf16[2048,128]{1,0:T(8,128)(2,1)}, u32[]{:S(2)}, u32[]{:S(2)}) collective-permute-start(bf16[2048,128]{1,0:T(8,128)(2,1)S(1)} %bitcast.29), channel_id=1, source_target_pairs={{0,1},{1,2},{2,3},{3,0},{4,5},{5,6},{6,7},{7,4},{8,9},{9,10},{10,1... | collective-permute-start | bytes 1572872 | tf_op jit(solution)/shard_map/ppermute | solution.py:375
  31.5 4.4 %collective-permute-start.4 = (bf16[128,2048]{1,0:T(8,128)(2,1)}, bf16[128,2048]{1,0:T(8,128)(2,1)}, u32[]{:S(2)}, u32[]{:S(2)}) collective-permute-start(bf16[128,2048]{1,0:T(8,128)(2,1)} %bitcast.7.refs_2_.down.down_w), channel_id=1, source_target_pairs={{0,3},{1,0},{2,1},{3,2},{4,7},{5,4},{6,5},{7,6},{8,11},{9,8},{10,9... | collective-permute-start | bytes 1572872 | tf_op jit(solution)/shard_map/ppermute | solution.py:375
  35.9 3.9 %collective-permute-start.7 = (bf16[2048,128]{1,0:T(8,128)(2,1)S(1)}, bf16[2048,128]{1,0:T(8,128)(2,1)}, u32[]{:S(2)}, u32[]{:S(2)}) collective-permute-start(bf16[2048,128]{1,0:T(8,128)(2,1)S(1)} %bitcast.30), channel_id=1, source_target_pairs={{0,3},{1,0},{2,1},{3,2},{4,7},{5,4},{6,5},{7,6},{8,11},{9,8},{10,9... | collective-permute-start | bytes 1572872 | tf_op jit(solution)/shard_map/ppermute | solution.py:375
  39.9 2.4 %collective-permute-start.8 = (bf16[128,2048]{1,0:T(8,128)(2,1)}, bf16[128,2048]{1,0:T(8,128)(2,1)}, u32[]{:S(2)}, u32[]{:S(2)}) collective-permute-start(bf16[128,2048]{1,0:T(8,128)(2,1)} %bitcast.7.refs_2_.down.down_w), channel_id=1, source_target_pairs={{0,1},{1,2},{2,3},{3,0},{4,5},{5,6},{6,7},{7,4},{8,9},{9,10},{10,1... | collective-permute-start | bytes 1572872 | tf_op jit(solution)/shard_map/ppermute | solution.py:375
  42.3 2.6 %collective-permute-done.refs_6_ = bf16[2048,128]{1,0:T(8,128)(2,1)} collective-permute-done((bf16[2048,128]{1,0:T(8,128)(2,1)S(1)}, bf16[2048,128]{1,0:T(8,128)(2,1)}, u32[]{:S(2)}, u32[]{:S(2)}) %collective-permute-start) | collective-permute-done | bytes 524320 | tf_op jit(solution)/shard_map/ppermute | solution.py:375
  44.9 1.9 %collective-permute-start.1 = (bf16[2048,128]{1,0:T(8,128)(2,1)}, bf16[2048,128]{1,0:T(8,128)(2,1)}, u32[]{:S(2)}, u32[]{:S(2)}) collective-permute-start(bf16[2048,128]{1,0:T(8,128)(2,1)} %collective-permute-done.refs_6_), channel_id=1, source_target_pairs={{0,1},{1,2},{2,3},{3,0},{4,5},{5,6},{6,7},{7,4},{8,9},{9,10},{10,1... | collective-permute-start | bytes 1572872 | tf_op jit(solution)/shard_map/ppermute | solution.py:375
  46.8 9.3 %collective-permute-done.2.refs_7_ = bf16[2048,128]{1,0:T(8,128)(2,1)} collective-permute-done((bf16[2048,128]{1,0:T(8,128)(2,1)S(1)}, bf16[2048,128]{1,0:T(8,128)(2,1)}, u32[]{:S(2)}, u32[]{:S(2)}) %collective-permute-start.2) | collective-permute-done | bytes 524320 | tf_op jit(solution)/shard_map/ppermute | solution.py:375
  56.1 1.9 %collective-permute-start.3 = (bf16[2048,128]{1,0:T(8,128)(2,1)}, bf16[2048,128]{1,0:T(8,128)(2,1)}, u32[]{:S(2)}, u32[]{:S(2)}) collective-permute-start(bf16[2048,128]{1,0:T(8,128)(2,1)} %collective-permute-done.2.refs_7_), channel_id=1, source_target_pairs={{0,1},{1,2},{2,3},{3,0},{4,5},{5,6},{6,7},{7,4},{8,9},{9,10},{10,1... | collective-permute-start | bytes 1572872 | tf_op jit(solution)/shard_map/ppermute | solution.py:375
  58.1 5.1 %collective-permute-start.5 = (bf16[128,2048]{1,0:T(8,128)(2,1)}, bf16[128,2048]{1,0:T(8,128)(2,1)}, u32[]{:S(2)}, u32[]{:S(2)}) collective-permute-start(bf16[128,2048]{1,0:T(8,128)(2,1)} %collective-permute-done.4.refs_5_), channel_id=1, source_target_pairs={{0,3},{1,0},{2,1},{3,2},{4,7},{5,4},{6,5},{7,6},{8,11},{9,8},{10,9... | collective-permute-start | bytes 1572872 | tf_op jit(solution)/shard_map/ppermute | solution.py:375
  63.2 1.2 shard_map.143.pair
  64.4 2.9 %collective-permute-done.8.refs_8_ = bf16[128,2048]{1,0:T(8,128)(2,1)} collective-permute-done((bf16[128,2048]{1,0:T(8,128)(2,1)}, bf16[128,2048]{1,0:T(8,128)(2,1)}, u32[]{:S(2)}, u32[]{:S(2)}) %collective-permute-start.8) | collective-permute-done | bytes 524320 | tf_op jit(solution)/shard_map/ppermute | solution.py:375
  67.4 4.3 %shard_map.144 = (bf16[128,384]{1,0:T(8,128)(2,1)}, f32[128,2048]{1,0:T(8,128)S(1)}, f32[128,128]{1,0:T(8,128)S(1)}) custom-call(s32[2]{0:T(128)S(1)} %pad_add_fusion.sc, bf16[128,4224]{1,0:T(8,128)(2,1)S(1)} %shard_map.143.pair, bf16[2048,128]{1,0:T(8,128)(2,1)} %bitcast.21, bf16[2048,128]{1,0:T(8,128)(2,1)} %bitcast.26, ...), custom_call_target="tpu_custom_call" | custom-call | tf_op jit(solution)/shard_map/pallas_call | solution.py:79
  71.7 6.9 %collective-permute-done.1.gate = bf16[2048,128]{1,0:T(8,128)(2,1)} collective-permute-done((bf16[2048,128]{1,0:T(8,128)(2,1)}, bf16[2048,128]{1,0:T(8,128)(2,1)}, u32[]{:S(2)}, u32[]{:S(2)}) %collective-permute-start.1) | collective-permute-done | bytes 524320 | tf_op jit(solution)/shard_map/ppermute | solution.py:375
  78.6 10.1 %collective-permute-done.3.up = bf16[2048,128]{1,0:T(8,128)(2,1)} collective-permute-done((bf16[2048,128]{1,0:T(8,128)(2,1)}, bf16[2048,128]{1,0:T(8,128)(2,1)}, u32[]{:S(2)}, u32[]{:S(2)}) %collective-permute-start.3) | collective-permute-done | bytes 524320 | tf_op jit(solution)/shard_map/ppermute | solution.py:375
  88.7 4.6 %shard_map.145 = bf16[1024,640]{1,0:T(8,128)(2,1)} custom-call(s32[2]{0:T(128)S(1)} %pad_add_fusion.sc, bf16[128,4224]{1,0:T(8,128)(2,1)S(1)} %shard_map.143.pair, bf16[2048,128]{1,0:T(8,128)(2,1)} %collective-permute-done.1.gate, bf16[2048,128]{1,0:T(8,128)(2,1)} %collective-permute-done.3.up, bf16[128,2048]{1,0:T(8,128)(2,1)} %collective-permute-done.5.down, ...), custom_call_target="tpu_custom_call" | custom-call | tf_op jit(solution)/shard_map/pallas_call | solution.py:79
  93.3 13.7 %all-to-all-start.1 = ((bf16[128,8,640]{2,1,0:T(8,128)(2,1)}), bf16[128,8,640]{2,1,0:T(8,128)(2,1)S(1)}, u32[]{:S(2)}, u32[]{:S(2)}) async-start(bf16[128,8,640]{2,1,0:T(8,128)(2,1)} %bitcast.20), calls=%async_computation.1 | async-start | bytes 2621440 | tf_op jit(solution)/shard_map/all_to_all | solution.py:435
  107.0 1.9 %collective-permute-start.11 = (bf16[128,4224]{1,0:T(8,128)(2,1)S(1)}, bf16[128,4224]{1,0:T(8,128)(2,1)S(1)}, u32[]{:S(2)}, u32[]{:S(2)}) collective-permute-start(bf16[128,4224]{1,0:T(8,128)(2,1)S(1)} %shard_map.143.pair), channel_id=1, source_target_pairs={{0,3},{1,0},{2,1},{3,2},{4,7},{5,4},{6,5},{7,6},{8,11},{9,8},{10,9... | collective-permute-start | bytes 3244040 | tf_op jit(solution)/shard_map/ppermute | solution.py:375
  109.0 3.9 %collective-permute-start.9 = (bf16[128,4224]{1,0:T(8,128)(2,1)S(1)}, bf16[128,4224]{1,0:T(8,128)(2,1)S(1)}, u32[]{:S(2)}, u32[]{:S(2)}) collective-permute-start(bf16[128,4224]{1,0:T(8,128)(2,1)S(1)} %shard_map.143.pair), channel_id=1, source_target_pairs={{0,1},{1,2},{2,3},{3,0},{4,5},{5,6},{6,7},{7,4},{8,9},{9,10},{10,1... | collective-permute-start | bytes 3244040 | tf_op jit(solution)/shard_map/ppermute | solution.py:375
  112.9 21.9 %collective-permute-done.11.pair_3 = bf16[128,4224]{1,0:T(8,128)(2,1)S(1)} collective-permute-done((bf16[128,4224]{1,0:T(8,128)(2,1)S(1)}, bf16[128,4224]{1,0:T(8,128)(2,1)S(1)}, u32[]{:S(2)}, u32[]{:S(2)}) %collective-permute-start.11) | collective-permute-done | bytes 1081376 | tf_op jit(solution)/shard_map/ppermute | solution.py:375
  134.9 3.4 %collective-permute-start.12 = (bf16[64,4224]{1,0:T(8,128)(2,1)S(1)}, bf16[64,4224]{1,0:T(8,128)(2,1)S(1)}, u32[]{:S(2)}, u32[]{:S(2)}) collective-permute-start(bf16[64,4224]{1,0:T(8,128)(2,1)S(1)} %slice.9), channel_id=1, source_target_pairs={{0,3},{1,0},{2,1},{3,2},{4,7},{5,4},{6,5},{7,6},{8,11},{9,8},{10,9... | collective-permute-start | bytes 1622024 | tf_op jit(solution)/shard_map/ppermute | solution.py:375
  138.3 2.6 %collective-permute-start.10 = (bf16[64,4224]{1,0:T(8,128)(2,1)S(1)}, bf16[64,4224]{1,0:T(8,128)(2,1)S(1)}, u32[]{:S(2)}, u32[]{:S(2)}) collective-permute-start(bf16[64,4224]{1,0:T(8,128)(2,1)S(1)} %slice.8), channel_id=1, source_target_pairs={{0,1},{1,2},{2,3},{3,0},{4,5},{5,6},{6,7},{7,4},{8,9},{9,10},{10,1... | collective-permute-start | bytes 1622024 | tf_op jit(solution)/shard_map/ppermute | solution.py:375
  141.0 3.9 %shard_map.146 = (bf16[128,384]{1,0:T(8,128)(2,1)}, bf16[128,384]{1,0:T(8,128)(2,1)}) custom-call(s32[2]{0:T(128)S(1)} %pad_add_fusion.sc, bf16[128,4224]{1,0:T(8,128)(2,1)} %copy-done.7, bf16[128,4224]{1,0:T(8,128)(2,1)} %copy-done.6, bf16[2048,128]{1,0:T(8,128)(2,1)} %bitcast.22, bf16[2048,128]{1,0:T(8,128)(2,1)} %bitcast.27, ...), custom_call_target="tpu_custom_call" | custom-call | tf_op jit(solution)/shard_map/pallas_call | solution.py:79
  144.9 5.3 %collective-permute-done.12.bottom = bf16[64,4224]{1,0:T(8,128)(2,1)S(1)} collective-permute-done((bf16[64,4224]{1,0:T(8,128)(2,1)S(1)}, bf16[64,4224]{1,0:T(8,128)(2,1)S(1)}, u32[]{:S(2)}, u32[]{:S(2)}) %collective-permute-start.12) | collective-permute-done | bytes 540704 | tf_op jit(solution)/shard_map/ppermute | solution.py:375
  150.2 4.7 %collective-permute-done.10.top = bf16[64,4224]{1,0:T(8,128)(2,1)S(1)} collective-permute-done((bf16[64,4224]{1,0:T(8,128)(2,1)S(1)}, bf16[64,4224]{1,0:T(8,128)(2,1)S(1)}, u32[]{:S(2)}, u32[]{:S(2)}) %collective-permute-start.10) | collective-permute-done | bytes 540704 | tf_op jit(solution)/shard_map/ppermute | solution.py:375
  155.7 5.7 %shard_map.147 = (bf16[2048,128]{1,0:T(8,128)(2,1)}, bf16[2048,128]{1,0:T(8,128)(2,1)}, bf16[128,2048]{1,0:T(8,128)(2,1)}, f32[1,128]{1,0:T(1,128)}, bf16[16,512]{1,0:T(8,128)(2,1)S(1)}) custom-call(s32[2]{0:T(128)S(1)} %pad_add_fusion.sc, bf16[128,4224]{1,0:T(8,128)(2,1)} %copy-done, bf16[128,4224]{1,0:T(8,128)(2,1)} %copy-done.7, ...), custom_call_target="tpu_custom_call" | custom-call | tf_op jit(solution)/shard_map/pallas_call | solution.py:79
  161.5 1.0 shard_map.148
  162.5 12.1 %all_to_all.15.got = bf16[4,160,512]{2,1,0:T(8,128)(2,1)S(1)} all-to-all(bf16[4,160,512]{2,1,0:T(8,128)(2,1)S(1)} %shard_map.148), channel_id=1, replica_groups=mesh['ep_0'=8,'ep_1'=8,'ep_2'=2,'tp'=4] {'tp'}, dimensions={0} | all-to-all | bytes 1310720 | tf_op jit(solution)/shard_map/all_to_all | solution.py:468
  174.7 1.4 shard_map.149
  (36 shorter events, 1.0 us)
Async XLA Ops:
  4.7 17.5 %copy-start.8 = (bf16[1,2048,128]{2,1,0:T(8,128)(2,1)S(1)}, bf16[1,2048,128]{2,1,0:T(8,128)(2,1)}, u32[]{:S(2)}) copy-start(bf16[1,2048,128]{2,1,0:T(8,128)(2,1)} %param.11) | copy-start | bytes 1572868
  4.7 24.1 %copy-start.9 = (bf16[1,2048,128]{2,1,0:T(8,128)(2,1)S(1)}, bf16[1,2048,128]{2,1,0:T(8,128)(2,1)}, u32[]{:S(2)}) copy-start(bf16[1,2048,128]{2,1,0:T(8,128)(2,1)} %param.12) | copy-start | bytes 1572868
  4.7 58.5 %all-to-all-start = ((bf16[128,8,640]{2,1,0:T(8,128)(2,1)}), bf16[128,8,640]{2,1,0:T(8,128)(2,1)S(1)}, u32[]{:S(2)}, u32[]{:S(2)}) async-start(bf16[128,8,640]{2,1,0:T(8,128)(2,1)} %bitcast.31), calls=%async_computation | async-start | bytes 2621440 | tf_op jit(solution)/shard_map/all_to_all | solution.py:399
  22.2 17.6 %collective-permute-start.6 = (bf16[2048,128]{1,0:T(8,128)(2,1)S(1)}, bf16[2048,128]{1,0:T(8,128)(2,1)S(1)}, u32[]{:S(2)}, u32[]{:S(2)}) collective-permute-start(bf16[2048,128]{1,0:T(8,128)(2,1)S(1)} %bitcast.24), channel_id=1, source_target_pairs={{0,3},{1,0},{2,1},{3,2},{4,7},{5,4},{6,5},{7,6},{8,11},{9,8},{10,9... | collective-permute-start | bytes 1572872 | tf_op jit(solution)/shard_map/ppermute | solution.py:375
  26.9 18.0 %collective-permute-start = (bf16[2048,128]{1,0:T(8,128)(2,1)S(1)}, bf16[2048,128]{1,0:T(8,128)(2,1)}, u32[]{:S(2)}, u32[]{:S(2)}) collective-permute-start(bf16[2048,128]{1,0:T(8,128)(2,1)S(1)} %bitcast.25), channel_id=1, source_target_pairs={{0,1},{1,2},{2,3},{3,0},{4,5},{5,6},{6,7},{7,4},{8,9},{9,10},{10,1... | collective-permute-start | bytes 1572872 | tf_op jit(solution)/shard_map/ppermute | solution.py:375
  28.8 27.3 %collective-permute-start.2 = (bf16[2048,128]{1,0:T(8,128)(2,1)S(1)}, bf16[2048,128]{1,0:T(8,128)(2,1)}, u32[]{:S(2)}, u32[]{:S(2)}) collective-permute-start(bf16[2048,128]{1,0:T(8,128)(2,1)S(1)} %bitcast.29), channel_id=1, source_target_pairs={{0,1},{1,2},{2,3},{3,0},{4,5},{5,6},{6,7},{7,4},{8,9},{9,10},{10,1... | collective-permute-start | bytes 1572872 | tf_op jit(solution)/shard_map/ppermute | solution.py:375
  31.5 26.6 %collective-permute-start.4 = (bf16[128,2048]{1,0:T(8,128)(2,1)}, bf16[128,2048]{1,0:T(8,128)(2,1)}, u32[]{:S(2)}, u32[]{:S(2)}) collective-permute-start(bf16[128,2048]{1,0:T(8,128)(2,1)} %bitcast.7.refs_2_.down.down_w), channel_id=1, source_target_pairs={{0,3},{1,0},{2,1},{3,2},{4,7},{5,4},{6,5},{7,6},{8,11},{9,8},{10,9... | collective-permute-start | bytes 1572872 | tf_op jit(solution)/shard_map/ppermute | solution.py:375
  35.9 28.5 %collective-permute-start.7 = (bf16[2048,128]{1,0:T(8,128)(2,1)S(1)}, bf16[2048,128]{1,0:T(8,128)(2,1)}, u32[]{:S(2)}, u32[]{:S(2)}) collective-permute-start(bf16[2048,128]{1,0:T(8,128)(2,1)S(1)} %bitcast.30), channel_id=1, source_target_pairs={{0,3},{1,0},{2,1},{3,2},{4,7},{5,4},{6,5},{7,6},{8,11},{9,8},{10,9... | collective-permute-start | bytes 1572872 | tf_op jit(solution)/shard_map/ppermute | solution.py:375
  39.9 27.5 %copy-start.12 = (bf16[2048,128]{1,0:T(8,128)(2,1)}, bf16[2048,128]{1,0:T(8,128)(2,1)S(1)}, u32[]{:S(2)}) copy-start(bf16[2048,128]{1,0:T(8,128)(2,1)S(1)} %collective-permute-done.6.refs_3_) | copy-start | bytes 1572868
  39.9 27.5 %collective-permute-start.8 = (bf16[128,2048]{1,0:T(8,128)(2,1)}, bf16[128,2048]{1,0:T(8,128)(2,1)}, u32[]{:S(2)}, u32[]{:S(2)}) collective-permute-start(bf16[128,2048]{1,0:T(8,128)(2,1)} %bitcast.7.refs_2_.down.down_w), channel_id=1, source_target_pairs={{0,1},{1,2},{2,3},{3,0},{4,5},{5,6},{6,7},{7,4},{8,9},{9,10},{10,1... | collective-permute-start | bytes 1572872 | tf_op jit(solution)/shard_map/ppermute | solution.py:375
  44.9 33.7 %collective-permute-start.1 = (bf16[2048,128]{1,0:T(8,128)(2,1)}, bf16[2048,128]{1,0:T(8,128)(2,1)}, u32[]{:S(2)}, u32[]{:S(2)}) collective-permute-start(bf16[2048,128]{1,0:T(8,128)(2,1)} %collective-permute-done.refs_6_), channel_id=1, source_target_pairs={{0,1},{1,2},{2,3},{3,0},{4,5},{5,6},{6,7},{7,4},{8,9},{9,10},{10,1... | collective-permute-start | bytes 1572872 | tf_op jit(solution)/shard_map/ppermute | solution.py:375
  56.1 32.6 %collective-permute-start.3 = (bf16[2048,128]{1,0:T(8,128)(2,1)}, bf16[2048,128]{1,0:T(8,128)(2,1)}, u32[]{:S(2)}, u32[]{:S(2)}) collective-permute-start(bf16[2048,128]{1,0:T(8,128)(2,1)} %collective-permute-done.2.refs_7_), channel_id=1, source_target_pairs={{0,1},{1,2},{2,3},{3,0},{4,5},{5,6},{6,7},{7,4},{8,9},{9,10},{10,1... | collective-permute-start | bytes 1572872 | tf_op jit(solution)/shard_map/ppermute | solution.py:375
  58.1 30.7 %collective-permute-start.5 = (bf16[128,2048]{1,0:T(8,128)(2,1)}, bf16[128,2048]{1,0:T(8,128)(2,1)}, u32[]{:S(2)}, u32[]{:S(2)}) collective-permute-start(bf16[128,2048]{1,0:T(8,128)(2,1)} %collective-permute-done.4.refs_5_), channel_id=1, source_target_pairs={{0,3},{1,0},{2,1},{3,2},{4,7},{5,4},{6,5},{7,6},{8,11},{9,8},{10,9... | collective-permute-start | bytes 1572872 | tf_op jit(solution)/shard_map/ppermute | solution.py:375
  64.4 44.5 %copy-start = (bf16[128,4224]{1,0:T(8,128)(2,1)}, bf16[128,4224]{1,0:T(8,128)(2,1)S(1)}, u32[]{:S(2)}) copy-start(bf16[128,4224]{1,0:T(8,128)(2,1)S(1)} %shard_map.143.pair) | copy-start | bytes 3244036
  93.3 68.1 %all-to-all-start.1 = ((bf16[128,8,640]{2,1,0:T(8,128)(2,1)}), bf16[128,8,640]{2,1,0:T(8,128)(2,1)S(1)}, u32[]{:S(2)}, u32[]{:S(2)}) async-start(bf16[128,8,640]{2,1,0:T(8,128)(2,1)} %bitcast.20), calls=%async_computation.1 | async-start | bytes 2621440 | tf_op jit(solution)/shard_map/all_to_all | solution.py:435
  107.0 27.8 %collective-permute-start.11 = (bf16[128,4224]{1,0:T(8,128)(2,1)S(1)}, bf16[128,4224]{1,0:T(8,128)(2,1)S(1)}, u32[]{:S(2)}, u32[]{:S(2)}) collective-permute-start(bf16[128,4224]{1,0:T(8,128)(2,1)S(1)} %shard_map.143.pair), channel_id=1, source_target_pairs={{0,3},{1,0},{2,1},{3,2},{4,7},{5,4},{6,5},{7,6},{8,11},{9,8},{10,9... | collective-permute-start | bytes 3244040 | tf_op jit(solution)/shard_map/ppermute | solution.py:375
  109.0 29.3 %collective-permute-start.9 = (bf16[128,4224]{1,0:T(8,128)(2,1)S(1)}, bf16[128,4224]{1,0:T(8,128)(2,1)S(1)}, u32[]{:S(2)}, u32[]{:S(2)}) collective-permute-start(bf16[128,4224]{1,0:T(8,128)(2,1)S(1)} %shard_map.143.pair), channel_id=1, source_target_pairs={{0,1},{1,2},{2,3},{3,0},{4,5},{5,6},{6,7},{7,4},{8,9},{9,10},{10,1... | collective-permute-start | bytes 3244040 | tf_op jit(solution)/shard_map/ppermute | solution.py:375
  134.8 6.2 %copy-start.6 = (bf16[128,4224]{1,0:T(8,128)(2,1)}, bf16[128,4224]{1,0:T(8,128)(2,1)S(1)}, u32[]{:S(2)}) copy-start(bf16[128,4224]{1,0:T(8,128)(2,1)S(1)} %collective-permute-done.11.pair_3) | copy-start | bytes 3244036
  134.9 15.3 %collective-permute-start.12 = (bf16[64,4224]{1,0:T(8,128)(2,1)S(1)}, bf16[64,4224]{1,0:T(8,128)(2,1)S(1)}, u32[]{:S(2)}, u32[]{:S(2)}) collective-permute-start(bf16[64,4224]{1,0:T(8,128)(2,1)S(1)} %slice.9), channel_id=1, source_target_pairs={{0,3},{1,0},{2,1},{3,2},{4,7},{5,4},{6,5},{7,6},{8,11},{9,8},{10,9... | collective-permute-start | bytes 1622024 | tf_op jit(solution)/shard_map/ppermute | solution.py:375
  138.3 2.7 %copy-start.7 = (bf16[128,4224]{1,0:T(8,128)(2,1)}, bf16[128,4224]{1,0:T(8,128)(2,1)S(1)}, u32[]{:S(2)}) copy-start(bf16[128,4224]{1,0:T(8,128)(2,1)S(1)} %collective-permute-done.9.pair_1) | copy-start | bytes 3244036
  138.3 16.5 %collective-permute-start.10 = (bf16[64,4224]{1,0:T(8,128)(2,1)S(1)}, bf16[64,4224]{1,0:T(8,128)(2,1)S(1)}, u32[]{:S(2)}, u32[]{:S(2)}) collective-permute-start(bf16[64,4224]{1,0:T(8,128)(2,1)S(1)} %slice.8), channel_id=1, source_target_pairs={{0,1},{1,2},{2,3},{3,0},{4,5},{5,6},{6,7},{7,4},{8,9},{9,10},{10,1... | collective-permute-start | bytes 1622024 | tf_op jit(solution)/shard_map/ppermute | solution.py:375
  150.2 4.7 %copy-start.10 = (bf16[64,4224]{1,0:T(8,128)(2,1)}, bf16[64,4224]{1,0:T(8,128)(2,1)S(1)}, u32[]{:S(2)}) copy-start(bf16[64,4224]{1,0:T(8,128)(2,1)S(1)} %collective-permute-done.12.bottom) | copy-start | bytes 1622020
  154.9 0.8 copy-start.11
  155.7 5.7 %copy-start.2 = (bf16[128,128]{1,0:T(8,128)(2,1)S(1)}, bf16[128,128]{1,0:T(8,128)(2,1)}, u32[]{:S(2)}) copy-start(bf16[128,128]{1,0:T(8,128)(2,1)} %get-tuple-element.31.hit0) | copy-start | bytes 98308
  155.7 5.7 %copy-start.3 = (bf16[128,128]{1,0:T(8,128)(2,1)S(1)}, bf16[128,128]{1,0:T(8,128)(2,1)}, u32[]{:S(2)}) copy-start(bf16[128,128]{1,0:T(8,128)(2,1)} %get-tuple-element.32.hit1) | copy-start | bytes 98308
  161.4 13.2 %copy-start.1 = (bf16[2048,128]{1,0:T(8,128)(2,1)S(1)}, bf16[2048,128]{1,0:T(8,128)(2,1)}, u32[]{:S(2)}) copy-start(bf16[2048,128]{1,0:T(8,128)(2,1)} %router.3) | copy-start | bytes 1572868
  161.4 13.2 %copy-start.4 = (f32[8,128]{1,0:T(8,128)S(1)}, f32[8,128]{1,0:T(8,128)}, u32[]{:S(2)}) copy-start(f32[8,128]{1,0:T(8,128)} %get-tuple-element.37.stats) | copy-start | bytes 12292
  161.5 13.2 %copy-start.5 = (s32[128,2]{0,1:T(2,128)S(1)}, s32[128,2]{0,1:T(2,128)}, u32[]{:S(2)}) copy-start(s32[128,2]{0,1:T(2,128)} %param.9) | copy-start | bytes 3076

commit v8 on v7

--- a/solution.py
+++ b/solution.py
@@ -57,10 +57,6 @@
     return jnp.concatenate(
         [scratch[c, pl.ds(u, 128, stride=8), :].astype(BF16) for c in range(scratch.shape[0])], axis=1
     )
-
-
-def every():
-    return (iota((SENT, 128), 0) // 8 == iota((SENT, 128), 1)).astype(BF16)
 
 
 ON_CHIP = pl.BlockSpec(memory_space=pltpu.VMEM)
@@ -138,14 +134,13 @@
     any_hit = (hits[0] + hits[1]).astype(BF16)
     toks = dot(any_hit, tok[...])
     cots = dot(any_hit, cot[...])
-    send[:, 0 : 2 * CH] = spread(
+    send[...] = spread(
         scratch,
         [
-            jnp.concatenate([x[:, CH * u : CH * (u + 1)] for x in (toks, cots)], axis=1)
+            jnp.concatenate([*(x[:, CH * u : CH * (u + 1)] for x in (toks, cots)), info], axis=1)
             for u in range(8)
         ],
     )
-    send[:, 2 * CH :] = dot(every(), info.astype(BF16)).astype(BF16)
     stats[...] = jnp.concatenate(
         [s[0], s[1], total, g[0], g[1], total, total, total], axis=0
     )
@@ -247,13 +242,17 @@
     mix_lo = (mix - mix_hi.astype(F32)).astype(BF16)
     router = dot(pair[:, 0:D], jnp.concatenate([mix_hi, mix_lo], axis=1), 0, 0)
     router = (router[:, 0:EXPERTS] + router[:, EXPERTS:]).reshape(128, 2, 8, EXPERTS)
-    send[:, 0:CH] = spread(scratch, [term[:, CH * u : CH * (u + 1)] for u in range(8)])
     for h in range(2):
         send[:, CH + 128 * h : CH + 128 * (h + 1)] = router[:, h].reshape(SENT, EXPERTS).astype(BF16)
     tail = jnp.zeros((128, 128), F32)
     for c, v in enumerate(pieces(gg)):
         tail = jnp.where(lane == c, v, tail)
-    send[:, 2 * CH :] = dot(every(), tail.astype(BF16)).astype(BF16)
+    rows = spread(
+        scratch,
+        [jnp.concatenate([term[:, CH * u : CH * (u + 1)], tail], axis=1) for u in range(8)],
+    )
+    send[:, 0:CH] = rows[:, 0:CH]
+    send[:, 2 * CH :] = rows[:, CH:]
 
 
 def row_sums(x):
@@ -394,7 +393,7 @@
             hbm((EXPERTS, TOK), BF16),
             hbm((8, TOK), F32),
         ),
-        (pltpu.VMEM((2 * CH // 128, SENT, 128), F32),),
+        (pltpu.VMEM((2 * CH // 128 + 1, SENT, 128), F32),),
     )
     got = lax.all_to_all(send.reshape(EXPERTS, 8, 2 * CH + 128), EP, 0, 0, tiled=True)
     (pair,) = call(
@@ -426,7 +425,7 @@
         (pair, *((far(x), in_place) for x in (gate_2, up_2, down_2)), back, gg),
         (hbm((SENT, 2 * CH + 128), BF16),),
         (
-            pltpu.VMEM((CH // 128, SENT, 128), F32),
+            pltpu.VMEM((CH // 128 + 1, SENT, 128), F32),
             pltpu.VMEM((D, 2 * FQ), BF16),
             pltpu.VMEM((FQ, D), BF16),
             pltpu.SemaphoreType.DMA((3,)),

time: 177 us -> 177 us (level)
  no operation moved by 1% of the time
where the time goes in v8:
time: 177 us; the launch traced here: 176 us
  starting transfers between devices  72.1 us (41%)
  waiting for transfers between devices  63.7 us (36%)
  Pallas kernels  26.3 us (15%)
  blocking collectives  12.1 us (7%)
    ppermute x13, waiting for transfers between devices, shift(): return lax.ppermute(x, 'tp', [(a, (a + d) % TP) for a in range(TP)])  63.7 us
    ppermute x13, starting transfers between devices, shift(): return lax.ppermute(x, 'tp', [(a, (a + d) % TP) for a in range(TP)])  40.8 us
    pallas_call x8, Pallas kernels, call(): pl.pallas_call(kernel, grid_spec=pltpu.PrefetchScalarGridSpec(num_scalar_...  26.3 us
    all_to_all x1, starting transfers between devices, layer(): lax.all_to_all(send.reshape(EXPERTS, 8, 2 * CH + 128), EP, 0, 0, tiled=True)  17.5 us
    all_to_all x1, starting transfers between devices, layer(): lax.all_to_all(send_back.reshape(EXPERTS, 8, 2 * CH + 128), EP, 0, 0, til...  13.7 us
    all_to_all x1, blocking collectives, layer(): parts = lax.all_to_all(parts, 'tp', 0, 0, tiled=True)  12.1 us
  transfers between devices with their start and end apart: 15, of which 8 were waited for; matrix products, arithmetic and copies ran while one was open for 0% of the time, Pallas kernels for 9%

profile of v8, /device:TPU:8, one launch (start us, length us, event | category | flops | bytes accessed | tf_op | source)
XLA Modules:
  0.0 176.2 jit_solution(16494309204837988202)
XLA Ops:
  0.7 4.0 %shard_map.142 = (bf16[1024,640]{1,0:T(8,128)(2,1)}, bf16[128,128]{1,0:T(8,128)(2,1)}, bf16[128,128]{1,0:T(8,128)(2,1)}, f32[8,128]{1,0:T(8,128)}) custom-call(s32[2]{0:T(128)S(1)} %pad_add_fusion.sc, bf16[128,2048]{1,0:T(8,128)(2,1)} %tok.1, bf16[128,2048]{1,0:T(8,128)(2,1)} %cot.1, s32[2,128]{1,0:T(2,128)} %bitcast.18, bf16[2048,128]{1,0:T(8,128)(2,1)} %router.3), custom_call_target="tpu_custom_call" | custom-call | tf_op jit(solution)/shard_map/pallas_call | solution.py:75
  4.8 17.5 %all-to-all-start = ((bf16[128,8,640]{2,1,0:T(8,128)(2,1)}), bf16[128,8,640]{2,1,0:T(8,128)(2,1)S(1)}, u32[]{:S(2)}, u32[]{:S(2)}) async-start(bf16[128,8,640]{2,1,0:T(8,128)(2,1)} %bitcast.31), calls=%async_computation | async-start | bytes 2621440 | tf_op jit(solution)/shard_map/all_to_all | solution.py:398
  22.3 4.7 %collective-permute-start.6 = (bf16[2048,128]{1,0:T(8,128)(2,1)S(1)}, bf16[2048,128]{1,0:T(8,128)(2,1)S(1)}, u32[]{:S(2)}, u32[]{:S(2)}) collective-permute-start(bf16[2048,128]{1,0:T(8,128)(2,1)S(1)} %bitcast.24), channel_id=1, source_target_pairs={{0,3},{1,0},{2,1},{3,2},{4,7},{5,4},{6,5},{7,6},{8,11},{9,8},{10,9... | collective-permute-start | bytes 1572872 | tf_op jit(solution)/shard_map/ppermute | solution.py:374
  27.0 1.9 %collective-permute-start = (bf16[2048,128]{1,0:T(8,128)(2,1)S(1)}, bf16[2048,128]{1,0:T(8,128)(2,1)}, u32[]{:S(2)}, u32[]{:S(2)}) collective-permute-start(bf16[2048,128]{1,0:T(8,128)(2,1)S(1)} %bitcast.25), channel_id=1, source_target_pairs={{0,1},{1,2},{2,3},{3,0},{4,5},{5,6},{6,7},{7,4},{8,9},{9,10},{10,1... | collective-permute-start | bytes 1572872 | tf_op jit(solution)/shard_map/ppermute | solution.py:374
  28.9 2.7 %collective-permute-start.2 = (bf16[2048,128]{1,0:T(8,128)(2,1)S(1)}, bf16[2048,128]{1,0:T(8,128)(2,1)}, u32[]{:S(2)}, u32[]{:S(2)}) collective-permute-start(bf16[2048,128]{1,0:T(8,128)(2,1)S(1)} %bitcast.29), channel_id=1, source_target_pairs={{0,1},{1,2},{2,3},{3,0},{4,5},{5,6},{6,7},{7,4},{8,9},{9,10},{10,1... | collective-permute-start | bytes 1572872 | tf_op jit(solution)/shard_map/ppermute | solution.py:374
  31.6 4.4 %collective-permute-start.4 = (bf16[128,2048]{1,0:T(8,128)(2,1)}, bf16[128,2048]{1,0:T(8,128)(2,1)}, u32[]{:S(2)}, u32[]{:S(2)}) collective-permute-start(bf16[128,2048]{1,0:T(8,128)(2,1)} %bitcast.7.refs_2_.down.down_w), channel_id=1, source_target_pairs={{0,3},{1,0},{2,1},{3,2},{4,7},{5,4},{6,5},{7,6},{8,11},{9,8},{10,9... | collective-permute-start | bytes 1572872 | tf_op jit(solution)/shard_map/ppermute | solution.py:374
  36.0 3.9 %collective-permute-start.7 = (bf16[2048,128]{1,0:T(8,128)(2,1)S(1)}, bf16[2048,128]{1,0:T(8,128)(2,1)}, u32[]{:S(2)}, u32[]{:S(2)}) collective-permute-start(bf16[2048,128]{1,0:T(8,128)(2,1)S(1)} %bitcast.30), channel_id=1, source_target_pairs={{0,3},{1,0},{2,1},{3,2},{4,7},{5,4},{6,5},{7,6},{8,11},{9,8},{10,9... | collective-permute-start | bytes 1572872 | tf_op jit(solution)/shard_map/ppermute | solution.py:374
  39.9 2.4 %collective-permute-start.8 = (bf16[128,2048]{1,0:T(8,128)(2,1)}, bf16[128,2048]{1,0:T(8,128)(2,1)}, u32[]{:S(2)}, u32[]{:S(2)}) collective-permute-start(bf16[128,2048]{1,0:T(8,128)(2,1)} %bitcast.7.refs_2_.down.down_w), channel_id=1, source_target_pairs={{0,1},{1,2},{2,3},{3,0},{4,5},{5,6},{6,7},{7,4},{8,9},{9,10},{10,1... | collective-permute-start | bytes 1572872 | tf_op jit(solution)/shard_map/ppermute | solution.py:374
  42.4 2.6 %collective-permute-done.refs_6_ = bf16[2048,128]{1,0:T(8,128)(2,1)} collective-permute-done((bf16[2048,128]{1,0:T(8,128)(2,1)S(1)}, bf16[2048,128]{1,0:T(8,128)(2,1)}, u32[]{:S(2)}, u32[]{:S(2)}) %collective-permute-start) | collective-permute-done | bytes 524320 | tf_op jit(solution)/shard_map/ppermute | solution.py:374
  45.0 1.9 %collective-permute-start.1 = (bf16[2048,128]{1,0:T(8,128)(2,1)}, bf16[2048,128]{1,0:T(8,128)(2,1)}, u32[]{:S(2)}, u32[]{:S(2)}) collective-permute-start(bf16[2048,128]{1,0:T(8,128)(2,1)} %collective-permute-done.refs_6_), channel_id=1, source_target_pairs={{0,1},{1,2},{2,3},{3,0},{4,5},{5,6},{6,7},{7,4},{8,9},{9,10},{10,1... | collective-permute-start | bytes 1572872 | tf_op jit(solution)/shard_map/ppermute | solution.py:374
  46.9 9.3 %collective-permute-done.2.refs_7_ = bf16[2048,128]{1,0:T(8,128)(2,1)} collective-permute-done((bf16[2048,128]{1,0:T(8,128)(2,1)S(1)}, bf16[2048,128]{1,0:T(8,128)(2,1)}, u32[]{:S(2)}, u32[]{:S(2)}) %collective-permute-start.2) | collective-permute-done | bytes 524320 | tf_op jit(solution)/shard_map/ppermute | solution.py:374
  56.2 1.9 %collective-permute-start.3 = (bf16[2048,128]{1,0:T(8,128)(2,1)}, bf16[2048,128]{1,0:T(8,128)(2,1)}, u32[]{:S(2)}, u32[]{:S(2)}) collective-permute-start(bf16[2048,128]{1,0:T(8,128)(2,1)} %collective-permute-done.2.refs_7_), channel_id=1, source_target_pairs={{0,1},{1,2},{2,3},{3,0},{4,5},{5,6},{6,7},{7,4},{8,9},{9,10},{10,1... | collective-permute-start | bytes 1572872 | tf_op jit(solution)/shard_map/ppermute | solution.py:374
  58.1 5.1 %collective-permute-start.5 = (bf16[128,2048]{1,0:T(8,128)(2,1)}, bf16[128,2048]{1,0:T(8,128)(2,1)}, u32[]{:S(2)}, u32[]{:S(2)}) collective-permute-start(bf16[128,2048]{1,0:T(8,128)(2,1)} %collective-permute-done.4.refs_5_), channel_id=1, source_target_pairs={{0,3},{1,0},{2,1},{3,2},{4,7},{5,4},{6,5},{7,6},{8,11},{9,8},{10,9... | collective-permute-start | bytes 1572872 | tf_op jit(solution)/shard_map/ppermute | solution.py:374
  63.3 1.2 shard_map.143.pair
  64.5 2.9 %collective-permute-done.8.refs_8_ = bf16[128,2048]{1,0:T(8,128)(2,1)} collective-permute-done((bf16[128,2048]{1,0:T(8,128)(2,1)}, bf16[128,2048]{1,0:T(8,128)(2,1)}, u32[]{:S(2)}, u32[]{:S(2)}) %collective-permute-start.8) | collective-permute-done | bytes 524320 | tf_op jit(solution)/shard_map/ppermute | solution.py:374
  67.4 4.3 %shard_map.144 = (bf16[128,384]{1,0:T(8,128)(2,1)}, f32[128,2048]{1,0:T(8,128)S(1)}, f32[128,128]{1,0:T(8,128)S(1)}) custom-call(s32[2]{0:T(128)S(1)} %pad_add_fusion.sc, bf16[128,4224]{1,0:T(8,128)(2,1)S(1)} %shard_map.143.pair, bf16[2048,128]{1,0:T(8,128)(2,1)} %bitcast.21, bf16[2048,128]{1,0:T(8,128)(2,1)} %bitcast.26, ...), custom_call_target="tpu_custom_call" | custom-call | tf_op jit(solution)/shard_map/pallas_call | solution.py:75
  71.8 6.9 %collective-permute-done.1.gate = bf16[2048,128]{1,0:T(8,128)(2,1)} collective-permute-done((bf16[2048,128]{1,0:T(8,128)(2,1)}, bf16[2048,128]{1,0:T(8,128)(2,1)}, u32[]{:S(2)}, u32[]{:S(2)}) %collective-permute-start.1) | collective-permute-done | bytes 524320 | tf_op jit(solution)/shard_map/ppermute | solution.py:374
  78.7 10.1 %collective-permute-done.3.up = bf16[2048,128]{1,0:T(8,128)(2,1)} collective-permute-done((bf16[2048,128]{1,0:T(8,128)(2,1)}, bf16[2048,128]{1,0:T(8,128)(2,1)}, u32[]{:S(2)}, u32[]{:S(2)}) %collective-permute-start.3) | collective-permute-done | bytes 524320 | tf_op jit(solution)/shard_map/ppermute | solution.py:374
  88.8 4.6 %shard_map.145 = bf16[1024,640]{1,0:T(8,128)(2,1)} custom-call(s32[2]{0:T(128)S(1)} %pad_add_fusion.sc, bf16[128,4224]{1,0:T(8,128)(2,1)S(1)} %shard_map.143.pair, bf16[2048,128]{1,0:T(8,128)(2,1)} %collective-permute-done.1.gate, bf16[2048,128]{1,0:T(8,128)(2,1)} %collective-permute-done.3.up, bf16[128,2048]{1,0:T(8,128)(2,1)} %collective-permute-done.5.down, ...), custom_call_target="tpu_custom_call" | custom-call | tf_op jit(solution)/shard_map/pallas_call | solution.py:75
  93.4 13.7 %all-to-all-start.1 = ((bf16[128,8,640]{2,1,0:T(8,128)(2,1)}), bf16[128,8,640]{2,1,0:T(8,128)(2,1)S(1)}, u32[]{:S(2)}, u32[]{:S(2)}) async-start(bf16[128,8,640]{2,1,0:T(8,128)(2,1)} %bitcast.20), calls=%async_computation.1 | async-start | bytes 2621440 | tf_op jit(solution)/shard_map/all_to_all | solution.py:434
  107.2 1.9 %collective-permute-start.11 = (bf16[128,4224]{1,0:T(8,128)(2,1)S(1)}, bf16[128,4224]{1,0:T(8,128)(2,1)S(1)}, u32[]{:S(2)}, u32[]{:S(2)}) collective-permute-start(bf16[128,4224]{1,0:T(8,128)(2,1)S(1)} %shard_map.143.pair), channel_id=1, source_target_pairs={{0,3},{1,0},{2,1},{3,2},{4,7},{5,4},{6,5},{7,6},{8,11},{9,8},{10,9... | collective-permute-start | bytes 3244040 | tf_op jit(solution)/shard_map/ppermute | solution.py:374
  109.1 3.9 %collective-permute-start.9 = (bf16[128,4224]{1,0:T(8,128)(2,1)S(1)}, bf16[128,4224]{1,0:T(8,128)(2,1)S(1)}, u32[]{:S(2)}, u32[]{:S(2)}) collective-permute-start(bf16[128,4224]{1,0:T(8,128)(2,1)S(1)} %shard_map.143.pair), channel_id=1, source_target_pairs={{0,1},{1,2},{2,3},{3,0},{4,5},{5,6},{6,7},{7,4},{8,9},{9,10},{10,1... | collective-permute-start | bytes 3244040 | tf_op jit(solution)/shard_map/ppermute | solution.py:374
  113.0 21.9 %collective-permute-done.11.pair_3 = bf16[128,4224]{1,0:T(8,128)(2,1)S(1)} collective-permute-done((bf16[128,4224]{1,0:T(8,128)(2,1)S(1)}, bf16[128,4224]{1,0:T(8,128)(2,1)S(1)}, u32[]{:S(2)}, u32[]{:S(2)}) %collective-permute-start.11) | collective-permute-done | bytes 1081376 | tf_op jit(solution)/shard_map/ppermute | solution.py:374
  135.0 3.4 %collective-permute-start.12 = (bf16[64,4224]{1,0:T(8,128)(2,1)S(1)}, bf16[64,4224]{1,0:T(8,128)(2,1)S(1)}, u32[]{:S(2)}, u32[]{:S(2)}) collective-permute-start(bf16[64,4224]{1,0:T(8,128)(2,1)S(1)} %slice.9), channel_id=1, source_target_pairs={{0,3},{1,0},{2,1},{3,2},{4,7},{5,4},{6,5},{7,6},{8,11},{9,8},{10,9... | collective-permute-start | bytes 1622024 | tf_op jit(solution)/shard_map/ppermute | solution.py:374
  138.5 2.6 %collective-permute-start.10 = (bf16[64,4224]{1,0:T(8,128)(2,1)S(1)}, bf16[64,4224]{1,0:T(8,128)(2,1)S(1)}, u32[]{:S(2)}, u32[]{:S(2)}) collective-permute-start(bf16[64,4224]{1,0:T(8,128)(2,1)S(1)} %slice.8), channel_id=1, source_target_pairs={{0,1},{1,2},{2,3},{3,0},{4,5},{5,6},{6,7},{7,4},{8,9},{9,10},{10,1... | collective-permute-start | bytes 1622024 | tf_op jit(solution)/shard_map/ppermute | solution.py:374
  141.1 3.9 %shard_map.146 = (bf16[128,384]{1,0:T(8,128)(2,1)}, bf16[128,384]{1,0:T(8,128)(2,1)}) custom-call(s32[2]{0:T(128)S(1)} %pad_add_fusion.sc, bf16[128,4224]{1,0:T(8,128)(2,1)} %copy-done.7, bf16[128,4224]{1,0:T(8,128)(2,1)} %copy-done.6, bf16[2048,128]{1,0:T(8,128)(2,1)} %bitcast.22, bf16[2048,128]{1,0:T(8,128)(2,1)} %bitcast.27, ...), custom_call_target="tpu_custom_call" | custom-call | tf_op jit(solution)/shard_map/pallas_call | solution.py:75
  145.0 5.3 %collective-permute-done.12.bottom = bf16[64,4224]{1,0:T(8,128)(2,1)S(1)} collective-permute-done((bf16[64,4224]{1,0:T(8,128)(2,1)S(1)}, bf16[64,4224]{1,0:T(8,128)(2,1)S(1)}, u32[]{:S(2)}, u32[]{:S(2)}) %collective-permute-start.12) | collective-permute-done | bytes 540704 | tf_op jit(solution)/shard_map/ppermute | solution.py:374
  150.3 4.7 %collective-permute-done.10.top = bf16[64,4224]{1,0:T(8,128)(2,1)S(1)} collective-permute-done((bf16[64,4224]{1,0:T(8,128)(2,1)S(1)}, bf16[64,4224]{1,0:T(8,128)(2,1)S(1)}, u32[]{:S(2)}, u32[]{:S(2)}) %collective-permute-start.10) | collective-permute-done | bytes 540704 | tf_op jit(solution)/shard_map/ppermute | solution.py:374
  155.8 5.7 %shard_map.147 = (bf16[2048,128]{1,0:T(8,128)(2,1)}, bf16[2048,128]{1,0:T(8,128)(2,1)}, bf16[128,2048]{1,0:T(8,128)(2,1)}, f32[1,128]{1,0:T(1,128)}, bf16[16,512]{1,0:T(8,128)(2,1)S(1)}) custom-call(s32[2]{0:T(128)S(1)} %pad_add_fusion.sc, bf16[128,4224]{1,0:T(8,128)(2,1)} %copy-done, bf16[128,4224]{1,0:T(8,128)(2,1)} %copy-done.7, ...), custom_call_target="tpu_custom_call" | custom-call | tf_op jit(solution)/shard_map/pallas_call | solution.py:75
  161.6 1.0 shard_map.148
  162.6 12.1 %all_to_all.15.got = bf16[4,160,512]{2,1,0:T(8,128)(2,1)S(1)} all-to-all(bf16[4,160,512]{2,1,0:T(8,128)(2,1)S(1)} %shard_map.148), channel_id=1, replica_groups=mesh['ep_0'=8,'ep_1'=8,'ep_2'=2,'tp'=4] {'tp'}, dimensions={0} | all-to-all | bytes 1310720 | tf_op jit(solution)/shard_map/all_to_all | solution.py:467
  174.8 1.4 shard_map.149
  (36 shorter events, 1.0 us)
Async XLA Ops:
  4.7 17.5 %copy-start.8 = (bf16[1,2048,128]{2,1,0:T(8,128)(2,1)S(1)}, bf16[1,2048,128]{2,1,0:T(8,128)(2,1)}, u32[]{:S(2)}) copy-start(bf16[1,2048,128]{2,1,0:T(8,128)(2,1)} %param.11) | copy-start | bytes 1572868
  4.7 24.1 %copy-start.9 = (bf16[1,2048,128]{2,1,0:T(8,128)(2,1)S(1)}, bf16[1,2048,128]{2,1,0:T(8,128)(2,1)}, u32[]{:S(2)}) copy-start(bf16[1,2048,128]{2,1,0:T(8,128)(2,1)} %param.12) | copy-start | bytes 1572868
  4.8 58.5 %all-to-all-start = ((bf16[128,8,640]{2,1,0:T(8,128)(2,1)}), bf16[128,8,640]{2,1,0:T(8,128)(2,1)S(1)}, u32[]{:S(2)}, u32[]{:S(2)}) async-start(bf16[128,8,640]{2,1,0:T(8,128)(2,1)} %bitcast.31), calls=%async_computation | async-start | bytes 2621440 | tf_op jit(solution)/shard_map/all_to_all | solution.py:398
  22.3 17.6 %collective-permute-start.6 = (bf16[2048,128]{1,0:T(8,128)(2,1)S(1)}, bf16[2048,128]{1,0:T(8,128)(2,1)S(1)}, u32[]{:S(2)}, u32[]{:S(2)}) collective-permute-start(bf16[2048,128]{1,0:T(8,128)(2,1)S(1)} %bitcast.24), channel_id=1, source_target_pairs={{0,3},{1,0},{2,1},{3,2},{4,7},{5,4},{6,5},{7,6},{8,11},{9,8},{10,9... | collective-permute-start | bytes 1572872 | tf_op jit(solution)/shard_map/ppermute | solution.py:374
  27.0 18.0 %collective-permute-start = (bf16[2048,128]{1,0:T(8,128)(2,1)S(1)}, bf16[2048,128]{1,0:T(8,128)(2,1)}, u32[]{:S(2)}, u32[]{:S(2)}) collective-permute-start(bf16[2048,128]{1,0:T(8,128)(2,1)S(1)} %bitcast.25), channel_id=1, source_target_pairs={{0,1},{1,2},{2,3},{3,0},{4,5},{5,6},{6,7},{7,4},{8,9},{9,10},{10,1... | collective-permute-start | bytes 1572872 | tf_op jit(solution)/shard_map/ppermute | solution.py:374
  28.9 27.3 %collective-permute-start.2 = (bf16[2048,128]{1,0:T(8,128)(2,1)S(1)}, bf16[2048,128]{1,0:T(8,128)(2,1)}, u32[]{:S(2)}, u32[]{:S(2)}) collective-permute-start(bf16[2048,128]{1,0:T(8,128)(2,1)S(1)} %bitcast.29), channel_id=1, source_target_pairs={{0,1},{1,2},{2,3},{3,0},{4,5},{5,6},{6,7},{7,4},{8,9},{9,10},{10,1... | collective-permute-start | bytes 1572872 | tf_op jit(solution)/shard_map/ppermute | solution.py:374
  31.6 26.6 %collective-permute-start.4 = (bf16[128,2048]{1,0:T(8,128)(2,1)}, bf16[128,2048]{1,0:T(8,128)(2,1)}, u32[]{:S(2)}, u32[]{:S(2)}) collective-permute-start(bf16[128,2048]{1,0:T(8,128)(2,1)} %bitcast.7.refs_2_.down.down_w), channel_id=1, source_target_pairs={{0,3},{1,0},{2,1},{3,2},{4,7},{5,4},{6,5},{7,6},{8,11},{9,8},{10,9... | collective-permute-start | bytes 1572872 | tf_op jit(solution)/shard_map/ppermute | solution.py:374
  36.0 28.5 %collective-permute-start.7 = (bf16[2048,128]{1,0:T(8,128)(2,1)S(1)}, bf16[2048,128]{1,0:T(8,128)(2,1)}, u32[]{:S(2)}, u32[]{:S(2)}) collective-permute-start(bf16[2048,128]{1,0:T(8,128)(2,1)S(1)} %bitcast.30), channel_id=1, source_target_pairs={{0,3},{1,0},{2,1},{3,2},{4,7},{5,4},{6,5},{7,6},{8,11},{9,8},{10,9... | collective-permute-start | bytes 1572872 | tf_op jit(solution)/shard_map/ppermute | solution.py:374
  39.9 27.5 %copy-start.12 = (bf16[2048,128]{1,0:T(8,128)(2,1)}, bf16[2048,128]{1,0:T(8,128)(2,1)S(1)}, u32[]{:S(2)}) copy-start(bf16[2048,128]{1,0:T(8,128)(2,1)S(1)} %collective-permute-done.6.refs_3_) | copy-start | bytes 1572868
  39.9 27.5 %collective-permute-start.8 = (bf16[128,2048]{1,0:T(8,128)(2,1)}, bf16[128,2048]{1,0:T(8,128)(2,1)}, u32[]{:S(2)}, u32[]{:S(2)}) collective-permute-start(bf16[128,2048]{1,0:T(8,128)(2,1)} %bitcast.7.refs_2_.down.down_w), channel_id=1, source_target_pairs={{0,1},{1,2},{2,3},{3,0},{4,5},{5,6},{6,7},{7,4},{8,9},{9,10},{10,1... | collective-permute-start | bytes 1572872 | tf_op jit(solution)/shard_map/ppermute | solution.py:374
  45.0 33.7 %collective-permute-start.1 = (bf16[2048,128]{1,0:T(8,128)(2,1)}, bf16[2048,128]{1,0:T(8,128)(2,1)}, u32[]{:S(2)}, u32[]{:S(2)}) collective-permute-start(bf16[2048,128]{1,0:T(8,128)(2,1)} %collective-permute-done.refs_6_), channel_id=1, source_target_pairs={{0,1},{1,2},{2,3},{3,0},{4,5},{5,6},{6,7},{7,4},{8,9},{9,10},{10,1... | collective-permute-start | bytes 1572872 | tf_op jit(solution)/shard_map/ppermute | solution.py:374
  56.2 32.6 %collective-permute-start.3 = (bf16[2048,128]{1,0:T(8,128)(2,1)}, bf16[2048,128]{1,0:T(8,128)(2,1)}, u32[]{:S(2)}, u32[]{:S(2)}) collective-permute-start(bf16[2048,128]{1,0:T(8,128)(2,1)} %collective-permute-done.2.refs_7_), channel_id=1, source_target_pairs={{0,1},{1,2},{2,3},{3,0},{4,5},{5,6},{6,7},{7,4},{8,9},{9,10},{10,1... | collective-permute-start | bytes 1572872 | tf_op jit(solution)/shard_map/ppermute | solution.py:374
  58.1 30.7 %collective-permute-start.5 = (bf16[128,2048]{1,0:T(8,128)(2,1)}, bf16[128,2048]{1,0:T(8,128)(2,1)}, u32[]{:S(2)}, u32[]{:S(2)}) collective-permute-start(bf16[128,2048]{1,0:T(8,128)(2,1)} %collective-permute-done.4.refs_5_), channel_id=1, source_target_pairs={{0,3},{1,0},{2,1},{3,2},{4,7},{5,4},{6,5},{7,6},{8,11},{9,8},{10,9... | collective-permute-start | bytes 1572872 | tf_op jit(solution)/shard_map/ppermute | solution.py:374
  64.5 44.6 %copy-start = (bf16[128,4224]{1,0:T(8,128)(2,1)}, bf16[128,4224]{1,0:T(8,128)(2,1)S(1)}, u32[]{:S(2)}) copy-start(bf16[128,4224]{1,0:T(8,128)(2,1)S(1)} %shard_map.143.pair) | copy-start | bytes 3244036
  93.4 68.1 %all-to-all-start.1 = ((bf16[128,8,640]{2,1,0:T(8,128)(2,1)}), bf16[128,8,640]{2,1,0:T(8,128)(2,1)S(1)}, u32[]{:S(2)}, u32[]{:S(2)}) async-start(bf16[128,8,640]{2,1,0:T(8,128)(2,1)} %bitcast.20), calls=%async_computation.1 | async-start | bytes 2621440 | tf_op jit(solution)/shard_map/all_to_all | solution.py:434
  107.2 27.8 %collective-permute-start.11 = (bf16[128,4224]{1,0:T(8,128)(2,1)S(1)}, bf16[128,4224]{1,0:T(8,128)(2,1)S(1)}, u32[]{:S(2)}, u32[]{:S(2)}) collective-permute-start(bf16[128,4224]{1,0:T(8,128)(2,1)S(1)} %shard_map.143.pair), channel_id=1, source_target_pairs={{0,3},{1,0},{2,1},{3,2},{4,7},{5,4},{6,5},{7,6},{8,11},{9,8},{10,9... | collective-permute-start | bytes 3244040 | tf_op jit(solution)/shard_map/ppermute | solution.py:374
  109.1 29.3 %collective-permute-start.9 = (bf16[128,4224]{1,0:T(8,128)(2,1)S(1)}, bf16[128,4224]{1,0:T(8,128)(2,1)S(1)}, u32[]{:S(2)}, u32[]{:S(2)}) collective-permute-start(bf16[128,4224]{1,0:T(8,128)(2,1)S(1)} %shard_map.143.pair), channel_id=1, source_target_pairs={{0,1},{1,2},{2,3},{3,0},{4,5},{5,6},{6,7},{7,4},{8,9},{9,10},{10,1... | collective-permute-start | bytes 3244040 | tf_op jit(solution)/shard_map/ppermute | solution.py:374
  134.9 6.2 %copy-start.6 = (bf16[128,4224]{1,0:T(8,128)(2,1)}, bf16[128,4224]{1,0:T(8,128)(2,1)S(1)}, u32[]{:S(2)}) copy-start(bf16[128,4224]{1,0:T(8,128)(2,1)S(1)} %collective-permute-done.11.pair_3) | copy-start | bytes 3244036
  135.0 15.3 %collective-permute-start.12 = (bf16[64,4224]{1,0:T(8,128)(2,1)S(1)}, bf16[64,4224]{1,0:T(8,128)(2,1)S(1)}, u32[]{:S(2)}, u32[]{:S(2)}) collective-permute-start(bf16[64,4224]{1,0:T(8,128)(2,1)S(1)} %slice.9), channel_id=1, source_target_pairs={{0,3},{1,0},{2,1},{3,2},{4,7},{5,4},{6,5},{7,6},{8,11},{9,8},{10,9... | collective-permute-start | bytes 1622024 | tf_op jit(solution)/shard_map/ppermute | solution.py:374
  138.4 2.7 %copy-start.7 = (bf16[128,4224]{1,0:T(8,128)(2,1)}, bf16[128,4224]{1,0:T(8,128)(2,1)S(1)}, u32[]{:S(2)}) copy-start(bf16[128,4224]{1,0:T(8,128)(2,1)S(1)} %collective-permute-done.9.pair_1) | copy-start | bytes 3244036
  138.5 16.5 %collective-permute-start.10 = (bf16[64,4224]{1,0:T(8,128)(2,1)S(1)}, bf16[64,4224]{1,0:T(8,128)(2,1)S(1)}, u32[]{:S(2)}, u32[]{:S(2)}) collective-permute-start(bf16[64,4224]{1,0:T(8,128)(2,1)S(1)} %slice.8), channel_id=1, source_target_pairs={{0,1},{1,2},{2,3},{3,0},{4,5},{5,6},{6,7},{7,4},{8,9},{9,10},{10,1... | collective-permute-start | bytes 1622024 | tf_op jit(solution)/shard_map/ppermute | solution.py:374
  150.3 4.7 %copy-start.10 = (bf16[64,4224]{1,0:T(8,128)(2,1)}, bf16[64,4224]{1,0:T(8,128)(2,1)S(1)}, u32[]{:S(2)}) copy-start(bf16[64,4224]{1,0:T(8,128)(2,1)S(1)} %collective-permute-done.12.bottom) | copy-start | bytes 1622020
  155.0 0.8 copy-start.11
  155.8 5.7 %copy-start.2 = (bf16[128,128]{1,0:T(8,128)(2,1)S(1)}, bf16[128,128]{1,0:T(8,128)(2,1)}, u32[]{:S(2)}) copy-start(bf16[128,128]{1,0:T(8,128)(2,1)} %get-tuple-element.31.hit0) | copy-start | bytes 98308
  155.8 5.7 %copy-start.3 = (bf16[128,128]{1,0:T(8,128)(2,1)S(1)}, bf16[128,128]{1,0:T(8,128)(2,1)}, u32[]{:S(2)}) copy-start(bf16[128,128]{1,0:T(8,128)(2,1)} %get-tuple-element.32.hit1) | copy-start | bytes 98308
  161.6 13.2 %copy-start.1 = (bf16[2048,128]{1,0:T(8,128)(2,1)S(1)}, bf16[2048,128]{1,0:T(8,128)(2,1)}, u32[]{:S(2)}) copy-start(bf16[2048,128]{1,0:T(8,128)(2,1)} %router.3) | copy-start | bytes 1572868
  161.6 13.2 %copy-start.4 = (f32[8,128]{1,0:T(8,128)S(1)}, f32[8,128]{1,0:T(8,128)}, u32[]{:S(2)}) copy-start(f32[8,128]{1,0:T(8,128)} %get-tuple-element.37.stats) | copy-start | bytes 12292
  161.6 13.2 %copy-start.5 = (s32[128,2]{0,1:T(2,128)S(1)}, s32[128,2]{0,1:T(2,128)}, u32[]{:S(2)}) copy-start(s32[128,2]{0,1:T(2,128)} %param.9) | copy-start | bytes 3076
